TPU v7x, 512 devices: a whole 4x4x16 slice. The times are simulated.
512 devices in a mesh: fs: 16 (over y, x), tp: 32 (over z, core).
Axes of the slice: x: 4, y: 4, z: 16, core: 2. Of those that a mesh axis runs over, the one named last changes fastest.
Arguments:
- tokens: bfloat16 [8192, 2048], P('fs', 'tp'), may hold values from -6 to 6
- norm_gain: float32 [2048], P('fs'), may hold values from 0.1 to 1.9
- gate_train: float32 [2048, 8192], P('fs', 'tp'), may hold values from -0.125 to 0.125
- up_train: float32 [2048, 8192], P('fs', 'tp'), may hold values from -0.125 to 0.125
- down_train: float32 [8192, 2048], P('fs', 'tp'), may hold values from -0.0625 to 0.0625
Outputs:
- gate_serve: bfloat16 [2048, 8192], P(None, 'tp')
- up_serve: bfloat16 [2048, 8192], P(None, 'tp')
- down_serve: bfloat16 [8192, 2048], P('tp')
- layer_out: bfloat16 [8192, 2048], P(('fs', 'tp'))
All inputs are finite; a program needn't handle non-finite values.
Results may differ from a plain program's by a relative error of at most 0.024.
Values may be sent and summed in bfloat16 or wider, within the bound.
No kernel may reach another device: no remote copies, remote signals or barrier semaphores. Data moves between devices by JAX's collectives and lax.ppermute only.
A program may use at most 64 MiB of HBM per device.

v0:
```python
import jax
import jax.numpy as jnp
from jax import lax
from jax.sharding import Mesh
from jax.sharding import PartitionSpec as P


D = 2048
TP = ("zh", "zl", "c")
FS_TP = ("fs", "zh", "zl", "c")
EPS = 1e-06
BF = jnp.bfloat16
F32 = jnp.float32
EVERY = [(a, b) for a in range(16) for b in range(16)]


def pick(x, i, dim):
    return lax.dynamic_index_in_dim(x, i, dim, keepdims=False, allow_negative_indices=False)


def part_of(x, at, size, dim):
    return lax.dynamic_slice_in_dim(x, at, size, dim, allow_negative_indices=False)


def put(whole, part, at):
    return lax.dynamic_update_slice(whole, part, at, allow_negative_indices=False)


def shift(x, by):
    return lax.ppermute(x, TP[:2], [(i, (i + by) % 16) for i in range(16)])


def fan(x, by):
    pairs = [(2 * z + c, 2 * ((z + (by, -by)[c]) % 16) + c) for z in range(16) for c in range(2)]
    return lax.ppermute(x, TP, pairs)


def swap(x):
    return lax.ppermute(x, "c", [(0, 1), (1, 0)])


def by_core(c, mine, other, dim):
    return jnp.concatenate([jnp.where(c == 0, mine, other), jnp.where(c == 0, other, mine)], axis=dim)


def gather_tokens(tokens):
    zh, zl, c = (lax.axis_index(a) for a in TP)
    x = tokens.T
    chip = by_core(c, x, swap(x), 0)
    p = fan(chip, 4)
    q = fan(jnp.where(c == 0, chip[:, :256], chip[:, 256:]), 8)
    o = swap(jnp.concatenate([p, q], axis=1))
    own = put(jnp.zeros((4, 128, 512), BF), chip[None], (zh, 0, 0))
    own = put(own, p[None], ((zh + 3 + 2 * c) & 3, 0, 0))
    own = put(own, o[None, :, :512], ((zh + 1 + 2 * c) & 3, 0, 0))
    own = put(own, by_core(c, q, o[:, 512:], 1)[None], ((zh + 2) & 3, 0, 0))
    n = fan(own, 1)
    f = fan(part_of(own, 2 * c, 2, 0), 2)
    o = swap(jnp.concatenate([n, f], axis=0))
    whole = put(jnp.zeros((4, 4, 128, 512), BF), own[:, None], (0, zl, 0, 0))
    whole = put(whole, n[:, None], (0, (zl + 3 + 2 * c) & 3, 0, 0))
    whole = put(whole, f[:, None], (2 * c, (zl + 2) & 3, 0, 0))
    whole = put(whole, o[:4, None], (0, (zl + 1 + 2 * c) & 3, 0, 0))
    whole = put(whole, o[4:, None], (2 - 2 * c, (zl + 2) & 3, 0, 0))
    return whole.reshape(D, 512)


def place_down(down_train):
    c = lax.axis_index("c")
    x = down_train.astype(BF).T
    x = lax.ppermute(x, FS_TP[:3], [(a * 16 + b, (a ^ b) * 16 + b) for a, b in EVERY])
    x = lax.ppermute(x, FS_TP[:3], [((a ^ b) * 16 + b, b * 16 + a) for a, b in EVERY])
    keep, give = jnp.where(c == 0, x[:, :256], x[:, 256:]), jnp.where(c == 0, x[:, 256:], x[:, :256])
    return by_core(c, keep, swap(give), 0)


def scatter_sum(hidden, down):
    _, zl, c = (lax.axis_index(a) for a in TP)
    hidden = hidden.reshape(16, 2, 16, 256)
    across = (((1,), (1,)), ((), ()))
    keep, give = pick(hidden, c, 1).reshape(256, 256), pick(hidden, 1 - c, 1).reshape(256, 256)
    give = lax.dot_general(give, down, across, preferred_element_type=F32).astype(BF)
    got = swap(give)
    pair = lax.dot_general(keep, down, across, preferred_element_type=F32) + got.astype(F32)
    pair = pair.astype(BF).reshape(4, 4, 16, D)
    ahead, behind, far = (pick(pair, (zl + d) & 3, 1) for d in (1, 3, 2))
    near = pick(pair, zl, 1).astype(F32)
    near += shift(ahead, 1).astype(F32) + shift(behind, -1).astype(F32)
    far = jnp.concatenate([shift(far[:2], 2), shift(far[2:], -2)], axis=0)
    near = (near + far.astype(F32)).astype(BF)
    rows = lax.all_to_all(near, "zh", 0, 0, tiled=True)
    return jnp.sum(rows.astype(F32), axis=0).astype(BF)


def body(tokens, norm_gain, gate_train, up_train, down_train):
    gate_local = (norm_gain[:, None] * gate_train).astype(BF)
    up_local = (norm_gain[:, None] * up_train).astype(BF)
    local = jnp.concatenate([gate_local, up_local, place_down(down_train)], axis=1)
    every = lax.all_to_all(jnp.broadcast_to(local, (16, 128, 768)), "fs", 0, 0, tiled=True)
    every = every.reshape(D, 768)
    both, down = every[:, :512], every[:, 512:]
    x = gather_tokens(tokens)
    wide = x.astype(F32)
    scale = lax.rsqrt(jnp.sum(wide * wide, axis=0) / D + EPS)[:, None]
    sums = lax.dot_general(x, both, (((0,), (0,)), ((), ())), preferred_element_type=F32)
    gate, up = sums[:, :256], sums[:, 256:]
    hidden = (jax.nn.silu(gate * scale) * (up * scale)).astype(BF)
    return (both[:, :256], both[:, 256:], down.T, scatter_sum(hidden, down))


def solution(mesh):
    finer = Mesh(mesh.devices.reshape(mesh.shape["fs"], 4, 4, 2), FS_TP)
    placed = (P("fs", TP), P("fs"), P("fs", TP), P("fs", TP), P("fs", TP))
    return jax.shard_map(
        body,
        mesh=finer,
        in_specs=placed,
        out_specs=(P(None, TP), P(None, TP), P(TP, None), P(FS_TP, None)),
        check_vma=False,
    )
```

profile of v0, /device:TPU:64, one launch (start us, length us, event | category | flops | bytes accessed | tf_op | source)
XLA Modules:
  0.0 170.1 jit_solution(8739315897669502732)
XLA Ops:
  0.6 1.9 %collective-permute-start.3 = (bf16[64,512]{1,0:T(8,128)(2,1)}, bf16[64,512]{1,0:T(8,128)(2,1)S(1)}, u32[]{:S(2)}, u32[]{:S(2)}) collective-permute-start(bf16[64,512]{1,0:T(8,128)(2,1)} %bitcast.76), channel_id=1, source_target_pairs={{0,1},{1,0},{2,3},{3,2},{4,5},{5,4},{6,7},{7,6},{8,9},{9,8},{10,11... | collective-permute-start | bytes 196616 | tf_op jit(solution)/shard_map/ppermute | solution.py:39
  2.6 0.9 convert_bitcast_fusion
  3.5 4.9 %collective-permute-start = (bf16[64,512]{1,0:T(8,128)(2,1)S(1)}, bf16[64,512]{1,0:T(8,128)(2,1)S(1)}, u32[]{:S(2)}, u32[]{:S(2)}) collective-permute-start(bf16[64,512]{1,0:T(8,128)(2,1)S(1)} %convert_bitcast_fusion), channel_id=1, source_target_pairs={{0,0},{2,34},{4,68},{6,102},{8,136},{10,170},{12,204},{14,238},{16... | collective-permute-start | bytes 196616 | tf_op jit(solution)/shard_map/ppermute | solution.py:71
  8.4 1.1 multiply_convert_fusion.1
  9.5 0.0 collective-permute-done.3
  9.5 0.9 broadcast_select_fusion.3
  10.4 1.0 collective-permute-done
  11.4 4.9 %collective-permute-start.1 = (bf16[64,512]{1,0:T(8,128)(2,1)S(1)}, bf16[64,512]{1,0:T(8,128)(2,1)S(1)}, u32[]{:S(2)}, u32[]{:S(2)}) collective-permute-start(bf16[64,512]{1,0:T(8,128)(2,1)S(1)} %collective-permute-done), channel_id=1, source_target_pairs={{0,0},{34,32},{68,64},{102,96},{136,128},{170,160},{204,192},{238,... | collective-permute-start | bytes 196616 | tf_op jit(solution)/shard_map/ppermute | solution.py:72
  16.4 4.5 %collective-permute-done.1 = bf16[64,512]{1,0:T(8,128)(2,1)S(1)} collective-permute-done((bf16[64,512]{1,0:T(8,128)(2,1)S(1)}, bf16[64,512]{1,0:T(8,128)(2,1)S(1)}, u32[]{:S(2)}, u32[]{:S(2)}) %collective-permute-start.1) | collective-permute-done | bytes 65568 | tf_op jit(solution)/shard_map/ppermute | solution.py:72
  20.9 1.9 %collective-permute-start.2 = (bf16[64,256]{1,0:T(8,128)(2,1)S(1)}, bf16[64,256]{1,0:T(8,128)(2,1)S(1)}, u32[]{:S(2)}, u32[]{:S(2)}) collective-permute-start(bf16[64,256]{1,0:T(8,128)(2,1)S(1)} %broadcast_select_fusion.6), channel_id=1, source_target_pairs={{0,1},{1,0},{2,3},{3,2},{4,5},{5,4},{6,7},{7,6},{8,9},{9,8},{10,11... | collective-permute-start | bytes 98312 | tf_op jit(solution)/shard_map/ppermute | solution.py:39
  22.9 15.7 %collective-permute-start.4 = (bf16[128,512]{1,0:T(8,128)(2,1)S(1)}, bf16[128,512]{1,0:T(8,128)(2,1)S(1)}, u32[]{:S(2)}, u32[]{:S(2)}) collective-permute-start(bf16[128,512]{1,0:T(8,128)(2,1)S(1)} %pad_maximum_fusion.2), channel_id=1, source_target_pairs={{0,8},{1,25},{2,10},{3,27},{4,12},{5,29},{6,14},{7,31},{8,16},{9,1... | collective-permute-start | bytes 393224 | tf_op jit(solution)/shard_map/ppermute | solution.py:35
  38.6 13.6 %collective-permute-start.5 = (bf16[128,256]{1,0:T(8,128)(2,1)S(1)}, bf16[128,256]{1,0:T(8,128)(2,1)S(1)}, u32[]{:S(2)}, u32[]{:S(2)}) collective-permute-start(bf16[128,256]{1,0:T(8,128)(2,1)S(1)} %fusion.16), channel_id=1, source_target_pairs={{0,16},{1,17},{2,18},{3,19},{4,20},{5,21},{6,22},{7,23},{8,24},{9,... | collective-permute-start | bytes 196616 | tf_op jit(solution)/shard_map/ppermute | solution.py:35
  52.1 0.0 collective-permute-done.2
  52.2 0.2 copy.32
  52.4 2.3 %broadcast_in_dim.39 = bf16[16,128,768]{1,2,0:T(8,128)(2,1)} broadcast(bf16[128,768]{0,1:T(8,128)(2,1)S(1)} %copy.32), dimensions={1,2} | broadcast | bytes 3342336 | tf_op jit(solution)/shard_map/broadcast_in_dim | solution.py:99
  54.6 4.5 %all-to-all-start = ((bf16[16,128,768]{1,2,0:T(8,128)(2,1)}), bf16[16,128,768]{1,2,0:T(8,128)(2,1)}, u32[]{:S(2)}, u32[]{:S(2)}) async-start(bf16[16,128,768]{1,2,0:T(8,128)(2,1)} %broadcast_in_dim.39), calls=%async_computation | async-start | bytes 6291456 | tf_op jit(solution)/shard_map/all_to_all | solution.py:99
  59.2 0.0 collective-permute-done.5
  59.2 0.0 collective-permute-done.4
  59.2 2.1 %collective-permute-start.6 = (bf16[128,768]{1,0:T(8,128)(2,1)S(1)}, bf16[128,768]{1,0:T(8,128)(2,1)S(1)}, u32[]{:S(2)}, u32[]{:S(2)}) collective-permute-start(bf16[128,768]{1,0:T(8,128)(2,1)S(1)} %pad_maximum_fusion.1), channel_id=1, source_target_pairs={{0,1},{1,0},{2,3},{3,2},{4,5},{5,4},{6,7},{7,6},{8,9},{9,8},{10,11... | collective-permute-start | bytes 589832 | tf_op jit(solution)/shard_map/ppermute | solution.py:39
  61.3 1.2 collective-permute-done.6
  62.6 3.2 %collective-permute-start.7 = (bf16[4,128,512]{2,1,0:T(8,128)(2,1)S(1)}, bf16[4,128,512]{2,1,0:T(8,128)(2,1)S(1)}, u32[]{:S(2)}, u32[]{:S(2)}) collective-permute-start(bf16[4,128,512]{2,1,0:T(8,128)(2,1)S(1)} %fusion.14), channel_id=1, source_target_pairs={{0,2},{1,31},{2,4},{3,1},{4,6},{5,3},{6,8},{7,5},{8,10},{9,7},{10,... | collective-permute-start | bytes 1572872 | tf_op jit(solution)/shard_map/ppermute | solution.py:35
  65.9 5.6 %collective-permute-start.8 = (bf16[2,128,512]{2,1,0:T(8,128)(2,1)S(1)}, bf16[2,128,512]{2,1,0:T(8,128)(2,1)S(1)}, u32[]{:S(2)}, u32[]{:S(2)}) collective-permute-start(bf16[2,128,512]{2,1,0:T(8,128)(2,1)S(1)} %constant_dynamic-slice_fusion.2), channel_id=1, source_target_pairs={{0,4},{1,29},{2,6},{3,31},{4,8},{5,1},{6,10},{7,3},{8,12},{9,5},{1... | collective-permute-start | bytes 786440 | tf_op jit(solution)/shard_map/ppermute | solution.py:35
  71.5 3.9 %collective-permute-done.8 = bf16[2,128,512]{2,1,0:T(8,128)(2,1)S(1)} collective-permute-done((bf16[2,128,512]{2,1,0:T(8,128)(2,1)S(1)}, bf16[2,128,512]{2,1,0:T(8,128)(2,1)S(1)}, u32[]{:S(2)}, u32[]{:S(2)}) %collective-permute-start.8) | collective-permute-done | bytes 262176 | tf_op jit(solution)/shard_map/ppermute | solution.py:35
  75.4 1.1 collective-permute-done.7
  76.5 0.1 pad_maximum_fusion
  76.6 5.5 %collective-permute-start.9 = (bf16[6,128,512]{2,1,0:T(8,128)(2,1)S(1)}, bf16[6,128,512]{2,1,0:T(8,128)(2,1)S(1)}, u32[]{:S(2)}, u32[]{:S(2)}) collective-permute-start(bf16[6,128,512]{2,1,0:T(8,128)(2,1)S(1)} %pad_maximum_fusion), channel_id=1, source_target_pairs={{0,1},{1,0},{2,3},{3,2},{4,5},{5,4},{6,7},{7,6},{8,9},{9,8},{10,11... | collective-permute-start | bytes 2359304 | tf_op jit(solution)/shard_map/ppermute | solution.py:39
  82.1 0.2 broadcast_in_dim.40
  82.5 1.5 collective-permute-done.9
  84.1 0.0 copy-start
  84.1 1.4 copy-done
  85.5 0.5 multiply_reduce_fusion
  86.0 22.2 %all-to-all-done = bf16[16,128,768]{1,2,0:T(8,128)(2,1)} async-done(((bf16[16,128,768]{1,2,0:T(8,128)(2,1)}), bf16[16,128,768]{1,2,0:T(8,128)(2,1)}, u32[]{:S(2)}, u32[]{:S(2)}) %all-to-all-start) | async-done | bytes 3145760 | tf_op jit(solution)/shard_map/all_to_all | solution.py:99
  108.2 3.2 %copy.33 = bf16[16,128,768]{2,1,0:T(8,128)(2,1)S(1)} copy(bf16[16,128,768]{1,2,0:T(8,128)(2,1)} %all-to-all-done) | data formatting | bytes 6291456 | tf_op jit(solution)/shard_map/all_to_all | solution.py:99
  111.4 2.9 %fusion = f32[512,512]{1,0:T(8,128)S(1)} fusion(bf16[2048,512]{1,0:T(8,128)(2,1)} %bitcast.69, bf16[2048,768]{1,0:T(8,128)(2,1)S(1)} %bitcast.65), kind=kOutput, calls=%fused_computation.2 | convolution fusion | flops 1073741824 | bytes 5242880 | tf_op jit(solution)/shard_map/dot_general | solution.py:105
  114.2 0.2 fusion.8
  114.5 1.4 convolution_convert_fusion
  115.9 1.9 %collective-permute-start.10 = (bf16[256,2048]{1,0:T(8,128)(2,1)}, bf16[256,2048]{1,0:T(8,128)(2,1)}, u32[]{:S(2)}, u32[]{:S(2)}) collective-permute-start(bf16[256,2048]{1,0:T(8,128)(2,1)} %convolution_convert_fusion), channel_id=1, source_target_pairs={{0,1},{1,0},{2,3},{3,2},{4,5},{5,4},{6,7},{7,6},{8,9},{9,8},{10,11... | collective-permute-start | bytes 3145736 | tf_op jit(solution)/shard_map/ppermute | solution.py:39
  117.9 3.0 %collective-permute-done.10 = bf16[256,2048]{1,0:T(8,128)(2,1)} collective-permute-done((bf16[256,2048]{1,0:T(8,128)(2,1)}, bf16[256,2048]{1,0:T(8,128)(2,1)}, u32[]{:S(2)}, u32[]{:S(2)}) %collective-permute-start.10) | collective-permute-done | bytes 1048608 | tf_op jit(solution)/shard_map/ppermute | solution.py:39
  120.8 1.7 add_convert_fusion
  122.5 0.1 dynamic-slice_bitcast_fusion
  122.6 3.2 %collective-permute-start.11 = (bf16[4,16,2048]{2,1,0:T(8,128)(2,1)S(1)}, bf16[4,16,2048]{2,1,0:T(8,128)(2,1)S(1)}, u32[]{:S(2)}, u32[]{:S(2)}) collective-permute-start(bf16[4,16,2048]{2,1,0:T(8,128)(2,1)S(1)} %get-tuple-element.25), channel_id=1, source_target_pairs={{0,2},{2,4},{4,6},{6,8},{8,10},{10,12},{12,14},{14,16},{16,18},{18... | collective-permute-start | bytes 786440 | tf_op jit(solution)/shard_map/ppermute | solution.py:30
  125.8 2.7 %collective-permute-start.12 = (bf16[4,16,2048]{2,1,0:T(8,128)(2,1)S(1)}, bf16[4,16,2048]{2,1,0:T(8,128)(2,1)S(1)}, u32[]{:S(2)}, u32[]{:S(2)}) collective-permute-start(bf16[4,16,2048]{2,1,0:T(8,128)(2,1)S(1)} %get-tuple-element.24), channel_id=1, source_target_pairs={{0,30},{2,0},{4,2},{6,4},{8,6},{10,8},{12,10},{14,12},{16,14},{18,... | collective-permute-start | bytes 786440 | tf_op jit(solution)/shard_map/ppermute | solution.py:30
  128.5 3.8 %collective-permute-start.13 = (bf16[2,16,2048]{2,1,0:T(8,128)(2,1)S(1)}, bf16[2,16,2048]{2,1,0:T(8,128)(2,1)S(1)}, u32[]{:S(2)}, u32[]{:S(2)}) collective-permute-start(bf16[2,16,2048]{2,1,0:T(8,128)(2,1)S(1)} %slice_bitcast_fusion.3), channel_id=1, source_target_pairs={{0,4},{2,6},{4,8},{6,10},{8,12},{10,14},{12,16},{14,18},{16,20},{1... | collective-permute-start | bytes 393224 | tf_op jit(solution)/shard_map/ppermute | solution.py:30
  132.4 2.9 %collective-permute-start.14 = (bf16[2,16,2048]{2,1,0:T(8,128)(2,1)S(1)}, bf16[2,16,2048]{2,1,0:T(8,128)(2,1)S(1)}, u32[]{:S(2)}, u32[]{:S(2)}) collective-permute-start(bf16[2,16,2048]{2,1,0:T(8,128)(2,1)S(1)} %dynamic-slice_bitcast_fusion.3), channel_id=1, source_target_pairs={{0,28},{2,30},{4,0},{6,2},{8,4},{10,6},{12,8},{14,10},{16,12},{18,... | collective-permute-start | bytes 393224 | tf_op jit(solution)/shard_map/ppermute | solution.py:30
  135.3 1.7 collective-permute-done.13
  136.9 6.3 %collective-permute-done.14 = bf16[2,16,2048]{2,1,0:T(8,128)(2,1)S(1)} collective-permute-done((bf16[2,16,2048]{2,1,0:T(8,128)(2,1)S(1)}, bf16[2,16,2048]{2,1,0:T(8,128)(2,1)S(1)}, u32[]{:S(2)}, u32[]{:S(2)}) %collective-permute-start.14) | collective-permute-done | bytes 131104 | tf_op jit(solution)/shard_map/ppermute | solution.py:30
  143.2 0.0 collective-permute-done.11
  143.2 0.0 collective-permute-done.12
  143.2 0.8 fusion.11
  144.1 5.9 %all-to-all-start.1 = ((bf16[4,16,2048]{2,1,0:T(8,128)(2,1)}), bf16[4,16,2048]{2,1,0:T(8,128)(2,1)S(1)}, u32[]{:S(2)}, u32[]{:S(2)}) async-start(bf16[4,16,2048]{2,1,0:T(8,128)(2,1)} %fusion.11), calls=%async_computation.1 | async-start | bytes 524288 | tf_op jit(solution)/shard_map/all_to_all | solution.py:91
  149.9 1.7 %slice_bitcast_fusion = (bf16[256,2048]{0,1:T(8,128)(2,1)}, bf16[2048,256]{1,0:T(8,128)(2,1)}, bf16[2048,256]{1,0:T(8,128)(2,1)}) fusion(bf16[2048,768]{1,0:T(8,128)(2,1)S(1)} %bitcast.68), kind=kLoop, calls=%fused_computation.8 | loop fusion | bytes 6291456 | tf_op jit(solution)/shard_map/transpose | solution.py:108
  151.6 2.3 %copy.40 = bf16[256,2048]{1,0:T(8,128)(2,1)} copy(bf16[256,2048]{0,1:T(8,128)(2,1)} %get-tuple-element.20) | data formatting | bytes 2097152
  153.9 15.5 %all-to-all-done.1 = bf16[4,16,2048]{2,1,0:T(8,128)(2,1)S(1)} async-done(((bf16[4,16,2048]{2,1,0:T(8,128)(2,1)}), bf16[4,16,2048]{2,1,0:T(8,128)(2,1)S(1)}, u32[]{:S(2)}, u32[]{:S(2)}) %all-to-all-start.1) | async-done | bytes 262176 | tf_op jit(solution)/shard_map/all_to_all | solution.py:91
  169.4 0.7 reduce_sum.22
  (22 shorter events, 0.5 us)
Async XLA Ops:
  0.6 8.9 %collective-permute-start.3 = (bf16[64,512]{1,0:T(8,128)(2,1)}, bf16[64,512]{1,0:T(8,128)(2,1)S(1)}, u32[]{:S(2)}, u32[]{:S(2)}) collective-permute-start(bf16[64,512]{1,0:T(8,128)(2,1)} %bitcast.76), channel_id=1, source_target_pairs={{0,1},{1,0},{2,3},{3,2},{4,5},{5,4},{6,7},{7,6},{8,9},{9,8},{10,11... | collective-permute-start | bytes 196616 | tf_op jit(solution)/shard_map/ppermute | solution.py:39
  3.5 7.9 %collective-permute-start = (bf16[64,512]{1,0:T(8,128)(2,1)S(1)}, bf16[64,512]{1,0:T(8,128)(2,1)S(1)}, u32[]{:S(2)}, u32[]{:S(2)}) collective-permute-start(bf16[64,512]{1,0:T(8,128)(2,1)S(1)} %convert_bitcast_fusion), channel_id=1, source_target_pairs={{0,0},{2,34},{4,68},{6,102},{8,136},{10,170},{12,204},{14,238},{16... | collective-permute-start | bytes 196616 | tf_op jit(solution)/shard_map/ppermute | solution.py:71
  11.4 9.5 %collective-permute-start.1 = (bf16[64,512]{1,0:T(8,128)(2,1)S(1)}, bf16[64,512]{1,0:T(8,128)(2,1)S(1)}, u32[]{:S(2)}, u32[]{:S(2)}) collective-permute-start(bf16[64,512]{1,0:T(8,128)(2,1)S(1)} %collective-permute-done), channel_id=1, source_target_pairs={{0,0},{34,32},{68,64},{102,96},{136,128},{170,160},{204,192},{238,... | collective-permute-start | bytes 196616 | tf_op jit(solution)/shard_map/ppermute | solution.py:72
  20.9 31.2 %collective-permute-start.2 = (bf16[64,256]{1,0:T(8,128)(2,1)S(1)}, bf16[64,256]{1,0:T(8,128)(2,1)S(1)}, u32[]{:S(2)}, u32[]{:S(2)}) collective-permute-start(bf16[64,256]{1,0:T(8,128)(2,1)S(1)} %broadcast_select_fusion.6), channel_id=1, source_target_pairs={{0,1},{1,0},{2,3},{3,2},{4,5},{5,4},{6,7},{7,6},{8,9},{9,8},{10,11... | collective-permute-start | bytes 98312 | tf_op jit(solution)/shard_map/ppermute | solution.py:39
  22.9 36.3 %collective-permute-start.4 = (bf16[128,512]{1,0:T(8,128)(2,1)S(1)}, bf16[128,512]{1,0:T(8,128)(2,1)S(1)}, u32[]{:S(2)}, u32[]{:S(2)}) collective-permute-start(bf16[128,512]{1,0:T(8,128)(2,1)S(1)} %pad_maximum_fusion.2), channel_id=1, source_target_pairs={{0,8},{1,25},{2,10},{3,27},{4,12},{5,29},{6,14},{7,31},{8,16},{9,1... | collective-permute-start | bytes 393224 | tf_op jit(solution)/shard_map/ppermute | solution.py:35
  38.6 20.6 %collective-permute-start.5 = (bf16[128,256]{1,0:T(8,128)(2,1)S(1)}, bf16[128,256]{1,0:T(8,128)(2,1)S(1)}, u32[]{:S(2)}, u32[]{:S(2)}) collective-permute-start(bf16[128,256]{1,0:T(8,128)(2,1)S(1)} %fusion.16), channel_id=1, source_target_pairs={{0,16},{1,17},{2,18},{3,19},{4,20},{5,21},{6,22},{7,23},{8,24},{9,... | collective-permute-start | bytes 196616 | tf_op jit(solution)/shard_map/ppermute | solution.py:35
  54.6 53.5 %all-to-all-start = ((bf16[16,128,768]{1,2,0:T(8,128)(2,1)}), bf16[16,128,768]{1,2,0:T(8,128)(2,1)}, u32[]{:S(2)}, u32[]{:S(2)}) async-start(bf16[16,128,768]{1,2,0:T(8,128)(2,1)} %broadcast_in_dim.39), calls=%async_computation | async-start | bytes 6291456 | tf_op jit(solution)/shard_map/all_to_all | solution.py:99
  59.2 3.3 %collective-permute-start.6 = (bf16[128,768]{1,0:T(8,128)(2,1)S(1)}, bf16[128,768]{1,0:T(8,128)(2,1)S(1)}, u32[]{:S(2)}, u32[]{:S(2)}) collective-permute-start(bf16[128,768]{1,0:T(8,128)(2,1)S(1)} %pad_maximum_fusion.1), channel_id=1, source_target_pairs={{0,1},{1,0},{2,3},{3,2},{4,5},{5,4},{6,7},{7,6},{8,9},{9,8},{10,11... | collective-permute-start | bytes 589832 | tf_op jit(solution)/shard_map/ppermute | solution.py:39
  62.6 13.9 %collective-permute-start.7 = (bf16[4,128,512]{2,1,0:T(8,128)(2,1)S(1)}, bf16[4,128,512]{2,1,0:T(8,128)(2,1)S(1)}, u32[]{:S(2)}, u32[]{:S(2)}) collective-permute-start(bf16[4,128,512]{2,1,0:T(8,128)(2,1)S(1)} %fusion.14), channel_id=1, source_target_pairs={{0,2},{1,31},{2,4},{3,1},{4,6},{5,3},{6,8},{7,5},{8,10},{9,7},{10,... | collective-permute-start | bytes 1572872 | tf_op jit(solution)/shard_map/ppermute | solution.py:35
  65.9 9.5 %collective-permute-start.8 = (bf16[2,128,512]{2,1,0:T(8,128)(2,1)S(1)}, bf16[2,128,512]{2,1,0:T(8,128)(2,1)S(1)}, u32[]{:S(2)}, u32[]{:S(2)}) collective-permute-start(bf16[2,128,512]{2,1,0:T(8,128)(2,1)S(1)} %constant_dynamic-slice_fusion.2), channel_id=1, source_target_pairs={{0,4},{1,29},{2,6},{3,31},{4,8},{5,1},{6,10},{7,3},{8,12},{9,5},{1... | collective-permute-start | bytes 786440 | tf_op jit(solution)/shard_map/ppermute | solution.py:35
  76.6 7.4 %collective-permute-start.9 = (bf16[6,128,512]{2,1,0:T(8,128)(2,1)S(1)}, bf16[6,128,512]{2,1,0:T(8,128)(2,1)S(1)}, u32[]{:S(2)}, u32[]{:S(2)}) collective-permute-start(bf16[6,128,512]{2,1,0:T(8,128)(2,1)S(1)} %pad_maximum_fusion), channel_id=1, source_target_pairs={{0,1},{1,0},{2,3},{3,2},{4,5},{5,4},{6,7},{7,6},{8,9},{9,8},{10,11... | collective-permute-start | bytes 2359304 | tf_op jit(solution)/shard_map/ppermute | solution.py:39
  84.1 1.4 copy-start
  115.9 4.9 %collective-permute-start.10 = (bf16[256,2048]{1,0:T(8,128)(2,1)}, bf16[256,2048]{1,0:T(8,128)(2,1)}, u32[]{:S(2)}, u32[]{:S(2)}) collective-permute-start(bf16[256,2048]{1,0:T(8,128)(2,1)} %convolution_convert_fusion), channel_id=1, source_target_pairs={{0,1},{1,0},{2,3},{3,2},{4,5},{5,4},{6,7},{7,6},{8,9},{9,8},{10,11... | collective-permute-start | bytes 3145736 | tf_op jit(solution)/shard_map/ppermute | solution.py:39
  122.6 20.6 %collective-permute-start.11 = (bf16[4,16,2048]{2,1,0:T(8,128)(2,1)S(1)}, bf16[4,16,2048]{2,1,0:T(8,128)(2,1)S(1)}, u32[]{:S(2)}, u32[]{:S(2)}) collective-permute-start(bf16[4,16,2048]{2,1,0:T(8,128)(2,1)S(1)} %get-tuple-element.25), channel_id=1, source_target_pairs={{0,2},{2,4},{4,6},{6,8},{8,10},{10,12},{12,14},{14,16},{16,18},{18... | collective-permute-start | bytes 786440 | tf_op jit(solution)/shard_map/ppermute | solution.py:30
  125.8 17.4 %collective-permute-start.12 = (bf16[4,16,2048]{2,1,0:T(8,128)(2,1)S(1)}, bf16[4,16,2048]{2,1,0:T(8,128)(2,1)S(1)}, u32[]{:S(2)}, u32[]{:S(2)}) collective-permute-start(bf16[4,16,2048]{2,1,0:T(8,128)(2,1)S(1)} %get-tuple-element.24), channel_id=1, source_target_pairs={{0,30},{2,0},{4,2},{6,4},{8,6},{10,8},{12,10},{14,12},{16,14},{18,... | collective-permute-start | bytes 786440 | tf_op jit(solution)/shard_map/ppermute | solution.py:30
  128.5 8.4 %collective-permute-start.13 = (bf16[2,16,2048]{2,1,0:T(8,128)(2,1)S(1)}, bf16[2,16,2048]{2,1,0:T(8,128)(2,1)S(1)}, u32[]{:S(2)}, u32[]{:S(2)}) collective-permute-start(bf16[2,16,2048]{2,1,0:T(8,128)(2,1)S(1)} %slice_bitcast_fusion.3), channel_id=1, source_target_pairs={{0,4},{2,6},{4,8},{6,10},{8,12},{10,14},{12,16},{14,18},{16,20},{1... | collective-permute-start | bytes 393224 | tf_op jit(solution)/shard_map/ppermute | solution.py:30
  132.4 10.8 %collective-permute-start.14 = (bf16[2,16,2048]{2,1,0:T(8,128)(2,1)S(1)}, bf16[2,16,2048]{2,1,0:T(8,128)(2,1)S(1)}, u32[]{:S(2)}, u32[]{:S(2)}) collective-permute-start(bf16[2,16,2048]{2,1,0:T(8,128)(2,1)S(1)} %dynamic-slice_bitcast_fusion.3), channel_id=1, source_target_pairs={{0,28},{2,30},{4,0},{6,2},{8,4},{10,6},{12,8},{14,10},{16,12},{18,... | collective-permute-start | bytes 393224 | tf_op jit(solution)/shard_map/ppermute | solution.py:30
  144.1 25.4 %all-to-all-start.1 = ((bf16[4,16,2048]{2,1,0:T(8,128)(2,1)}), bf16[4,16,2048]{2,1,0:T(8,128)(2,1)S(1)}, u32[]{:S(2)}, u32[]{:S(2)}) async-start(bf16[4,16,2048]{2,1,0:T(8,128)(2,1)} %fusion.11), calls=%async_computation.1 | async-start | bytes 524288 | tf_op jit(solution)/shard_map/all_to_all | solution.py:91
where the time goes:
time: 171 us; the launch traced here: 170 us
  starting transfers between devices  84.3 us (49%)
  waiting for transfers between devices  61.9 us (36%)
  local copies, waits for them, and re-layouts  11.6 us (7%)
  matrix products  5.99 us (4%)
  other arithmetic  5.31 us (3%)
    ppermute x4, starting transfers between devices, fan(): return lax.ppermute(x, TP, pairs)  38.1 us
    all_to_all x1, waiting for transfers between devices, body(): lax.all_to_all(jnp.broadcast_to(local, (16, 128, 768)), 'fs', 0, 0, tiled...  22.2 us
    all_to_all x1, waiting for transfers between devices, scatter_sum(): rows = lax.all_to_all(near, 'zh', 0, 0, tiled=True)  15.5 us
    ppermute x5, starting transfers between devices, swap(): return lax.ppermute(x, 'c', [(0, 1), (1, 0)])  13.4 us
    ppermute x4, starting transfers between devices, shift(): return lax.ppermute(x, TP[:2], [(i, (i + by) % 16) for i in range(16)])  12.6 us
    ppermute x4, waiting for transfers between devices, shift(): return lax.ppermute(x, TP[:2], [(i, (i + by) % 16) for i in range(16)])  7.93 us
    all_to_all x1, starting transfers between devices, scatter_sum(): rows = lax.all_to_all(near, 'zh', 0, 0, tiled=True)  5.86 us
    ppermute x5, waiting for transfers between devices, swap(): return lax.ppermute(x, 'c', [(0, 1), (1, 0)])  5.71 us
  transfers between devices with their start and end apart: 17, of which 11 were waited for; matrix products, arithmetic and copies ran while one was open for 6% of the time, Pallas kernels for 0%

commit v1 on v0

--- a/solution.py
+++ b/solution.py
@@ -1,6 +1,7 @@
 import jax
 import jax.numpy as jnp
 from jax import lax
+from jax.experimental.layout import Layout, with_layout_constraint
 from jax.sharding import Mesh
 from jax.sharding import PartitionSpec as P
 
@@ -18,21 +19,12 @@
     return lax.dynamic_index_in_dim(x, i, dim, keepdims=False, allow_negative_indices=False)
 
 
-def part_of(x, at, size, dim):
-    return lax.dynamic_slice_in_dim(x, at, size, dim, allow_negative_indices=False)
-
-
 def put(whole, part, at):
     return lax.dynamic_update_slice(whole, part, at, allow_negative_indices=False)
 
 
 def shift(x, by):
     return lax.ppermute(x, TP[:2], [(i, (i + by) % 16) for i in range(16)])
-
-
-def fan(x, by):
-    pairs = [(2 * z + c, 2 * ((z + (by, -by)[c]) % 16) + c) for z in range(16) for c in range(2)]
-    return lax.ppermute(x, TP, pairs)
 
 
 def swap(x):
@@ -43,26 +35,23 @@
     return jnp.concatenate([jnp.where(c == 0, mine, other), jnp.where(c == 0, other, mine)], axis=dim)
 
 
+def row_major(x):
+    return with_layout_constraint(x, Layout(major_to_minor=tuple(range(x.ndim))))
+
+
 def gather_tokens(tokens):
-    zh, zl, c = (lax.axis_index(a) for a in TP)
-    x = tokens.T
-    chip = by_core(c, x, swap(x), 0)
-    p = fan(chip, 4)
-    q = fan(jnp.where(c == 0, chip[:, :256], chip[:, 256:]), 8)
-    o = swap(jnp.concatenate([p, q], axis=1))
-    own = put(jnp.zeros((4, 128, 512), BF), chip[None], (zh, 0, 0))
-    own = put(own, p[None], ((zh + 3 + 2 * c) & 3, 0, 0))
-    own = put(own, o[None, :, :512], ((zh + 1 + 2 * c) & 3, 0, 0))
-    own = put(own, by_core(c, q, o[:, 512:], 1)[None], ((zh + 2) & 3, 0, 0))
-    n = fan(own, 1)
-    f = fan(part_of(own, 2 * c, 2, 0), 2)
-    o = swap(jnp.concatenate([n, f], axis=0))
-    whole = put(jnp.zeros((4, 4, 128, 512), BF), own[:, None], (0, zl, 0, 0))
-    whole = put(whole, n[:, None], (0, (zl + 3 + 2 * c) & 3, 0, 0))
-    whole = put(whole, f[:, None], (2 * c, (zl + 2) & 3, 0, 0))
-    whole = put(whole, o[:4, None], (0, (zl + 1 + 2 * c) & 3, 0, 0))
-    whole = put(whole, o[4:, None], (2 - 2 * c, (zl + 2) & 3, 0, 0))
-    return whole.reshape(D, 512)
+    zl, c = lax.axis_index("zl"), lax.axis_index("c")
+    own = lax.all_to_all(jnp.broadcast_to(tokens.T, (4, 64, 512)), "zh", 0, 0, tiled=True)
+    before, after = shift(own, 1), shift(own, -1)
+    far_a, far_b = shift(own[:2], 2), shift(own[2:], -2)
+    mine = put(jnp.zeros((4, 4, 64, 512), BF), own[:, None], (0, zl, 0, 0))
+    mine = put(mine, before[:, None], (0, (zl + 3) & 3, 0, 0))
+    mine = put(mine, after[:, None], (0, (zl + 1) & 3, 0, 0))
+    mine = put(mine, far_a[:, None], (0, (zl + 2) & 3, 0, 0))
+    mine = put(mine, far_b[:, None], (2, (zl + 2) & 3, 0, 0)).reshape(16, 1, 64, 512)
+    other = swap(mine)
+    whole = put(jnp.zeros((16, 2, 64, 512), BF), mine, (0, c, 0, 0))
+    return put(whole, other, (0, 1 - c, 0, 0)).reshape(D, 512)
 
 
 def place_down(down_train):
@@ -96,7 +85,8 @@
     gate_local = (norm_gain[:, None] * gate_train).astype(BF)
     up_local = (norm_gain[:, None] * up_train).astype(BF)
     local = jnp.concatenate([gate_local, up_local, place_down(down_train)], axis=1)
-    every = lax.all_to_all(jnp.broadcast_to(local, (16, 128, 768)), "fs", 0, 0, tiled=True)
+    every = row_major(jnp.broadcast_to(local, (16, 128, 768)))
+    every = row_major(lax.all_to_all(every, "fs", 0, 0, tiled=True))
     every = every.reshape(D, 768)
     both, down = every[:, :512], every[:, 512:]
     x = gather_tokens(tokens)

time: 171 us -> 165 us (0.965)
  waiting for transfers between devices: 61.9 us -> 55.9 us
  local copies, waits for them, and re-layouts: 11.6 us -> 15.9 us
  starting transfers between devices: 84.3 us -> 81.5 us
    ppermute x4 -> x0, starting transfers between devices: 38.1 us -> none  [fan(): return lax.ppermute(x, TP, pairs)]
    all_to_all x1 -> x2, starting transfers between devices: 4.5 us -> 24 us  [the longest x1 18.3 us: gather_tokens(): lax.all_to_all(jnp.broadcast_to(tokens.T, (4, 64, 512)), 'zh', 0, 0, tile...]
    ppermute x4 -> x8, starting transfers between devices: 12.6 us -> 31.4 us  [shift(): return lax.ppermute(x, TP[:2], [(i, (i + by) % 16) for i in range(16)])]
    ppermute x5 -> x3, starting transfers between devices: 13.4 us -> 5.74 us  [swap(): return lax.ppermute(x, 'c', [(0, 1), (1, 0)])]
    dynamic_update_slice x7, local copies, waits for them, and re-layouts: 0.21 us -> 6.12 us  [put(): lax.dynamic_update_slice(whole, part, at, allow_negative_indices=False)]
    ppermute x4 -> x0, waiting for transfers between devices: 5.02 us -> none  [fan(): return lax.ppermute(x, TP, pairs)]
    all_to_all x1, starting transfers between devices: 5.86 us -> 10.6 us  [scatter_sum(): rows = lax.all_to_all(near, 'zh', 0, 0, tiled=True)]
    ppermute x1, waiting for transfers between devices: 4.52 us -> 0.01 us  [place_down(): lax.ppermute(x, FS_TP[:3], [((a ^ b) * 16 + b, b * 16 + a) for a, b in EV...]
  transfers between devices with their start and end apart: 17 -> 16, of which waited for: 11 -> 10; matrix products, arithmetic and copies ran while one was open for 6% -> 9% of each run, Pallas kernels for 0% -> 0%
where the time goes in v1:
time: 165 us
  starting transfers between devices  81.5 us (49%)
  waiting for transfers between devices  55.9 us (34%)
  local copies, waits for them, and re-layouts  15.9 us (10%)
  matrix products  5.99 us (4%)
  other arithmetic  4.37 us (3%)
    ppermute x8, starting transfers between devices, shift(): return lax.ppermute(x, TP[:2], [(i, (i + by) % 16) for i in range(16)])  31.4 us
    all_to_all x1, starting transfers between devices, gather_tokens(): lax.all_to_all(jnp.broadcast_to(tokens.T, (4, 64, 512)), 'zh', 0, 0, tile...  18.3 us
    all_to_all x1, waiting for transfers between devices, scatter_sum(): rows = lax.all_to_all(near, 'zh', 0, 0, tiled=True)  13.8 us
    all_to_all x1, waiting for transfers between devices, gather_tokens(): lax.all_to_all(jnp.broadcast_to(tokens.T, (4, 64, 512)), 'zh', 0, 0, tile...  13.2 us
    ppermute x8, waiting for transfers between devices, shift(): return lax.ppermute(x, TP[:2], [(i, (i + by) % 16) for i in range(16)])  12.1 us
    all_to_all x1, starting transfers between devices, scatter_sum(): rows = lax.all_to_all(near, 'zh', 0, 0, tiled=True)  10.6 us
    all_to_all x1, waiting for transfers between devices, body(): every = row_major(lax.all_to_all(every, 'fs', 0, 0, tiled=True))  9.71 us
    dynamic_update_slice x7, local copies, waits for them, and re-layouts, put(): lax.dynamic_update_slice(whole, part, at, allow_negative_indices=False)  6.12 us
  transfers between devices with their start and end apart: 16, of which 10 were waited for; matrix products, arithmetic and copies ran while one was open for 9% of the time, Pallas kernels for 0%

profile of v1, /device:TPU:64, one launch (start us, length us, event | category | flops | bytes accessed | tf_op | source)
XLA Modules:
  0.0 164.6 jit_solution(12138918006408544533)
XLA Ops:
  0.6 0.9 convert_bitcast_fusion
  1.5 4.9 %collective-permute-start = (bf16[64,512]{1,0:T(8,128)(2,1)S(1)}, bf16[64,512]{1,0:T(8,128)(2,1)S(1)}, u32[]{:S(2)}, u32[]{:S(2)}) collective-permute-start(bf16[64,512]{1,0:T(8,128)(2,1)S(1)} %convert_bitcast_fusion), channel_id=1, source_target_pairs={{0,0},{2,34},{4,68},{6,102},{8,136},{10,170},{12,204},{14,238},{16... | collective-permute-start | bytes 196616 | tf_op jit(solution)/shard_map/ppermute | solution.py:60
  6.5 2.7 %collective-permute-done = bf16[64,512]{1,0:T(8,128)(2,1)S(1)} collective-permute-done((bf16[64,512]{1,0:T(8,128)(2,1)S(1)}, bf16[64,512]{1,0:T(8,128)(2,1)S(1)}, u32[]{:S(2)}, u32[]{:S(2)}) %collective-permute-start) | collective-permute-done | bytes 65568 | tf_op jit(solution)/shard_map/ppermute | solution.py:60
  9.2 4.9 %collective-permute-start.1 = (bf16[64,512]{1,0:T(8,128)(2,1)S(1)}, bf16[64,512]{1,0:T(8,128)(2,1)S(1)}, u32[]{:S(2)}, u32[]{:S(2)}) collective-permute-start(bf16[64,512]{1,0:T(8,128)(2,1)S(1)} %collective-permute-done), channel_id=1, source_target_pairs={{0,0},{34,32},{68,64},{102,96},{136,128},{170,160},{204,192},{238,... | collective-permute-start | bytes 196616 | tf_op jit(solution)/shard_map/ppermute | solution.py:61
  14.1 1.6 broadcast_in_dim.33
  15.7 18.3 %all-to-all-start.1 = ((bf16[4,64,512]{2,1,0:T(8,128)(2,1)}), bf16[4,64,512]{2,1,0:T(8,128)(2,1)S(1)}, u32[]{:S(2)}, u32[]{:S(2)}) async-start(bf16[4,64,512]{2,1,0:T(8,128)(2,1)} %broadcast_in_dim.33), calls=%async_computation.1 | async-start | bytes 524288 | tf_op jit(solution)/shard_map/all_to_all | solution.py:44
  34.0 0.0 collective-permute-done.1
  34.0 1.9 %collective-permute-start.2 = (bf16[64,256]{1,0:T(8,128)(2,1)S(1)}, bf16[64,256]{1,0:T(8,128)(2,1)S(1)}, u32[]{:S(2)}, u32[]{:S(2)}) collective-permute-start(bf16[64,256]{1,0:T(8,128)(2,1)S(1)} %broadcast_select_fusion.2), channel_id=1, source_target_pairs={{0,1},{1,0},{2,3},{3,2},{4,5},{5,4},{6,7},{7,6},{8,9},{9,8},{10,11... | collective-permute-start | bytes 98312 | tf_op jit(solution)/shard_map/ppermute | solution.py:31
  36.0 1.1 multiply_convert_fusion.1
  37.1 0.1 collective-permute-done.2
  37.2 13.2 %all-to-all-done.1 = bf16[4,64,512]{2,1,0:T(8,128)(2,1)S(1)} async-done(((bf16[4,64,512]{2,1,0:T(8,128)(2,1)}), bf16[4,64,512]{2,1,0:T(8,128)(2,1)S(1)}, u32[]{:S(2)}, u32[]{:S(2)}) %all-to-all-start.1) | async-done | bytes 262176 | tf_op jit(solution)/shard_map/all_to_all | solution.py:44
  50.4 2.0 %broadcast_in_dim.30 = bf16[16,128,768]{2,1,0:T(8,128)(2,1)} broadcast(bf16[128,768]{1,0:T(8,128)(2,1)S(1)} %maximum_maximum_fusion), dimensions={1,2} | broadcast | bytes 3342336 | tf_op jit(solution)/shard_map/broadcast_in_dim | solution.py:88
  52.3 5.6 %all-to-all-start = ((bf16[16,128,768]{2,1,0:T(8,128)(2,1)}), bf16[16,128,768]{2,1,0:T(8,128)(2,1)S(1)}, u32[]{:S(2)}, u32[]{:S(2)}) async-start(bf16[16,128,768]{2,1,0:T(8,128)(2,1)} %broadcast_in_dim.30), calls=%async_computation | async-start | bytes 6291456 | tf_op jit(solution)/shard_map/all_to_all | solution.py:89
  58.0 1.9 %collective-permute-start.3 = (bf16[4,64,512]{2,1,0:T(8,128)(2,1)S(1)}, bf16[4,64,512]{2,1,0:T(8,128)(2,1)S(1)}, u32[]{:S(2)}, u32[]{:S(2)}) collective-permute-start(bf16[4,64,512]{2,1,0:T(8,128)(2,1)S(1)} %all-to-all-done.1), channel_id=1, source_target_pairs={{0,2},{2,4},{4,6},{6,8},{8,10},{10,12},{12,14},{14,16},{16,18},{18... | collective-permute-start | bytes 786440 | tf_op jit(solution)/shard_map/ppermute | solution.py:27
  60.0 4.2 %collective-permute-start.5 = (bf16[2,64,512]{2,1,0:T(8,128)(2,1)S(1)}, bf16[2,64,512]{2,1,0:T(8,128)(2,1)S(1)}, u32[]{:S(2)}, u32[]{:S(2)}) collective-permute-start(bf16[2,64,512]{2,1,0:T(8,128)(2,1)S(1)} %get-tuple-element.13), channel_id=1, source_target_pairs={{0,4},{2,6},{4,8},{6,10},{8,12},{10,14},{12,16},{14,18},{16,20},{1... | collective-permute-start | bytes 393224 | tf_op jit(solution)/shard_map/ppermute | solution.py:27
  64.1 2.6 %collective-permute-start.6 = (bf16[2,64,512]{2,1,0:T(8,128)(2,1)S(1)}, bf16[2,64,512]{2,1,0:T(8,128)(2,1)S(1)}, u32[]{:S(2)}, u32[]{:S(2)}) collective-permute-start(bf16[2,64,512]{2,1,0:T(8,128)(2,1)S(1)} %get-tuple-element.12), channel_id=1, source_target_pairs={{0,28},{2,30},{4,0},{6,2},{8,4},{10,6},{12,8},{14,10},{16,12},{18,... | collective-permute-start | bytes 393224 | tf_op jit(solution)/shard_map/ppermute | solution.py:27
  66.7 5.1 %collective-permute-start.4 = (bf16[4,64,512]{2,1,0:T(8,128)(2,1)S(1)}, bf16[4,64,512]{2,1,0:T(8,128)(2,1)S(1)}, u32[]{:S(2)}, u32[]{:S(2)}) collective-permute-start(bf16[4,64,512]{2,1,0:T(8,128)(2,1)S(1)} %all-to-all-done.1), channel_id=1, source_target_pairs={{0,30},{2,0},{4,2},{6,4},{8,6},{10,8},{12,10},{14,12},{16,14},{18,... | collective-permute-start | bytes 786440 | tf_op jit(solution)/shard_map/ppermute | solution.py:27
  71.9 1.1 broadcast_in_dim.32
  72.9 0.7 bitcast_dynamic-update-slice_fusion.2
  73.6 0.0 collective-permute-done.3
  73.7 0.7 bitcast_dynamic-update-slice_fusion.1
  74.4 4.6 %collective-permute-done.4 = bf16[4,64,512]{2,1,0:T(8,128)(2,1)S(1)} collective-permute-done((bf16[4,64,512]{2,1,0:T(8,128)(2,1)S(1)}, bf16[4,64,512]{2,1,0:T(8,128)(2,1)S(1)}, u32[]{:S(2)}, u32[]{:S(2)}) %collective-permute-start.4) | collective-permute-done | bytes 262176 | tf_op jit(solution)/shard_map/ppermute | solution.py:27
  79.0 0.7 bitcast_dynamic-update-slice_fusion
  79.7 0.0 collective-permute-done.5
  79.7 0.7 bitcast_dynamic-update-slice_fusion.3
  80.4 0.0 collective-permute-done.6
  80.4 0.7 bitcast_dynamic-update-slice_fusion.4
  81.1 1.9 %collective-permute-start.7 = (bf16[16,1,64,512]{3,2,1,0:T(8,128)(2,1)}, bf16[16,1,64,512]{3,2,1,0:T(8,128)(2,1)}, u32[]{:S(2)}, u32[]{:S(2)}) collective-permute-start(bf16[16,1,64,512]{3,2,1,0:T(8,128)(2,1)} %bitcast.13), channel_id=1, source_target_pairs={{0,1},{1,0},{2,3},{3,2},{4,5},{5,4},{6,7},{7,6},{8,9},{9,8},{10,11... | collective-permute-start | bytes 3145736 | tf_op jit(solution)/shard_map/ppermute | solution.py:31
  83.0 0.2 broadcast_in_dim.31
  83.2 1.3 constant_dynamic-update-slice_fusion.1
  84.5 1.4 collective-permute-done.7
  86.0 1.3 constant_dynamic-update-slice_fusion
  87.3 0.0 copy-start
  87.3 0.6 multiply_reduce_fusion
  87.9 0.8 copy-done
  88.6 9.7 %all-to-all-done = bf16[16,128,768]{2,1,0:T(8,128)(2,1)S(1)} async-done(((bf16[16,128,768]{2,1,0:T(8,128)(2,1)}), bf16[16,128,768]{2,1,0:T(8,128)(2,1)S(1)}, u32[]{:S(2)}, u32[]{:S(2)}) %all-to-all-start) | async-done | bytes 3145760 | tf_op jit(solution)/shard_map/all_to_all | solution.py:89
  98.4 2.9 %fusion = f32[512,512]{1,0:T(8,128)S(1)} fusion(bf16[2048,512]{1,0:T(8,128)(2,1)} %bitcast.51, bf16[2048,768]{1,0:T(8,128)(2,1)S(1)} %bitcast.47), kind=kOutput, calls=%fused_computation.2 | convolution fusion | flops 1073741824 | bytes 5242880 | tf_op jit(solution)/shard_map/dot_general | solution.py:95
  101.2 0.2 fusion.3
  101.5 1.4 convolution_convert_fusion
  102.9 1.9 %collective-permute-start.8 = (bf16[256,2048]{1,0:T(8,128)(2,1)}, bf16[256,2048]{1,0:T(8,128)(2,1)}, u32[]{:S(2)}, u32[]{:S(2)}) collective-permute-start(bf16[256,2048]{1,0:T(8,128)(2,1)} %convolution_convert_fusion), channel_id=1, source_target_pairs={{0,1},{1,0},{2,3},{3,2},{4,5},{5,4},{6,7},{7,6},{8,9},{9,8},{10,11... | collective-permute-start | bytes 3145736 | tf_op jit(solution)/shard_map/ppermute | solution.py:31
  104.9 3.0 %collective-permute-done.8 = bf16[256,2048]{1,0:T(8,128)(2,1)} collective-permute-done((bf16[256,2048]{1,0:T(8,128)(2,1)}, bf16[256,2048]{1,0:T(8,128)(2,1)}, u32[]{:S(2)}, u32[]{:S(2)}) %collective-permute-start.8) | collective-permute-done | bytes 1048608 | tf_op jit(solution)/shard_map/ppermute | solution.py:31
  107.8 1.7 %add_convert_fusion = bf16[256,2048]{1,0:T(8,128)(2,1)S(1)} fusion(bf16[256,2048]{1,0:T(8,128)(2,1)} %collective-permute-done.8, bf16[256,256]{1,0:T(8,128)(2,1)S(1)} %bitcast.57, bf16[2048,768]{1,0:T(8,128)(2,1)S(1)} %bitcast.49), kind=kOutput, calls=%fused_computation.4 | convolution fusion | flops 270008320 | bytes 3276800 | tf_op jit(solution)/shard_map/dot_general | solution.py:73
  109.5 0.1 dynamic-slice_bitcast_fusion
  109.6 4.4 %collective-permute-start.10 = (bf16[4,16,2048]{2,1,0:T(8,128)(2,1)S(1)}, bf16[4,16,2048]{2,1,0:T(8,128)(2,1)S(1)}, u32[]{:S(2)}, u32[]{:S(2)}) collective-permute-start(bf16[4,16,2048]{2,1,0:T(8,128)(2,1)S(1)} %get-tuple-element.8), channel_id=1, source_target_pairs={{0,30},{2,0},{4,2},{6,4},{8,6},{10,8},{12,10},{14,12},{16,14},{18,... | collective-permute-start | bytes 786440 | tf_op jit(solution)/shard_map/ppermute | solution.py:27
  114.0 7.7 %collective-permute-start.11 = (bf16[2,16,2048]{2,1,0:T(8,128)(2,1)S(1)}, bf16[2,16,2048]{2,1,0:T(8,128)(2,1)S(1)}, u32[]{:S(2)}, u32[]{:S(2)}) collective-permute-start(bf16[2,16,2048]{2,1,0:T(8,128)(2,1)S(1)} %slice_bitcast_fusion), channel_id=1, source_target_pairs={{0,4},{2,6},{4,8},{6,10},{8,12},{10,14},{12,16},{14,18},{16,20},{1... | collective-permute-start | bytes 393224 | tf_op jit(solution)/shard_map/ppermute | solution.py:27
  121.7 3.6 %collective-permute-start.9 = (bf16[4,16,2048]{2,1,0:T(8,128)(2,1)S(1)}, bf16[4,16,2048]{2,1,0:T(8,128)(2,1)S(1)}, u32[]{:S(2)}, u32[]{:S(2)}) collective-permute-start(bf16[4,16,2048]{2,1,0:T(8,128)(2,1)S(1)} %get-tuple-element.9), channel_id=1, source_target_pairs={{0,2},{2,4},{4,6},{6,8},{8,10},{10,12},{12,14},{14,16},{16,18},{18... | collective-permute-start | bytes 786440 | tf_op jit(solution)/shard_map/ppermute | solution.py:27
  125.4 1.9 %collective-permute-start.12 = (bf16[2,16,2048]{2,1,0:T(8,128)(2,1)S(1)}, bf16[2,16,2048]{2,1,0:T(8,128)(2,1)S(1)}, u32[]{:S(2)}, u32[]{:S(2)}) collective-permute-start(bf16[2,16,2048]{2,1,0:T(8,128)(2,1)S(1)} %dynamic-slice_bitcast_fusion.3), channel_id=1, source_target_pairs={{0,28},{2,30},{4,0},{6,2},{8,4},{10,6},{12,8},{14,10},{16,12},{18,... | collective-permute-start | bytes 393224 | tf_op jit(solution)/shard_map/ppermute | solution.py:27
  127.3 1.9 %collective-permute-done.11 = bf16[2,16,2048]{2,1,0:T(8,128)(2,1)S(1)} collective-permute-done((bf16[2,16,2048]{2,1,0:T(8,128)(2,1)S(1)}, bf16[2,16,2048]{2,1,0:T(8,128)(2,1)S(1)}, u32[]{:S(2)}, u32[]{:S(2)}) %collective-permute-start.11) | collective-permute-done | bytes 131104 | tf_op jit(solution)/shard_map/ppermute | solution.py:27
  129.2 5.5 %collective-permute-done.12 = bf16[2,16,2048]{2,1,0:T(8,128)(2,1)S(1)} collective-permute-done((bf16[2,16,2048]{2,1,0:T(8,128)(2,1)S(1)}, bf16[2,16,2048]{2,1,0:T(8,128)(2,1)S(1)}, u32[]{:S(2)}, u32[]{:S(2)}) %collective-permute-start.12) | collective-permute-done | bytes 131104 | tf_op jit(solution)/shard_map/ppermute | solution.py:27
  134.7 0.0 collective-permute-done.10
  134.7 0.0 collective-permute-done.9
  134.7 0.9 fusion.5
  135.6 10.6 %all-to-all-start.2 = ((bf16[4,16,2048]{2,1,0:T(8,128)(2,1)}), bf16[4,16,2048]{2,1,0:T(8,128)(2,1)S(1)}, u32[]{:S(2)}, u32[]{:S(2)}) async-start(bf16[4,16,2048]{2,1,0:T(8,128)(2,1)} %fusion.5), calls=%async_computation.2 | async-start | bytes 524288 | tf_op jit(solution)/shard_map/all_to_all | solution.py:80
  146.1 1.7 %fusion.11 = (bf16[2048,256]{1,0:T(8,128)(2,1)}, bf16[2048,256]{1,0:T(8,128)(2,1)}, bf16[2048,256]{1,0:T(8,128)(2,1)}) fusion(bf16[2048,768]{1,0:T(8,128)(2,1)S(1)} %bitcast.50), kind=kLoop, calls=%fused_computation.38 | loop fusion | bytes 6291456
  147.9 2.3 %copy.23 = bf16[2048,256]{0,1:T(8,128)(2,1)} copy(bf16[2048,256]{1,0:T(8,128)(2,1)} %get-tuple-element.4) | data formatting | bytes 2097152
  150.1 13.8 %all-to-all-done.2 = bf16[4,16,2048]{2,1,0:T(8,128)(2,1)S(1)} async-done(((bf16[4,16,2048]{2,1,0:T(8,128)(2,1)}), bf16[4,16,2048]{2,1,0:T(8,128)(2,1)S(1)}, u32[]{:S(2)}, u32[]{:S(2)}) %all-to-all-start.2) | async-done | bytes 262176 | tf_op jit(solution)/shard_map/all_to_all | solution.py:80
  163.9 0.7 reduce_sum.22
  (8 shorter events, 0.1 us)
Async XLA Ops:
  1.5 7.7 %collective-permute-start = (bf16[64,512]{1,0:T(8,128)(2,1)S(1)}, bf16[64,512]{1,0:T(8,128)(2,1)S(1)}, u32[]{:S(2)}, u32[]{:S(2)}) collective-permute-start(bf16[64,512]{1,0:T(8,128)(2,1)S(1)} %convert_bitcast_fusion), channel_id=1, source_target_pairs={{0,0},{2,34},{4,68},{6,102},{8,136},{10,170},{12,204},{14,238},{16... | collective-permute-start | bytes 196616 | tf_op jit(solution)/shard_map/ppermute | solution.py:60
  9.2 24.8 %collective-permute-start.1 = (bf16[64,512]{1,0:T(8,128)(2,1)S(1)}, bf16[64,512]{1,0:T(8,128)(2,1)S(1)}, u32[]{:S(2)}, u32[]{:S(2)}) collective-permute-start(bf16[64,512]{1,0:T(8,128)(2,1)S(1)} %collective-permute-done), channel_id=1, source_target_pairs={{0,0},{34,32},{68,64},{102,96},{136,128},{170,160},{204,192},{238,... | collective-permute-start | bytes 196616 | tf_op jit(solution)/shard_map/ppermute | solution.py:61
  15.7 34.7 %all-to-all-start.1 = ((bf16[4,64,512]{2,1,0:T(8,128)(2,1)}), bf16[4,64,512]{2,1,0:T(8,128)(2,1)S(1)}, u32[]{:S(2)}, u32[]{:S(2)}) async-start(bf16[4,64,512]{2,1,0:T(8,128)(2,1)} %broadcast_in_dim.33), calls=%async_computation.1 | async-start | bytes 524288 | tf_op jit(solution)/shard_map/all_to_all | solution.py:44
  34.0 3.1 %collective-permute-start.2 = (bf16[64,256]{1,0:T(8,128)(2,1)S(1)}, bf16[64,256]{1,0:T(8,128)(2,1)S(1)}, u32[]{:S(2)}, u32[]{:S(2)}) collective-permute-start(bf16[64,256]{1,0:T(8,128)(2,1)S(1)} %broadcast_select_fusion.2), channel_id=1, source_target_pairs={{0,1},{1,0},{2,3},{3,2},{4,5},{5,4},{6,7},{7,6},{8,9},{9,8},{10,11... | collective-permute-start | bytes 98312 | tf_op jit(solution)/shard_map/ppermute | solution.py:31
  52.3 46.0 %all-to-all-start = ((bf16[16,128,768]{2,1,0:T(8,128)(2,1)}), bf16[16,128,768]{2,1,0:T(8,128)(2,1)S(1)}, u32[]{:S(2)}, u32[]{:S(2)}) async-start(bf16[16,128,768]{2,1,0:T(8,128)(2,1)} %broadcast_in_dim.30), calls=%async_computation | async-start | bytes 6291456 | tf_op jit(solution)/shard_map/all_to_all | solution.py:89
  58.0 15.7 %collective-permute-start.3 = (bf16[4,64,512]{2,1,0:T(8,128)(2,1)S(1)}, bf16[4,64,512]{2,1,0:T(8,128)(2,1)S(1)}, u32[]{:S(2)}, u32[]{:S(2)}) collective-permute-start(bf16[4,64,512]{2,1,0:T(8,128)(2,1)S(1)} %all-to-all-done.1), channel_id=1, source_target_pairs={{0,2},{2,4},{4,6},{6,8},{8,10},{10,12},{12,14},{14,16},{16,18},{18... | collective-permute-start | bytes 786440 | tf_op jit(solution)/shard_map/ppermute | solution.py:27
  60.0 19.8 %collective-permute-start.5 = (bf16[2,64,512]{2,1,0:T(8,128)(2,1)S(1)}, bf16[2,64,512]{2,1,0:T(8,128)(2,1)S(1)}, u32[]{:S(2)}, u32[]{:S(2)}) collective-permute-start(bf16[2,64,512]{2,1,0:T(8,128)(2,1)S(1)} %get-tuple-element.13), channel_id=1, source_target_pairs={{0,4},{2,6},{4,8},{6,10},{8,12},{10,14},{12,16},{14,18},{16,20},{1... | collective-permute-start | bytes 393224 | tf_op jit(solution)/shard_map/ppermute | solution.py:27
  64.1 16.3 %collective-permute-start.6 = (bf16[2,64,512]{2,1,0:T(8,128)(2,1)S(1)}, bf16[2,64,512]{2,1,0:T(8,128)(2,1)S(1)}, u32[]{:S(2)}, u32[]{:S(2)}) collective-permute-start(bf16[2,64,512]{2,1,0:T(8,128)(2,1)S(1)} %get-tuple-element.12), channel_id=1, source_target_pairs={{0,28},{2,30},{4,0},{6,2},{8,4},{10,6},{12,8},{14,10},{16,12},{18,... | collective-permute-start | bytes 393224 | tf_op jit(solution)/shard_map/ppermute | solution.py:27
  66.7 12.3 %collective-permute-start.4 = (bf16[4,64,512]{2,1,0:T(8,128)(2,1)S(1)}, bf16[4,64,512]{2,1,0:T(8,128)(2,1)S(1)}, u32[]{:S(2)}, u32[]{:S(2)}) collective-permute-start(bf16[4,64,512]{2,1,0:T(8,128)(2,1)S(1)} %all-to-all-done.1), channel_id=1, source_target_pairs={{0,30},{2,0},{4,2},{6,4},{8,6},{10,8},{12,10},{14,12},{16,14},{18,... | collective-permute-start | bytes 786440 | tf_op jit(solution)/shard_map/ppermute | solution.py:27
  81.1 4.9 %collective-permute-start.7 = (bf16[16,1,64,512]{3,2,1,0:T(8,128)(2,1)}, bf16[16,1,64,512]{3,2,1,0:T(8,128)(2,1)}, u32[]{:S(2)}, u32[]{:S(2)}) collective-permute-start(bf16[16,1,64,512]{3,2,1,0:T(8,128)(2,1)} %bitcast.13), channel_id=1, source_target_pairs={{0,1},{1,0},{2,3},{3,2},{4,5},{5,4},{6,7},{7,6},{8,9},{9,8},{10,11... | collective-permute-start | bytes 3145736 | tf_op jit(solution)/shard_map/ppermute | solution.py:31
  87.3 1.4 copy-start
  102.9 4.9 %collective-permute-start.8 = (bf16[256,2048]{1,0:T(8,128)(2,1)}, bf16[256,2048]{1,0:T(8,128)(2,1)}, u32[]{:S(2)}, u32[]{:S(2)}) collective-permute-start(bf16[256,2048]{1,0:T(8,128)(2,1)} %convolution_convert_fusion), channel_id=1, source_target_pairs={{0,1},{1,0},{2,3},{3,2},{4,5},{5,4},{6,7},{7,6},{8,9},{9,8},{10,11... | collective-permute-start | bytes 3145736 | tf_op jit(solution)/shard_map/ppermute | solution.py:31
  109.6 25.1 %collective-permute-start.10 = (bf16[4,16,2048]{2,1,0:T(8,128)(2,1)S(1)}, bf16[4,16,2048]{2,1,0:T(8,128)(2,1)S(1)}, u32[]{:S(2)}, u32[]{:S(2)}) collective-permute-start(bf16[4,16,2048]{2,1,0:T(8,128)(2,1)S(1)} %get-tuple-element.8), channel_id=1, source_target_pairs={{0,30},{2,0},{4,2},{6,4},{8,6},{10,8},{12,10},{14,12},{16,14},{18,... | collective-permute-start | bytes 786440 | tf_op jit(solution)/shard_map/ppermute | solution.py:27
  114.0 15.2 %collective-permute-start.11 = (bf16[2,16,2048]{2,1,0:T(8,128)(2,1)S(1)}, bf16[2,16,2048]{2,1,0:T(8,128)(2,1)S(1)}, u32[]{:S(2)}, u32[]{:S(2)}) collective-permute-start(bf16[2,16,2048]{2,1,0:T(8,128)(2,1)S(1)} %slice_bitcast_fusion), channel_id=1, source_target_pairs={{0,4},{2,6},{4,8},{6,10},{8,12},{10,14},{12,16},{14,18},{16,20},{1... | collective-permute-start | bytes 393224 | tf_op jit(solution)/shard_map/ppermute | solution.py:27
  121.7 13.0 %collective-permute-start.9 = (bf16[4,16,2048]{2,1,0:T(8,128)(2,1)S(1)}, bf16[4,16,2048]{2,1,0:T(8,128)(2,1)S(1)}, u32[]{:S(2)}, u32[]{:S(2)}) collective-permute-start(bf16[4,16,2048]{2,1,0:T(8,128)(2,1)S(1)} %get-tuple-element.9), channel_id=1, source_target_pairs={{0,2},{2,4},{4,6},{6,8},{8,10},{10,12},{12,14},{14,16},{16,18},{18... | collective-permute-start | bytes 786440 | tf_op jit(solution)/shard_map/ppermute | solution.py:27
  125.4 9.3 %collective-permute-start.12 = (bf16[2,16,2048]{2,1,0:T(8,128)(2,1)S(1)}, bf16[2,16,2048]{2,1,0:T(8,128)(2,1)S(1)}, u32[]{:S(2)}, u32[]{:S(2)}) collective-permute-start(bf16[2,16,2048]{2,1,0:T(8,128)(2,1)S(1)} %dynamic-slice_bitcast_fusion.3), channel_id=1, source_target_pairs={{0,28},{2,30},{4,0},{6,2},{8,4},{10,6},{12,8},{14,10},{16,12},{18,... | collective-permute-start | bytes 393224 | tf_op jit(solution)/shard_map/ppermute | solution.py:27
  135.6 28.3 %all-to-all-start.2 = ((bf16[4,16,2048]{2,1,0:T(8,128)(2,1)}), bf16[4,16,2048]{2,1,0:T(8,128)(2,1)S(1)}, u32[]{:S(2)}, u32[]{:S(2)}) async-start(bf16[4,16,2048]{2,1,0:T(8,128)(2,1)} %fusion.5), calls=%async_computation.2 | async-start | bytes 524288 | tf_op jit(solution)/shard_map/all_to_all | solution.py:80

commit v2 on v0

--- a/solution.py
+++ b/solution.py
@@ -1,6 +1,7 @@
 import jax
 import jax.numpy as jnp
 from jax import lax
+from jax.experimental.layout import Layout, with_layout_constraint
 from jax.sharding import Mesh
 from jax.sharding import PartitionSpec as P
 
@@ -43,6 +44,15 @@
     return jnp.concatenate([jnp.where(c == 0, mine, other), jnp.where(c == 0, other, mine)], axis=dim)
 
 
+def row_major(x):
+    return with_layout_constraint(x, Layout(major_to_minor=tuple(range(x.ndim))))
+
+
+def spread(x):
+    every = row_major(jnp.broadcast_to(x, (16, *x.shape)))
+    return row_major(lax.all_to_all(every, "fs", 0, 0, tiled=True)).reshape(D, x.shape[1])
+
+
 def gather_tokens(tokens):
     zh, zl, c = (lax.axis_index(a) for a in TP)
     x = tokens.T
@@ -74,7 +84,7 @@
     return by_core(c, keep, swap(give), 0)
 
 
-def scatter_sum(hidden, down):
+def scatter_sum(hidden, down, ready):
     _, zl, c = (lax.axis_index(a) for a in TP)
     hidden = hidden.reshape(16, 2, 16, 256)
     across = (((1,), (1,)), ((), ()))
@@ -87,25 +97,23 @@
     near = pick(pair, zl, 1).astype(F32)
     near += shift(ahead, 1).astype(F32) + shift(behind, -1).astype(F32)
     far = jnp.concatenate([shift(far[:2], 2), shift(far[2:], -2)], axis=0)
-    near = (near + far.astype(F32)).astype(BF)
+    near, ready = lax.optimization_barrier(((near + far.astype(F32)).astype(BF), ready))
     rows = lax.all_to_all(near, "zh", 0, 0, tiled=True)
-    return jnp.sum(rows.astype(F32), axis=0).astype(BF)
+    return (*ready, jnp.sum(rows.astype(F32), axis=0).astype(BF))
 
 
 def body(tokens, norm_gain, gate_train, up_train, down_train):
     gate_local = (norm_gain[:, None] * gate_train).astype(BF)
     up_local = (norm_gain[:, None] * up_train).astype(BF)
-    local = jnp.concatenate([gate_local, up_local, place_down(down_train)], axis=1)
-    every = lax.all_to_all(jnp.broadcast_to(local, (16, 128, 768)), "fs", 0, 0, tiled=True)
-    every = every.reshape(D, 768)
-    both, down = every[:, :512], every[:, 512:]
+    both = spread(jnp.concatenate([gate_local, up_local], axis=1))
+    down = spread(place_down(down_train))
     x = gather_tokens(tokens)
     wide = x.astype(F32)
     scale = lax.rsqrt(jnp.sum(wide * wide, axis=0) / D + EPS)[:, None]
     sums = lax.dot_general(x, both, (((0,), (0,)), ((), ())), preferred_element_type=F32)
     gate, up = sums[:, :256], sums[:, 256:]
     hidden = (jax.nn.silu(gate * scale) * (up * scale)).astype(BF)
-    return (both[:, :256], both[:, 256:], down.T, scatter_sum(hidden, down))
+    return scatter_sum(hidden, down, (both[:, :256], both[:, 256:], down.T))
 
 
 def solution(mesh):

time: 171 us -> 171 us (level)
  the two profiles are of different devices: /device:TPU:64 before, /device:TPU:65 now
where the time goes in v2:
time: 171 us; the launch traced here: 170 us
  starting transfers between devices  76.8 us (45%)
  waiting for transfers between devices  48.6 us (28%)
  blocking collectives  28 us (16%)
  local copies, waits for them, and re-layouts  7.6 us (4%)
  other arithmetic  4.6 us (3%)
  matrix products  3.79 us (2%)
    all_to_all x2, waiting for transfers between devices, spread(): lax.all_to_all(every, 'fs', 0, 0, tiled=True)  29.7 us
    all_to_all x1, blocking collectives, scatter_sum(): rows = lax.all_to_all(near, 'zh', 0, 0, tiled=True)  28 us
    ppermute x4, starting transfers between devices, fan(): return lax.ppermute(x, TP, pairs)  22 us
    ppermute x4, starting transfers between devices, shift(): return lax.ppermute(x, TP[:2], [(i, (i + by) % 16) for i in range(16)])  19 us
    ppermute x5, starting transfers between devices, swap(): return lax.ppermute(x, 'c', [(0, 1), (1, 0)])  16.9 us
    all_to_all x2, starting transfers between devices, spread(): lax.all_to_all(every, 'fs', 0, 0, tiled=True)  12.1 us
    ppermute x4, waiting for transfers between devices, fan(): return lax.ppermute(x, TP, pairs)  11 us
    ppermute x1, starting transfers between devices, place_down(): lax.ppermute(x, FS_TP[:3], [(a * 16 + b, (a ^ b) * 16 + b) for a, b in EV...  4.65 us
  transfers between devices with their start and end apart: 17, of which 9 were waited for; matrix products, arithmetic and copies ran while one was open for 8% of the time, Pallas kernels for 0%

profile of v2, /device:TPU:65, one launch (start us, length us, event | category | flops | bytes accessed | tf_op | source)
XLA Modules:
  0.0 170.5 jit_solution(12189706971452537766)
XLA Ops:
  0.6 2.6 %collective-permute-start = (bf16[64,512]{1,0:T(8,128)(2,1)}, bf16[64,512]{1,0:T(8,128)(2,1)S(1)}, u32[]{:S(2)}, u32[]{:S(2)}) collective-permute-start(bf16[64,512]{1,0:T(8,128)(2,1)} %bitcast.79), channel_id=1, source_target_pairs={{0,1},{1,0},{2,3},{3,2},{4,5},{5,4},{6,7},{7,6},{8,9},{9,8},{10,11... | collective-permute-start | bytes 196616 | tf_op jit(solution)/shard_map/ppermute | solution.py:40
  3.2 0.9 convert_bitcast_fusion
  4.1 4.7 %collective-permute-start.7 = (bf16[64,512]{1,0:T(8,128)(2,1)S(1)}, bf16[64,512]{1,0:T(8,128)(2,1)S(1)}, u32[]{:S(2)}, u32[]{:S(2)}) collective-permute-start(bf16[64,512]{1,0:T(8,128)(2,1)S(1)} %convert_bitcast_fusion), channel_id=1, source_target_pairs={{0,0},{2,34},{4,68},{6,102},{8,136},{10,170},{12,204},{14,238},{16... | collective-permute-start | bytes 196616 | tf_op jit(solution)/shard_map/ppermute | solution.py:81
  8.8 1.1 multiply_convert_fusion.1
  9.9 0.0 collective-permute-done
  9.9 0.9 broadcast_select_fusion.3
  10.8 13.1 %collective-permute-start.1 = (bf16[128,512]{1,0:T(8,128)(2,1)S(1)}, bf16[128,512]{1,0:T(8,128)(2,1)S(1)}, u32[]{:S(2)}, u32[]{:S(2)}) collective-permute-start(bf16[128,512]{1,0:T(8,128)(2,1)S(1)} %pad_maximum_fusion.2), channel_id=1, source_target_pairs={{0,8},{1,25},{2,10},{3,27},{4,12},{5,29},{6,14},{7,31},{8,16},{9,1... | collective-permute-start | bytes 393224 | tf_op jit(solution)/shard_map/ppermute | solution.py:36
  23.9 5.1 %collective-permute-start.2 = (bf16[128,256]{1,0:T(8,128)(2,1)S(1)}, bf16[128,256]{1,0:T(8,128)(2,1)S(1)}, u32[]{:S(2)}, u32[]{:S(2)}) collective-permute-start(bf16[128,256]{1,0:T(8,128)(2,1)S(1)} %fusion.9), channel_id=1, source_target_pairs={{0,16},{1,17},{2,18},{3,19},{4,20},{5,21},{6,22},{7,23},{8,24},{9,... | collective-permute-start | bytes 196616 | tf_op jit(solution)/shard_map/ppermute | solution.py:36
  29.0 0.0 collective-permute-done.7
  29.0 2.1 %collective-permute-start.8 = (bf16[64,512]{1,0:T(8,128)(2,1)S(1)}, bf16[64,512]{1,0:T(8,128)(2,1)S(1)}, u32[]{:S(2)}, u32[]{:S(2)}) collective-permute-start(bf16[64,512]{1,0:T(8,128)(2,1)S(1)} %collective-permute-done.7), channel_id=1, source_target_pairs={{0,0},{34,32},{68,64},{102,96},{136,128},{170,160},{204,192},{238,... | collective-permute-start | bytes 196616 | tf_op jit(solution)/shard_map/ppermute | solution.py:82
  31.2 7.1 %collective-permute-done.2 = bf16[128,256]{1,0:T(8,128)(2,1)S(1)} collective-permute-done((bf16[128,256]{1,0:T(8,128)(2,1)S(1)}, bf16[128,256]{1,0:T(8,128)(2,1)S(1)}, u32[]{:S(2)}, u32[]{:S(2)}) %collective-permute-start.2) | collective-permute-done | bytes 65568 | tf_op jit(solution)/shard_map/ppermute | solution.py:36
  38.4 0.0 collective-permute-done.1
  38.4 2.1 %collective-permute-start.3 = (bf16[128,768]{1,0:T(8,128)(2,1)S(1)}, bf16[128,768]{1,0:T(8,128)(2,1)S(1)}, u32[]{:S(2)}, u32[]{:S(2)}) collective-permute-start(bf16[128,768]{1,0:T(8,128)(2,1)S(1)} %pad_maximum_fusion.1), channel_id=1, source_target_pairs={{0,1},{1,0},{2,3},{3,2},{4,5},{5,4},{6,7},{7,6},{8,9},{9,8},{10,11... | collective-permute-start | bytes 589832 | tf_op jit(solution)/shard_map/ppermute | solution.py:40
  40.6 1.2 collective-permute-done.3
  41.8 1.9 %collective-permute-start.4 = (bf16[4,128,512]{2,1,0:T(8,128)(2,1)S(1)}, bf16[4,128,512]{2,1,0:T(8,128)(2,1)S(1)}, u32[]{:S(2)}, u32[]{:S(2)}) collective-permute-start(bf16[4,128,512]{2,1,0:T(8,128)(2,1)S(1)} %fusion.7), channel_id=1, source_target_pairs={{0,2},{1,31},{2,4},{3,1},{4,6},{5,3},{6,8},{7,5},{8,10},{9,7},{10,... | collective-permute-start | bytes 1572872 | tf_op jit(solution)/shard_map/ppermute | solution.py:36
  43.7 0.0 collective-permute-done.8
  43.7 5.4 %collective-permute-start.9 = (bf16[64,256]{1,0:T(8,128)(2,1)S(1)}, bf16[64,256]{1,0:T(8,128)(2,1)S(1)}, u32[]{:S(2)}, u32[]{:S(2)}) collective-permute-start(bf16[64,256]{1,0:T(8,128)(2,1)S(1)} %broadcast_select_fusion.6), channel_id=1, source_target_pairs={{0,1},{1,0},{2,3},{3,2},{4,5},{5,4},{6,7},{7,6},{8,9},{9,8},{10,11... | collective-permute-start | bytes 98312 | tf_op jit(solution)/shard_map/ppermute | solution.py:40
  49.1 1.9 %collective-permute-start.5 = (bf16[2,128,512]{2,1,0:T(8,128)(2,1)S(1)}, bf16[2,128,512]{2,1,0:T(8,128)(2,1)S(1)}, u32[]{:S(2)}, u32[]{:S(2)}) collective-permute-start(bf16[2,128,512]{2,1,0:T(8,128)(2,1)S(1)} %constant_dynamic-slice_fusion.2), channel_id=1, source_target_pairs={{0,4},{1,29},{2,6},{3,31},{4,8},{5,1},{6,10},{7,3},{8,12},{9,5},{1... | collective-permute-start | bytes 786440 | tf_op jit(solution)/shard_map/ppermute | solution.py:36
  51.1 1.5 broadcast_in_dim.53
  52.6 4.5 %all-to-all-start = ((bf16[16,128,512]{2,1,0:T(8,128)(2,1)}), bf16[16,128,512]{2,1,0:T(8,128)(2,1)}, u32[]{:S(2)}, u32[]{:S(2)}) async-start(bf16[16,128,512]{2,1,0:T(8,128)(2,1)} %broadcast_in_dim.53), calls=%async_computation | async-start | bytes 4194304 | tf_op jit(solution)/shard_map/all_to_all | solution.py:53
  57.2 0.0 collective-permute-done.9
  57.2 3.9 %collective-permute-done.5 = bf16[2,128,512]{2,1,0:T(8,128)(2,1)S(1)} collective-permute-done((bf16[2,128,512]{2,1,0:T(8,128)(2,1)S(1)}, bf16[2,128,512]{2,1,0:T(8,128)(2,1)S(1)}, u32[]{:S(2)}, u32[]{:S(2)}) %collective-permute-start.5) | collective-permute-done | bytes 262176 | tf_op jit(solution)/shard_map/ppermute | solution.py:36
  61.1 0.0 collective-permute-done.4
  61.1 0.1 pad_maximum_fusion
  61.2 1.9 %collective-permute-start.6 = (bf16[6,128,512]{2,1,0:T(8,128)(2,1)S(1)}, bf16[6,128,512]{2,1,0:T(8,128)(2,1)S(1)}, u32[]{:S(2)}, u32[]{:S(2)}) collective-permute-start(bf16[6,128,512]{2,1,0:T(8,128)(2,1)S(1)} %pad_maximum_fusion), channel_id=1, source_target_pairs={{0,1},{1,0},{2,3},{3,2},{4,5},{5,4},{6,7},{7,6},{8,9},{9,8},{10,11... | collective-permute-start | bytes 2359304 | tf_op jit(solution)/shard_map/ppermute | solution.py:40
  63.1 0.2 broadcast_in_dim.42
  63.5 1.9 %collective-permute-done.6 = bf16[6,128,512]{2,1,0:T(8,128)(2,1)S(1)} collective-permute-done((bf16[6,128,512]{2,1,0:T(8,128)(2,1)S(1)}, bf16[6,128,512]{2,1,0:T(8,128)(2,1)S(1)}, u32[]{:S(2)}, u32[]{:S(2)}) %collective-permute-start.6) | collective-permute-done | bytes 786464 | tf_op jit(solution)/shard_map/ppermute | solution.py:40
  65.4 0.5 multiply_reduce_fusion
  65.9 17.4 %all-to-all-done = bf16[16,128,512]{2,1,0:T(8,128)(2,1)} async-done(((bf16[16,128,512]{2,1,0:T(8,128)(2,1)}), bf16[16,128,512]{2,1,0:T(8,128)(2,1)}, u32[]{:S(2)}, u32[]{:S(2)}) %all-to-all-start) | async-done | bytes 2097184 | tf_op jit(solution)/shard_map/all_to_all | solution.py:53
  83.3 1.1 broadcast_in_dim.54
  84.4 7.6 %all-to-all-start.1 = ((bf16[16,128,256]{2,1,0:T(8,128)(2,1)}), bf16[16,128,256]{2,1,0:T(8,128)(2,1)S(1)}, u32[]{:S(2)}, u32[]{:S(2)}) async-start(bf16[16,128,256]{2,1,0:T(8,128)(2,1)} %broadcast_in_dim.54), calls=%async_computation.1 | async-start | bytes 2097152 | tf_op jit(solution)/shard_map/all_to_all | solution.py:53
  92.0 2.9 %fusion.12 = f32[512,512]{1,0:T(8,128)S(1)} fusion(bf16[2048,512]{1,0:T(8,128)(2,1)S(1)} %bitcast.71, bf16[2048,512]{1,0:T(8,128)(2,1)} %bitcast.15), kind=kOutput, calls=%fused_computation.56 | convolution fusion | flops 1073741824 | bytes 5242880 | tf_op jit(solution)/shard_map/dot_general | solution.py:113
  94.8 0.2 fusion.1
  95.1 12.4 %all-to-all-done.1 = bf16[16,128,256]{2,1,0:T(8,128)(2,1)S(1)} async-done(((bf16[16,128,256]{2,1,0:T(8,128)(2,1)}), bf16[16,128,256]{2,1,0:T(8,128)(2,1)S(1)}, u32[]{:S(2)}, u32[]{:S(2)}) %all-to-all-start.1) | async-done | bytes 1048608 | tf_op jit(solution)/shard_map/all_to_all | solution.py:53
  107.5 0.5 convolution_convert_fusion
  107.9 4.9 %collective-permute-start.10 = (bf16[256,2048]{1,0:T(8,128)(2,1)S(1)}, bf16[256,2048]{1,0:T(8,128)(2,1)S(1)}, u32[]{:S(2)}, u32[]{:S(2)}) collective-permute-start(bf16[256,2048]{1,0:T(8,128)(2,1)S(1)} %convolution_convert_fusion), channel_id=1, source_target_pairs={{0,1},{1,0},{2,3},{3,2},{4,5},{5,4},{6,7},{7,6},{8,9},{9,8},{10,11... | collective-permute-start | bytes 3145736 | tf_op jit(solution)/shard_map/ppermute | solution.py:40
  112.8 1.4 copy.18
  114.3 0.8 collective-permute-done.10
  115.1 0.5 add_convert_fusion
  115.6 0.1 dynamic-slice_bitcast_fusion
  115.7 2.1 %collective-permute-start.11 = (bf16[4,16,2048]{2,1,0:T(8,128)(2,1)S(1)}, bf16[4,16,2048]{2,1,0:T(8,128)(2,1)S(1)}, u32[]{:S(2)}, u32[]{:S(2)}) collective-permute-start(bf16[4,16,2048]{2,1,0:T(8,128)(2,1)S(1)} %get-tuple-element.16), channel_id=1, source_target_pairs={{0,2},{2,4},{4,6},{6,8},{8,10},{10,12},{12,14},{14,16},{16,18},{18... | collective-permute-start | bytes 786440 | tf_op jit(solution)/shard_map/ppermute | solution.py:31
  117.7 10.6 %collective-permute-start.12 = (bf16[4,16,2048]{2,1,0:T(8,128)(2,1)S(1)}, bf16[4,16,2048]{2,1,0:T(8,128)(2,1)S(1)}, u32[]{:S(2)}, u32[]{:S(2)}) collective-permute-start(bf16[4,16,2048]{2,1,0:T(8,128)(2,1)S(1)} %get-tuple-element.15), channel_id=1, source_target_pairs={{0,30},{2,0},{4,2},{6,4},{8,6},{10,8},{12,10},{14,12},{16,14},{18,... | collective-permute-start | bytes 786440 | tf_op jit(solution)/shard_map/ppermute | solution.py:31
  128.4 1.9 %collective-permute-start.13 = (bf16[2,16,2048]{2,1,0:T(8,128)(2,1)S(1)}, bf16[2,16,2048]{2,1,0:T(8,128)(2,1)S(1)}, u32[]{:S(2)}, u32[]{:S(2)}) collective-permute-start(bf16[2,16,2048]{2,1,0:T(8,128)(2,1)S(1)} %slice_bitcast_fusion.2), channel_id=1, source_target_pairs={{0,4},{2,6},{4,8},{6,10},{8,12},{10,14},{12,16},{14,18},{16,20},{1... | collective-permute-start | bytes 393224 | tf_op jit(solution)/shard_map/ppermute | solution.py:31
  130.3 4.4 %collective-permute-start.14 = (bf16[2,16,2048]{2,1,0:T(8,128)(2,1)S(1)}, bf16[2,16,2048]{2,1,0:T(8,128)(2,1)S(1)}, u32[]{:S(2)}, u32[]{:S(2)}) collective-permute-start(bf16[2,16,2048]{2,1,0:T(8,128)(2,1)S(1)} %dynamic-slice_bitcast_fusion.3), channel_id=1, source_target_pairs={{0,28},{2,30},{4,0},{6,2},{8,4},{10,6},{12,8},{14,10},{16,12},{18,... | collective-permute-start | bytes 393224 | tf_op jit(solution)/shard_map/ppermute | solution.py:31
  134.7 3.0 %fusion.11 = (bf16[2048,256]{1,0:T(8,128)(2,1)}, bf16[2048,256]{1,0:T(8,128)(2,1)}) fusion(bf16[2048,512]{1,0:T(8,128)(2,1)} %bitcast.15), kind=kLoop, calls=%fused_computation.55 | loop fusion | bytes 4194304 | tf_op jit(solution)/shard_map/slice | solution.py:116
  137.7 0.4 collective-permute-done.13
  138.1 3.5 %collective-permute-done.14 = bf16[2,16,2048]{2,1,0:T(8,128)(2,1)S(1)} collective-permute-done((bf16[2,16,2048]{2,1,0:T(8,128)(2,1)S(1)}, bf16[2,16,2048]{2,1,0:T(8,128)(2,1)S(1)}, u32[]{:S(2)}, u32[]{:S(2)}) %collective-permute-start.14) | collective-permute-done | bytes 131104 | tf_op jit(solution)/shard_map/ppermute | solution.py:31
  141.6 0.0 collective-permute-done.11
  141.6 0.0 collective-permute-done.12
  141.6 0.1 fusion.4
  141.8 28.0 %all_to_all.15 = bf16[4,16,2048]{2,1,0:T(8,128)(2,1)S(1)} all-to-all(bf16[4,16,2048]{2,1,0:T(8,128)(2,1)S(1)} %fusion.4), channel_id=1, replica_groups=mesh['fs'=16,'zh'=4,'zl'=4,'c'=2] {'zh'}, dimensions={0} | all-to-all | bytes 524288 | tf_op jit(solution)/shard_map/all_to_all | solution.py:101
  169.8 0.7 reduce_sum.22
  (23 shorter events, 0.5 us)
Async XLA Ops:
  0.6 9.3 %collective-permute-start = (bf16[64,512]{1,0:T(8,128)(2,1)}, bf16[64,512]{1,0:T(8,128)(2,1)S(1)}, u32[]{:S(2)}, u32[]{:S(2)}) collective-permute-start(bf16[64,512]{1,0:T(8,128)(2,1)} %bitcast.79), channel_id=1, source_target_pairs={{0,1},{1,0},{2,3},{3,2},{4,5},{5,4},{6,7},{7,6},{8,9},{9,8},{10,11... | collective-permute-start | bytes 196616 | tf_op jit(solution)/shard_map/ppermute | solution.py:40
  4.1 24.9 %collective-permute-start.7 = (bf16[64,512]{1,0:T(8,128)(2,1)S(1)}, bf16[64,512]{1,0:T(8,128)(2,1)S(1)}, u32[]{:S(2)}, u32[]{:S(2)}) collective-permute-start(bf16[64,512]{1,0:T(8,128)(2,1)S(1)} %convert_bitcast_fusion), channel_id=1, source_target_pairs={{0,0},{2,34},{4,68},{6,102},{8,136},{10,170},{12,204},{14,238},{16... | collective-permute-start | bytes 196616 | tf_op jit(solution)/shard_map/ppermute | solution.py:81
  10.8 27.6 %collective-permute-start.1 = (bf16[128,512]{1,0:T(8,128)(2,1)S(1)}, bf16[128,512]{1,0:T(8,128)(2,1)S(1)}, u32[]{:S(2)}, u32[]{:S(2)}) collective-permute-start(bf16[128,512]{1,0:T(8,128)(2,1)S(1)} %pad_maximum_fusion.2), channel_id=1, source_target_pairs={{0,8},{1,25},{2,10},{3,27},{4,12},{5,29},{6,14},{7,31},{8,16},{9,1... | collective-permute-start | bytes 393224 | tf_op jit(solution)/shard_map/ppermute | solution.py:36
  23.9 14.4 %collective-permute-start.2 = (bf16[128,256]{1,0:T(8,128)(2,1)S(1)}, bf16[128,256]{1,0:T(8,128)(2,1)S(1)}, u32[]{:S(2)}, u32[]{:S(2)}) collective-permute-start(bf16[128,256]{1,0:T(8,128)(2,1)S(1)} %fusion.9), channel_id=1, source_target_pairs={{0,16},{1,17},{2,18},{3,19},{4,20},{5,21},{6,22},{7,23},{8,24},{9,... | collective-permute-start | bytes 196616 | tf_op jit(solution)/shard_map/ppermute | solution.py:36
  29.0 14.7 %collective-permute-start.8 = (bf16[64,512]{1,0:T(8,128)(2,1)S(1)}, bf16[64,512]{1,0:T(8,128)(2,1)S(1)}, u32[]{:S(2)}, u32[]{:S(2)}) collective-permute-start(bf16[64,512]{1,0:T(8,128)(2,1)S(1)} %collective-permute-done.7), channel_id=1, source_target_pairs={{0,0},{34,32},{68,64},{102,96},{136,128},{170,160},{204,192},{238,... | collective-permute-start | bytes 196616 | tf_op jit(solution)/shard_map/ppermute | solution.py:82
  38.4 3.3 %collective-permute-start.3 = (bf16[128,768]{1,0:T(8,128)(2,1)S(1)}, bf16[128,768]{1,0:T(8,128)(2,1)S(1)}, u32[]{:S(2)}, u32[]{:S(2)}) collective-permute-start(bf16[128,768]{1,0:T(8,128)(2,1)S(1)} %pad_maximum_fusion.1), channel_id=1, source_target_pairs={{0,1},{1,0},{2,3},{3,2},{4,5},{5,4},{6,7},{7,6},{8,9},{9,8},{10,11... | collective-permute-start | bytes 589832 | tf_op jit(solution)/shard_map/ppermute | solution.py:40
  41.8 19.3 %collective-permute-start.4 = (bf16[4,128,512]{2,1,0:T(8,128)(2,1)S(1)}, bf16[4,128,512]{2,1,0:T(8,128)(2,1)S(1)}, u32[]{:S(2)}, u32[]{:S(2)}) collective-permute-start(bf16[4,128,512]{2,1,0:T(8,128)(2,1)S(1)} %fusion.7), channel_id=1, source_target_pairs={{0,2},{1,31},{2,4},{3,1},{4,6},{5,3},{6,8},{7,5},{8,10},{9,7},{10,... | collective-permute-start | bytes 1572872 | tf_op jit(solution)/shard_map/ppermute | solution.py:36
  43.7 13.4 %collective-permute-start.9 = (bf16[64,256]{1,0:T(8,128)(2,1)S(1)}, bf16[64,256]{1,0:T(8,128)(2,1)S(1)}, u32[]{:S(2)}, u32[]{:S(2)}) collective-permute-start(bf16[64,256]{1,0:T(8,128)(2,1)S(1)} %broadcast_select_fusion.6), channel_id=1, source_target_pairs={{0,1},{1,0},{2,3},{3,2},{4,5},{5,4},{6,7},{7,6},{8,9},{9,8},{10,11... | collective-permute-start | bytes 98312 | tf_op jit(solution)/shard_map/ppermute | solution.py:40
  49.1 11.9 %collective-permute-start.5 = (bf16[2,128,512]{2,1,0:T(8,128)(2,1)S(1)}, bf16[2,128,512]{2,1,0:T(8,128)(2,1)S(1)}, u32[]{:S(2)}, u32[]{:S(2)}) collective-permute-start(bf16[2,128,512]{2,1,0:T(8,128)(2,1)S(1)} %constant_dynamic-slice_fusion.2), channel_id=1, source_target_pairs={{0,4},{1,29},{2,6},{3,31},{4,8},{5,1},{6,10},{7,3},{8,12},{9,5},{1... | collective-permute-start | bytes 786440 | tf_op jit(solution)/shard_map/ppermute | solution.py:36
  52.6 30.7 %all-to-all-start = ((bf16[16,128,512]{2,1,0:T(8,128)(2,1)}), bf16[16,128,512]{2,1,0:T(8,128)(2,1)}, u32[]{:S(2)}, u32[]{:S(2)}) async-start(bf16[16,128,512]{2,1,0:T(8,128)(2,1)} %broadcast_in_dim.53), calls=%async_computation | async-start | bytes 4194304 | tf_op jit(solution)/shard_map/all_to_all | solution.py:53
  61.2 4.2 %collective-permute-start.6 = (bf16[6,128,512]{2,1,0:T(8,128)(2,1)S(1)}, bf16[6,128,512]{2,1,0:T(8,128)(2,1)S(1)}, u32[]{:S(2)}, u32[]{:S(2)}) collective-permute-start(bf16[6,128,512]{2,1,0:T(8,128)(2,1)S(1)} %pad_maximum_fusion), channel_id=1, source_target_pairs={{0,1},{1,0},{2,3},{3,2},{4,5},{5,4},{6,7},{7,6},{8,9},{9,8},{10,11... | collective-permute-start | bytes 2359304 | tf_op jit(solution)/shard_map/ppermute | solution.py:40
  84.4 23.1 %all-to-all-start.1 = ((bf16[16,128,256]{2,1,0:T(8,128)(2,1)}), bf16[16,128,256]{2,1,0:T(8,128)(2,1)S(1)}, u32[]{:S(2)}, u32[]{:S(2)}) async-start(bf16[16,128,256]{2,1,0:T(8,128)(2,1)} %broadcast_in_dim.54), calls=%async_computation.1 | async-start | bytes 2097152 | tf_op jit(solution)/shard_map/all_to_all | solution.py:53
  107.9 7.2 %collective-permute-start.10 = (bf16[256,2048]{1,0:T(8,128)(2,1)S(1)}, bf16[256,2048]{1,0:T(8,128)(2,1)S(1)}, u32[]{:S(2)}, u32[]{:S(2)}) collective-permute-start(bf16[256,2048]{1,0:T(8,128)(2,1)S(1)} %convolution_convert_fusion), channel_id=1, source_target_pairs={{0,1},{1,0},{2,3},{3,2},{4,5},{5,4},{6,7},{7,6},{8,9},{9,8},{10,11... | collective-permute-start | bytes 3145736 | tf_op jit(solution)/shard_map/ppermute | solution.py:40
  115.7 26.0 %collective-permute-start.11 = (bf16[4,16,2048]{2,1,0:T(8,128)(2,1)S(1)}, bf16[4,16,2048]{2,1,0:T(8,128)(2,1)S(1)}, u32[]{:S(2)}, u32[]{:S(2)}) collective-permute-start(bf16[4,16,2048]{2,1,0:T(8,128)(2,1)S(1)} %get-tuple-element.16), channel_id=1, source_target_pairs={{0,2},{2,4},{4,6},{6,8},{8,10},{10,12},{12,14},{14,16},{16,18},{18... | collective-permute-start | bytes 786440 | tf_op jit(solution)/shard_map/ppermute | solution.py:31
  117.7 23.9 %collective-permute-start.12 = (bf16[4,16,2048]{2,1,0:T(8,128)(2,1)S(1)}, bf16[4,16,2048]{2,1,0:T(8,128)(2,1)S(1)}, u32[]{:S(2)}, u32[]{:S(2)}) collective-permute-start(bf16[4,16,2048]{2,1,0:T(8,128)(2,1)S(1)} %get-tuple-element.15), channel_id=1, source_target_pairs={{0,30},{2,0},{4,2},{6,4},{8,6},{10,8},{12,10},{14,12},{16,14},{18,... | collective-permute-start | bytes 786440 | tf_op jit(solution)/shard_map/ppermute | solution.py:31
  128.4 9.7 %collective-permute-start.13 = (bf16[2,16,2048]{2,1,0:T(8,128)(2,1)S(1)}, bf16[2,16,2048]{2,1,0:T(8,128)(2,1)S(1)}, u32[]{:S(2)}, u32[]{:S(2)}) collective-permute-start(bf16[2,16,2048]{2,1,0:T(8,128)(2,1)S(1)} %slice_bitcast_fusion.2), channel_id=1, source_target_pairs={{0,4},{2,6},{4,8},{6,10},{8,12},{10,14},{12,16},{14,18},{16,20},{1... | collective-permute-start | bytes 393224 | tf_op jit(solution)/shard_map/ppermute | solution.py:31
  130.3 11.3 %collective-permute-start.14 = (bf16[2,16,2048]{2,1,0:T(8,128)(2,1)S(1)}, bf16[2,16,2048]{2,1,0:T(8,128)(2,1)S(1)}, u32[]{:S(2)}, u32[]{:S(2)}) collective-permute-start(bf16[2,16,2048]{2,1,0:T(8,128)(2,1)S(1)} %dynamic-slice_bitcast_fusion.3), channel_id=1, source_target_pairs={{0,28},{2,30},{4,0},{6,2},{8,4},{10,6},{12,8},{14,10},{16,12},{18,... | collective-permute-start | bytes 393224 | tf_op jit(solution)/shard_map/ppermute | solution.py:31

commit v3 on v2

--- a/solution.py
+++ b/solution.py
@@ -10,6 +10,7 @@
 TP = ("zh", "zl", "c")
 FS_TP = ("fs", "zh", "zl", "c")
 EPS = 1e-06
+SCALE = 8192.0
 BF = jnp.bfloat16
 F32 = jnp.float32
 EVERY = [(a, b) for a in range(16) for b in range(16)]
@@ -19,21 +20,12 @@
     return lax.dynamic_index_in_dim(x, i, dim, keepdims=False, allow_negative_indices=False)
 
 
-def part_of(x, at, size, dim):
-    return lax.dynamic_slice_in_dim(x, at, size, dim, allow_negative_indices=False)
-
-
 def put(whole, part, at):
     return lax.dynamic_update_slice(whole, part, at, allow_negative_indices=False)
 
 
 def shift(x, by):
     return lax.ppermute(x, TP[:2], [(i, (i + by) % 16) for i in range(16)])
-
-
-def fan(x, by):
-    pairs = [(2 * z + c, 2 * ((z + (by, -by)[c]) % 16) + c) for z in range(16) for c in range(2)]
-    return lax.ppermute(x, TP, pairs)
 
 
 def swap(x):
@@ -54,25 +46,13 @@
 
 
 def gather_tokens(tokens):
-    zh, zl, c = (lax.axis_index(a) for a in TP)
-    x = tokens.T
-    chip = by_core(c, x, swap(x), 0)
-    p = fan(chip, 4)
-    q = fan(jnp.where(c == 0, chip[:, :256], chip[:, 256:]), 8)
-    o = swap(jnp.concatenate([p, q], axis=1))
-    own = put(jnp.zeros((4, 128, 512), BF), chip[None], (zh, 0, 0))
-    own = put(own, p[None], ((zh + 3 + 2 * c) & 3, 0, 0))
-    own = put(own, o[None, :, :512], ((zh + 1 + 2 * c) & 3, 0, 0))
-    own = put(own, by_core(c, q, o[:, 512:], 1)[None], ((zh + 2) & 3, 0, 0))
-    n = fan(own, 1)
-    f = fan(part_of(own, 2 * c, 2, 0), 2)
-    o = swap(jnp.concatenate([n, f], axis=0))
-    whole = put(jnp.zeros((4, 4, 128, 512), BF), own[:, None], (0, zl, 0, 0))
-    whole = put(whole, n[:, None], (0, (zl + 3 + 2 * c) & 3, 0, 0))
-    whole = put(whole, f[:, None], (2 * c, (zl + 2) & 3, 0, 0))
-    whole = put(whole, o[:4, None], (0, (zl + 1 + 2 * c) & 3, 0, 0))
-    whole = put(whole, o[4:, None], (2 - 2 * c, (zl + 2) & 3, 0, 0))
-    return whole.reshape(D, 512)
+    c = lax.axis_index("c")
+    x = (tokens.T.astype(F32) * SCALE).astype(jnp.float16)
+    mine = lax.all_gather(x, TP[:2])[:, None]
+    other = swap(mine)
+    mine, other = ((v.astype(F32) / SCALE).astype(BF) for v in (mine, other))
+    whole = put(jnp.zeros((16, 2, 64, 512), BF), mine, (0, c, 0, 0))
+    return put(whole, other, (0, 1 - c, 0, 0)).reshape(D, 512)
 
 
 def place_down(down_train):

time: 171 us -> 164 us (0.959)
  the two profiles are of different devices: /device:TPU:65 before, /device:TPU:32 now
where the time goes in v3:
time: 164 us; the launch traced here: 163 us
  blocking collectives  74.2 us (45%)
  starting transfers between devices  48 us (29%)
  waiting for transfers between devices  23.4 us (14%)
  local copies, waits for them, and re-layouts  7.49 us (5%)
  other arithmetic  5.64 us (3%)
  matrix products  3.79 us (2%)
    all_gather x1, blocking collectives, gather_tokens(): mine = lax.all_gather(x, TP[:2])[:, None]  45.5 us
    all_to_all x1, blocking collectives, scatter_sum(): rows = lax.all_to_all(near, 'zh', 0, 0, tiled=True)  28.7 us
    all_to_all x2, starting transfers between devices, spread(): lax.all_to_all(every, 'fs', 0, 0, tiled=True)  21 us
    ppermute x4, starting transfers between devices, shift(): return lax.ppermute(x, TP[:2], [(i, (i + by) % 16) for i in range(16)])  15.2 us
    all_to_all x2, waiting for transfers between devices, spread(): lax.all_to_all(every, 'fs', 0, 0, tiled=True)  14.7 us
    ppermute x3, starting transfers between devices, swap(): return lax.ppermute(x, 'c', [(0, 1), (1, 0)])  5.75 us
    ppermute x1, starting transfers between devices, place_down(): lax.ppermute(x, FS_TP[:3], [(a * 16 + b, (a ^ b) * 16 + b) for a, b in EV...  3.78 us
    ppermute x1, waiting for transfers between devices, place_down(): lax.ppermute(x, FS_TP[:3], [((a ^ b) * 16 + b, b * 16 + a) for a, b in EV...  3.52 us
  transfers between devices with their start and end apart: 11, of which 5 were waited for; matrix products, arithmetic and copies ran while one was open for 7% of the time, Pallas kernels for 0%

profile of v3, /device:TPU:32, one launch (start us, length us, event | category | flops | bytes accessed | tf_op | source)
XLA Modules:
  0.0 163.5 jit_solution(10056871695844611885)
XLA Ops:
  0.6 1.1 multiply_convert_fusion.3
  1.7 1.5 broadcast_in_dim.17
  3.3 0.0 copy-start
  3.3 0.0 copy-start.1
  3.3 7.2 %all-to-all-start = ((bf16[16,128,512]{2,1,0:T(8,128)(2,1)}), bf16[16,128,512]{2,1,0:T(8,128)(2,1)}, u32[]{:S(2)}, u32[]{:S(2)}) async-start(bf16[16,128,512]{2,1,0:T(8,128)(2,1)} %broadcast_in_dim.17), calls=%async_computation | async-start | bytes 4194304 | tf_op jit(solution)/shard_map/all_to_all | solution.py:45
  10.5 0.0 copy-done
  10.5 3.8 %collective-permute-start.1 = (bf16[64,512]{1,0:T(8,128)(2,1)S(1)}, bf16[64,512]{1,0:T(8,128)(2,1)S(1)}, u32[]{:S(2)}, u32[]{:S(2)}) collective-permute-start(bf16[64,512]{1,0:T(8,128)(2,1)S(1)} %convert_bitcast_fusion), channel_id=1, source_target_pairs={{0,0},{2,34},{4,68},{6,102},{8,136},{10,170},{12,204},{14,238},{16... | collective-permute-start | bytes 196616 | tf_op jit(solution)/shard_map/ppermute | solution.py:61
  14.3 0.0 copy-done.1
  14.3 45.5 %all-gather.2 = f16[1024,512]{1,0:T(8,128)(2,1)} all-gather(f16[64,512]{1,0:T(8,128)(2,1)S(1)} %fusion.5), channel_id=2, replica_groups=mesh['fs'=16,'zh'=4,'zl'=4,'c'=2] {'zh','zl'}, dimensions={0}, use_global_device_ids=true | all-gather | bytes 1114112 | tf_op jit(solution)/shard_map/all_gather | solution.py:51
  59.8 1.9 %collective-permute-start = (f16[16,1,64,512]{3,2,1,0:T(8,128)(2,1)}, f16[16,1,64,512]{3,2,1,0:T(8,128)(2,1)}, u32[]{:S(2)}, u32[]{:S(2)}) collective-permute-start(f16[16,1,64,512]{3,2,1,0:T(8,128)(2,1)} %bitcast.2), channel_id=1, source_target_pairs={{0,1},{1,0},{2,3},{3,2},{4,5},{5,4},{6,7},{7,6},{8,9},{9,8},{10,11... | collective-permute-start | bytes 3145736 | tf_op jit(solution)/shard_map/ppermute | solution.py:32
  61.8 0.0 collective-permute-done.1
  61.8 2.3 %collective-permute-start.2 = (bf16[64,512]{1,0:T(8,128)(2,1)S(1)}, bf16[64,512]{1,0:T(8,128)(2,1)S(1)}, u32[]{:S(2)}, u32[]{:S(2)}) collective-permute-start(bf16[64,512]{1,0:T(8,128)(2,1)S(1)} %collective-permute-done.1), channel_id=1, source_target_pairs={{0,0},{34,32},{68,64},{102,96},{136,128},{170,160},{204,192},{238,... | collective-permute-start | bytes 196616 | tf_op jit(solution)/shard_map/ppermute | solution.py:62
  64.1 1.4 multiply_convert_fusion
  65.5 3.5 %collective-permute-done.2 = bf16[64,512]{1,0:T(8,128)(2,1)S(1)} collective-permute-done((bf16[64,512]{1,0:T(8,128)(2,1)S(1)}, bf16[64,512]{1,0:T(8,128)(2,1)S(1)}, u32[]{:S(2)}, u32[]{:S(2)}) %collective-permute-start.2) | collective-permute-done | bytes 65568 | tf_op jit(solution)/shard_map/ppermute | solution.py:62
  69.1 1.9 %collective-permute-start.3 = (bf16[64,256]{1,0:T(8,128)(2,1)S(1)}, bf16[64,256]{1,0:T(8,128)(2,1)S(1)}, u32[]{:S(2)}, u32[]{:S(2)}) collective-permute-start(bf16[64,256]{1,0:T(8,128)(2,1)S(1)} %broadcast_select_fusion.2), channel_id=1, source_target_pairs={{0,1},{1,0},{2,3},{3,2},{4,5},{5,4},{6,7},{7,6},{8,9},{9,8},{10,11... | collective-permute-start | bytes 98312 | tf_op jit(solution)/shard_map/ppermute | solution.py:32
  71.0 0.2 broadcast_in_dim.15
  71.2 0.1 constant_dynamic-update-slice_fusion
  71.4 0.8 collective-permute-done.3
  72.2 0.0 collective-permute-done
  72.2 1.5 fusion
  73.7 0.6 multiply_reduce_fusion
  74.2 0.0 all-to-all-done
  74.3 1.1 broadcast_in_dim.18
  75.3 13.7 %all-to-all-start.1 = ((bf16[16,128,256]{2,1,0:T(8,128)(2,1)}), bf16[16,128,256]{2,1,0:T(8,128)(2,1)S(1)}, u32[]{:S(2)}, u32[]{:S(2)}) async-start(bf16[16,128,256]{2,1,0:T(8,128)(2,1)} %broadcast_in_dim.18), calls=%async_computation.1 | async-start | bytes 2097152 | tf_op jit(solution)/shard_map/all_to_all | solution.py:45
  89.1 2.9 %fusion.7 = f32[512,512]{1,0:T(8,128)S(1)} fusion(bf16[2048,512]{1,0:T(8,128)(2,1)S(1)} %bitcast.38, bf16[2048,512]{1,0:T(8,128)(2,1)} %bitcast.4), kind=kOutput, calls=%fused_computation.34 | convolution fusion | flops 1073741824 | bytes 5242880 | tf_op jit(solution)/shard_map/dot_general | solution.py:93
  92.0 0.2 fusion.2
  92.2 14.7 %all-to-all-done.1 = bf16[16,128,256]{2,1,0:T(8,128)(2,1)S(1)} async-done(((bf16[16,128,256]{2,1,0:T(8,128)(2,1)}), bf16[16,128,256]{2,1,0:T(8,128)(2,1)S(1)}, u32[]{:S(2)}, u32[]{:S(2)}) %all-to-all-start.1) | async-done | bytes 1048608 | tf_op jit(solution)/shard_map/all_to_all | solution.py:45
  106.9 0.5 convolution_convert_fusion
  107.4 1.9 %collective-permute-start.4 = (bf16[256,2048]{1,0:T(8,128)(2,1)S(1)}, bf16[256,2048]{1,0:T(8,128)(2,1)S(1)}, u32[]{:S(2)}, u32[]{:S(2)}) collective-permute-start(bf16[256,2048]{1,0:T(8,128)(2,1)S(1)} %convolution_convert_fusion), channel_id=1, source_target_pairs={{0,1},{1,0},{2,3},{3,2},{4,5},{5,4},{6,7},{7,6},{8,9},{9,8},{10,11... | collective-permute-start | bytes 3145736 | tf_op jit(solution)/shard_map/ppermute | solution.py:32
  109.3 1.4 copy.14
  110.7 1.2 collective-permute-done.4
  111.9 0.5 add_convert_fusion
  112.4 0.1 dynamic-slice_bitcast_fusion
  112.5 1.9 %collective-permute-start.5 = (bf16[4,16,2048]{2,1,0:T(8,128)(2,1)S(1)}, bf16[4,16,2048]{2,1,0:T(8,128)(2,1)S(1)}, u32[]{:S(2)}, u32[]{:S(2)}) collective-permute-start(bf16[4,16,2048]{2,1,0:T(8,128)(2,1)S(1)} %get-tuple-element.16), channel_id=1, source_target_pairs={{0,2},{2,4},{4,6},{6,8},{8,10},{10,12},{12,14},{14,16},{16,18},{18... | collective-permute-start | bytes 786440 | tf_op jit(solution)/shard_map/ppermute | solution.py:28
  114.4 3.9 %collective-permute-start.6 = (bf16[4,16,2048]{2,1,0:T(8,128)(2,1)S(1)}, bf16[4,16,2048]{2,1,0:T(8,128)(2,1)S(1)}, u32[]{:S(2)}, u32[]{:S(2)}) collective-permute-start(bf16[4,16,2048]{2,1,0:T(8,128)(2,1)S(1)} %get-tuple-element.15), channel_id=1, source_target_pairs={{0,30},{2,0},{4,2},{6,4},{8,6},{10,8},{12,10},{14,12},{16,14},{18,... | collective-permute-start | bytes 786440 | tf_op jit(solution)/shard_map/ppermute | solution.py:28
  118.4 1.9 %collective-permute-start.7 = (bf16[2,16,2048]{2,1,0:T(8,128)(2,1)S(1)}, bf16[2,16,2048]{2,1,0:T(8,128)(2,1)S(1)}, u32[]{:S(2)}, u32[]{:S(2)}) collective-permute-start(bf16[2,16,2048]{2,1,0:T(8,128)(2,1)S(1)} %slice_bitcast_fusion), channel_id=1, source_target_pairs={{0,4},{2,6},{4,8},{6,10},{8,12},{10,14},{12,16},{14,18},{16,20},{1... | collective-permute-start | bytes 393224 | tf_op jit(solution)/shard_map/ppermute | solution.py:28
  120.3 7.4 %collective-permute-start.8 = (bf16[2,16,2048]{2,1,0:T(8,128)(2,1)S(1)}, bf16[2,16,2048]{2,1,0:T(8,128)(2,1)S(1)}, u32[]{:S(2)}, u32[]{:S(2)}) collective-permute-start(bf16[2,16,2048]{2,1,0:T(8,128)(2,1)S(1)} %dynamic-slice_bitcast_fusion.3), channel_id=1, source_target_pairs={{0,28},{2,30},{4,0},{6,2},{8,4},{10,6},{12,8},{14,10},{16,12},{18,... | collective-permute-start | bytes 393224 | tf_op jit(solution)/shard_map/ppermute | solution.py:28
  127.7 3.0 %fusion.6 = (bf16[2048,256]{1,0:T(8,128)(2,1)}, bf16[2048,256]{1,0:T(8,128)(2,1)}) fusion(bf16[2048,512]{1,0:T(8,128)(2,1)} %bitcast.4), kind=kLoop, calls=%fused_computation.33 | loop fusion | bytes 4194304 | tf_op jit(solution)/shard_map/slice | solution.py:96
  130.7 0.0 collective-permute-done.7
  130.7 3.2 %collective-permute-done.8 = bf16[2,16,2048]{2,1,0:T(8,128)(2,1)S(1)} collective-permute-done((bf16[2,16,2048]{2,1,0:T(8,128)(2,1)S(1)}, bf16[2,16,2048]{2,1,0:T(8,128)(2,1)S(1)}, u32[]{:S(2)}, u32[]{:S(2)}) %collective-permute-start.8) | collective-permute-done | bytes 131104 | tf_op jit(solution)/shard_map/ppermute | solution.py:28
  133.9 0.0 collective-permute-done.5
  133.9 0.0 collective-permute-done.6
  133.9 0.1 fusion.4
  134.1 28.7 %all_to_all.15 = bf16[4,16,2048]{2,1,0:T(8,128)(2,1)S(1)} all-to-all(bf16[4,16,2048]{2,1,0:T(8,128)(2,1)S(1)} %fusion.4), channel_id=1, replica_groups=mesh['fs'=16,'zh'=4,'zl'=4,'c'=2] {'zh'}, dimensions={0} | all-to-all | bytes 524288 | tf_op jit(solution)/shard_map/all_to_all | solution.py:81
  162.8 0.7 reduce_sum.22
  (10 shorter events, 0.1 us)
Async XLA Ops:
  3.3 7.2 %copy-start = (f32[512,64]{0,1:T(8,128)S(1)}, f32[512,64]{0,1:T(8,128)}, u32[]{:S(2)}) copy-start(f32[512,64]{0,1:T(8,128)} %param.9) | copy-start | bytes 393220
  3.3 11.0 %copy-start.1 = (bf16[512,64]{0,1:T(8,128)(2,1)S(1)}, bf16[512,64]{0,1:T(8,128)(2,1)}, u32[]{:S(2)}) copy-start(bf16[512,64]{0,1:T(8,128)(2,1)} %param.5) | copy-start | bytes 196612
  3.3 71.0 %all-to-all-start = ((bf16[16,128,512]{2,1,0:T(8,128)(2,1)}), bf16[16,128,512]{2,1,0:T(8,128)(2,1)}, u32[]{:S(2)}, u32[]{:S(2)}) async-start(bf16[16,128,512]{2,1,0:T(8,128)(2,1)} %broadcast_in_dim.17), calls=%async_computation | async-start | bytes 4194304 | tf_op jit(solution)/shard_map/all_to_all | solution.py:45
  10.5 51.3 %collective-permute-start.1 = (bf16[64,512]{1,0:T(8,128)(2,1)S(1)}, bf16[64,512]{1,0:T(8,128)(2,1)S(1)}, u32[]{:S(2)}, u32[]{:S(2)}) collective-permute-start(bf16[64,512]{1,0:T(8,128)(2,1)S(1)} %convert_bitcast_fusion), channel_id=1, source_target_pairs={{0,0},{2,34},{4,68},{6,102},{8,136},{10,170},{12,204},{14,238},{16... | collective-permute-start | bytes 196616 | tf_op jit(solution)/shard_map/ppermute | solution.py:61
  59.8 12.4 %collective-permute-start = (f16[16,1,64,512]{3,2,1,0:T(8,128)(2,1)}, f16[16,1,64,512]{3,2,1,0:T(8,128)(2,1)}, u32[]{:S(2)}, u32[]{:S(2)}) collective-permute-start(f16[16,1,64,512]{3,2,1,0:T(8,128)(2,1)} %bitcast.2), channel_id=1, source_target_pairs={{0,1},{1,0},{2,3},{3,2},{4,5},{5,4},{6,7},{7,6},{8,9},{9,8},{10,11... | collective-permute-start | bytes 3145736 | tf_op jit(solution)/shard_map/ppermute | solution.py:32
  61.8 7.3 %collective-permute-start.2 = (bf16[64,512]{1,0:T(8,128)(2,1)S(1)}, bf16[64,512]{1,0:T(8,128)(2,1)S(1)}, u32[]{:S(2)}, u32[]{:S(2)}) collective-permute-start(bf16[64,512]{1,0:T(8,128)(2,1)S(1)} %collective-permute-done.1), channel_id=1, source_target_pairs={{0,0},{34,32},{68,64},{102,96},{136,128},{170,160},{204,192},{238,... | collective-permute-start | bytes 196616 | tf_op jit(solution)/shard_map/ppermute | solution.py:62
  69.1 3.1 %collective-permute-start.3 = (bf16[64,256]{1,0:T(8,128)(2,1)S(1)}, bf16[64,256]{1,0:T(8,128)(2,1)S(1)}, u32[]{:S(2)}, u32[]{:S(2)}) collective-permute-start(bf16[64,256]{1,0:T(8,128)(2,1)S(1)} %broadcast_select_fusion.2), channel_id=1, source_target_pairs={{0,1},{1,0},{2,3},{3,2},{4,5},{5,4},{6,7},{7,6},{8,9},{9,8},{10,11... | collective-permute-start | bytes 98312 | tf_op jit(solution)/shard_map/ppermute | solution.py:32
  75.3 31.6 %all-to-all-start.1 = ((bf16[16,128,256]{2,1,0:T(8,128)(2,1)}), bf16[16,128,256]{2,1,0:T(8,128)(2,1)S(1)}, u32[]{:S(2)}, u32[]{:S(2)}) async-start(bf16[16,128,256]{2,1,0:T(8,128)(2,1)} %broadcast_in_dim.18), calls=%async_computation.1 | async-start | bytes 2097152 | tf_op jit(solution)/shard_map/all_to_all | solution.py:45
  107.4 4.6 %collective-permute-start.4 = (bf16[256,2048]{1,0:T(8,128)(2,1)S(1)}, bf16[256,2048]{1,0:T(8,128)(2,1)S(1)}, u32[]{:S(2)}, u32[]{:S(2)}) collective-permute-start(bf16[256,2048]{1,0:T(8,128)(2,1)S(1)} %convolution_convert_fusion), channel_id=1, source_target_pairs={{0,1},{1,0},{2,3},{3,2},{4,5},{5,4},{6,7},{7,6},{8,9},{9,8},{10,11... | collective-permute-start | bytes 3145736 | tf_op jit(solution)/shard_map/ppermute | solution.py:32
  112.5 21.5 %collective-permute-start.5 = (bf16[4,16,2048]{2,1,0:T(8,128)(2,1)S(1)}, bf16[4,16,2048]{2,1,0:T(8,128)(2,1)S(1)}, u32[]{:S(2)}, u32[]{:S(2)}) collective-permute-start(bf16[4,16,2048]{2,1,0:T(8,128)(2,1)S(1)} %get-tuple-element.16), channel_id=1, source_target_pairs={{0,2},{2,4},{4,6},{6,8},{8,10},{10,12},{12,14},{14,16},{16,18},{18... | collective-permute-start | bytes 786440 | tf_op jit(solution)/shard_map/ppermute | solution.py:28
  114.4 19.5 %collective-permute-start.6 = (bf16[4,16,2048]{2,1,0:T(8,128)(2,1)S(1)}, bf16[4,16,2048]{2,1,0:T(8,128)(2,1)S(1)}, u32[]{:S(2)}, u32[]{:S(2)}) collective-permute-start(bf16[4,16,2048]{2,1,0:T(8,128)(2,1)S(1)} %get-tuple-element.15), channel_id=1, source_target_pairs={{0,30},{2,0},{4,2},{6,4},{8,6},{10,8},{12,10},{14,12},{16,14},{18,... | collective-permute-start | bytes 786440 | tf_op jit(solution)/shard_map/ppermute | solution.py:28
  118.4 12.3 %collective-permute-start.7 = (bf16[2,16,2048]{2,1,0:T(8,128)(2,1)S(1)}, bf16[2,16,2048]{2,1,0:T(8,128)(2,1)S(1)}, u32[]{:S(2)}, u32[]{:S(2)}) collective-permute-start(bf16[2,16,2048]{2,1,0:T(8,128)(2,1)S(1)} %slice_bitcast_fusion), channel_id=1, source_target_pairs={{0,4},{2,6},{4,8},{6,10},{8,12},{10,14},{12,16},{14,18},{16,20},{1... | collective-permute-start | bytes 393224 | tf_op jit(solution)/shard_map/ppermute | solution.py:28
  120.3 13.6 %collective-permute-start.8 = (bf16[2,16,2048]{2,1,0:T(8,128)(2,1)S(1)}, bf16[2,16,2048]{2,1,0:T(8,128)(2,1)S(1)}, u32[]{:S(2)}, u32[]{:S(2)}) collective-permute-start(bf16[2,16,2048]{2,1,0:T(8,128)(2,1)S(1)} %dynamic-slice_bitcast_fusion.3), channel_id=1, source_target_pairs={{0,28},{2,30},{4,0},{6,2},{8,4},{10,6},{12,8},{14,10},{16,12},{18,... | collective-permute-start | bytes 393224 | tf_op jit(solution)/shard_map/ppermute | solution.py:28

commit v4 on v3

--- a/solution.py
+++ b/solution.py
@@ -40,11 +40,6 @@
     return with_layout_constraint(x, Layout(major_to_minor=tuple(range(x.ndim))))
 
 
-def spread(x):
-    every = row_major(jnp.broadcast_to(x, (16, *x.shape)))
-    return row_major(lax.all_to_all(every, "fs", 0, 0, tiled=True)).reshape(D, x.shape[1])
-
-
 def gather_tokens(tokens):
     c = lax.axis_index("c")
     x = (tokens.T.astype(F32) * SCALE).astype(jnp.float16)
@@ -58,10 +53,10 @@
 def place_down(down_train):
     c = lax.axis_index("c")
     x = down_train.astype(BF).T
+    keep, give = jnp.where(c == 0, x[:, :256], x[:, 256:]), jnp.where(c == 0, x[:, 256:], x[:, :256])
+    x = by_core(c, keep, swap(give), 0)
     x = lax.ppermute(x, FS_TP[:3], [(a * 16 + b, (a ^ b) * 16 + b) for a, b in EVERY])
-    x = lax.ppermute(x, FS_TP[:3], [((a ^ b) * 16 + b, b * 16 + a) for a, b in EVERY])
-    keep, give = jnp.where(c == 0, x[:, :256], x[:, 256:]), jnp.where(c == 0, x[:, 256:], x[:, :256])
-    return by_core(c, keep, swap(give), 0)
+    return lax.ppermute(x, FS_TP[:3], [((a ^ b) * 16 + b, b * 16 + a) for a, b in EVERY])
 
 
 def scatter_sum(hidden, down, ready):
@@ -85,8 +80,12 @@
 def body(tokens, norm_gain, gate_train, up_train, down_train):
     gate_local = (norm_gain[:, None] * gate_train).astype(BF)
     up_local = (norm_gain[:, None] * up_train).astype(BF)
-    both = spread(jnp.concatenate([gate_local, up_local], axis=1))
-    down = spread(place_down(down_train))
+    local = jnp.concatenate([gate_local, up_local, jnp.zeros((128, 256), BF)], axis=1)
+    every = lax.optimization_barrier(row_major(jnp.broadcast_to(local, (16, 128, 768))))
+    down = jnp.broadcast_to(place_down(down_train), (16, 128, 256))
+    every = lax.dynamic_update_slice(every, down, (0, 0, 512))
+    every = row_major(lax.all_to_all(every, "fs", 0, 0, tiled=True)).reshape(D, 768)
+    both, down = every[:, :512], every[:, 512:]
     x = gather_tokens(tokens)
     wide = x.astype(F32)
     scale = lax.rsqrt(jnp.sum(wide * wide, axis=0) / D + EPS)[:, None]

time: 164 us -> 155 us (0.945)
  waiting for transfers between devices: 23.4 us -> 13.7 us
  blocking collectives: 74.2 us -> 67.6 us
  local copies, waits for them, and re-layouts: 7.49 us -> 10.5 us
  matrix products: 3.79 us -> 6 us
  other arithmetic: 5.64 us -> 7.68 us
    all_to_all x2 -> x1, waiting for transfers between devices: 14.7 us -> 0.01 us  [body(): lax.all_to_all(every, 'fs', 0, 0, tiled=True)]
    all_gather x1, blocking collectives: 45.5 us -> 40.3 us  [gather_tokens(): mine = lax.all_gather(x, TP[:2])[:, None]]
    unnamed x4 -> x8, local copies, waits for them, and re-layouts: 0.01 us -> 4.77 us
    ppermute x3, waiting for transfers between devices: 2.01 us -> 5.18 us  [swap(): return lax.ppermute(x, 'c', [(0, 1), (1, 0)])]
    slice x1 -> x0, local copies, waits for them, and re-layouts: 2.99 us -> none  [body(): return scatter_sum(hidden, down, (both[:, :256], both[:, 256:], down.T))]
    ppermute x4, waiting for transfers between devices: 3.25 us -> 5.23 us  [shift(): return lax.ppermute(x, TP[:2], [(i, (i + by) % 16) for i in range(16)])]
    ppermute x1, waiting for transfers between devices: 3.52 us -> 1.67 us  [place_down(): lax.ppermute(x, FS_TP[:3], [((a ^ b) * 16 + b, b * 16 + a) for a, b in EV...]
    ppermute x1, waiting for transfers between devices: 0.01 us -> 1.65 us  [place_down(): lax.ppermute(x, FS_TP[:3], [(a * 16 + b, (a ^ b) * 16 + b) for a, b in EV...]
  transfers between devices with their start and end apart: 11 -> 10, of which waited for: 5 -> 6; matrix products, arithmetic and copies ran while one was open for 7% -> 8% of each run, Pallas kernels for 0% -> 0%
where the time goes in v4:
time: 155 us; the launch traced here: 154 us
  blocking collectives  67.6 us (44%)
  starting transfers between devices  47.8 us (31%)
  waiting for transfers between devices  13.7 us (9%)
  local copies, waits for them, and re-layouts  10.5 us (7%)
  other arithmetic  7.68 us (5%)
  matrix products  6 us (4%)
    all_gather x1, blocking collectives, gather_tokens(): mine = lax.all_gather(x, TP[:2])[:, None]  40.3 us
    all_to_all x1, blocking collectives, scatter_sum(): rows = lax.all_to_all(near, 'zh', 0, 0, tiled=True)  27.3 us
    all_to_all x1, starting transfers between devices, body(): lax.all_to_all(every, 'fs', 0, 0, tiled=True)  21.6 us
    ppermute x4, starting transfers between devices, shift(): return lax.ppermute(x, TP[:2], [(i, (i + by) % 16) for i in range(16)])  13.5 us
    ppermute x3, starting transfers between devices, swap(): return lax.ppermute(x, 'c', [(0, 1), (1, 0)])  5.87 us
    ppermute x4, waiting for transfers between devices, shift(): return lax.ppermute(x, TP[:2], [(i, (i + by) % 16) for i in range(16)])  5.23 us
    ppermute x3, waiting for transfers between devices, swap(): return lax.ppermute(x, 'c', [(0, 1), (1, 0)])  5.18 us
    unnamed x8, local copies, waits for them, and re-layouts  4.77 us
  transfers between devices with their start and end apart: 10, of which 6 were waited for; matrix products, arithmetic and copies ran while one was open for 8% of the time, Pallas kernels for 0%

profile of v4, /device:TPU:32, one launch (start us, length us, event | category | flops | bytes accessed | tf_op | source)
XLA Modules:
  0.0 154.2 jit_solution(2392615947487890648)
XLA Ops:
  0.6 0.9 convert_bitcast_fusion
  1.6 1.9 %collective-permute-start.1 = (bf16[64,256]{1,0:T(8,128)(2,1)S(1)}, bf16[64,256]{1,0:T(8,128)(2,1)S(1)}, u32[]{:S(2)}, u32[]{:S(2)}) collective-permute-start(bf16[64,256]{1,0:T(8,128)(2,1)S(1)} %broadcast_select_fusion.2), channel_id=1, source_target_pairs={{0,1},{1,0},{2,3},{3,2},{4,5},{5,4},{6,7},{7,6},{8,9},{9,8},{10,11... | collective-permute-start | bytes 98312 | tf_op jit(solution)/shard_map/ppermute | solution.py:32
  3.5 1.2 collective-permute-done.1
  4.7 3.4 %collective-permute-start.2 = (bf16[128,256]{1,0:T(8,128)(2,1)S(1)}, bf16[128,256]{1,0:T(8,128)(2,1)S(1)}, u32[]{:S(2)}, u32[]{:S(2)}) collective-permute-start(bf16[128,256]{1,0:T(8,128)(2,1)S(1)} %pad_maximum_fusion), channel_id=1, source_target_pairs={{0,0},{2,34},{4,68},{6,102},{8,136},{10,170},{12,204},{14,238},{16... | collective-permute-start | bytes 196616 | tf_op jit(solution)/shard_map/ppermute | solution.py:58
  8.1 1.1 multiply_convert_fusion.3
  9.2 1.7 %collective-permute-done.2 = bf16[128,256]{1,0:T(8,128)(2,1)S(1)} collective-permute-done((bf16[128,256]{1,0:T(8,128)(2,1)S(1)}, bf16[128,256]{1,0:T(8,128)(2,1)S(1)}, u32[]{:S(2)}, u32[]{:S(2)}) %collective-permute-start.2) | collective-permute-done | bytes 65568 | tf_op jit(solution)/shard_map/ppermute | solution.py:58
  10.9 3.4 %collective-permute-start.3 = (bf16[128,256]{1,0:T(8,128)(2,1)S(1)}, bf16[128,256]{1,0:T(8,128)(2,1)S(1)}, u32[]{:S(2)}, u32[]{:S(2)}) collective-permute-start(bf16[128,256]{1,0:T(8,128)(2,1)S(1)} %collective-permute-done.2), channel_id=1, source_target_pairs={{0,0},{34,32},{68,64},{102,96},{136,128},{170,160},{204,192},{238,... | collective-permute-start | bytes 196616 | tf_op jit(solution)/shard_map/ppermute | solution.py:59
  14.3 1.9 %broadcast_in_dim.21 = bf16[16,128,768]{2,1,0:T(8,128)(2,1)} broadcast(bf16[128,768]{1,0:T(8,128)(2,1)S(1)} %maximum_maximum_fusion), dimensions={1,2} | broadcast | bytes 3342336 | tf_op jit(solution)/shard_map/broadcast_in_dim | solution.py:84
  16.2 1.7 %collective-permute-done.3 = bf16[128,256]{1,0:T(8,128)(2,1)S(1)} collective-permute-done((bf16[128,256]{1,0:T(8,128)(2,1)S(1)}, bf16[128,256]{1,0:T(8,128)(2,1)S(1)}, u32[]{:S(2)}, u32[]{:S(2)}) %collective-permute-start.3) | collective-permute-done | bytes 65568 | tf_op jit(solution)/shard_map/ppermute | solution.py:59
  17.9 1.1 broadcast_dynamic-update-slice_fusion
  19.0 0.0 copy-start.2
  19.0 21.6 %all-to-all-start = ((bf16[16,128,768]{2,1,0:T(8,128)(2,1)}), bf16[16,128,768]{2,1,0:T(8,128)(2,1)S(1)}, u32[]{:S(2)}, u32[]{:S(2)}) async-start(bf16[16,128,768]{2,1,0:T(8,128)(2,1)} %broadcast_dynamic-update-slice_fusion), calls=%async_computation | async-start | bytes 6291456 | tf_op jit(solution)/shard_map/all_to_all | solution.py:87
  40.6 0.0 copy-done.2
  40.7 40.3 %all-gather.2 = f16[1024,512]{1,0:T(8,128)(2,1)} all-gather(f16[64,512]{1,0:T(8,128)(2,1)S(1)} %fusion.7), channel_id=2, replica_groups=mesh['fs'=16,'zh'=4,'zl'=4,'c'=2] {'zh','zl'}, dimensions={0}, use_global_device_ids=true | all-gather | bytes 1114112 | tf_op jit(solution)/shard_map/all_gather | solution.py:46
  81.0 1.9 %collective-permute-start = (f16[16,1,64,512]{3,2,1,0:T(8,128)(2,1)}, f16[16,1,64,512]{3,2,1,0:T(8,128)(2,1)}, u32[]{:S(2)}, u32[]{:S(2)}) collective-permute-start(f16[16,1,64,512]{3,2,1,0:T(8,128)(2,1)} %bitcast.2), channel_id=1, source_target_pairs={{0,1},{1,0},{2,3},{3,2},{4,5},{5,4},{6,7},{7,6},{8,9},{9,8},{10,11... | collective-permute-start | bytes 3145736 | tf_op jit(solution)/shard_map/ppermute | solution.py:32
  82.9 1.4 multiply_convert_fusion
  84.3 0.2 broadcast_in_dim.18
  84.6 0.1 constant_dynamic-update-slice_fusion
  84.7 1.2 collective-permute-done
  85.9 1.5 fusion.2
  87.3 0.0 copy-start
  87.4 0.6 multiply_reduce_fusion
  87.9 0.8 copy-done
  88.7 0.0 all-to-all-done
  88.7 2.9 %fusion = f32[512,512]{1,0:T(8,128)S(1)} fusion(bf16[2048,512]{1,0:T(8,128)(2,1)} %bitcast.35, bf16[2048,768]{1,0:T(8,128)(2,1)S(1)} %bitcast.31), kind=kOutput, calls=%fused_computation.2 | convolution fusion | flops 1073741824 | bytes 5242880 | tf_op jit(solution)/shard_map/dot_general | solution.py:92
  91.6 0.2 fusion.4
  91.9 1.4 convolution_convert_fusion
  93.3 2.0 %collective-permute-start.4 = (bf16[256,2048]{1,0:T(8,128)(2,1)}, bf16[256,2048]{1,0:T(8,128)(2,1)}, u32[]{:S(2)}, u32[]{:S(2)}) collective-permute-start(bf16[256,2048]{1,0:T(8,128)(2,1)} %convolution_convert_fusion), channel_id=1, source_target_pairs={{0,1},{1,0},{2,3},{3,2},{4,5},{5,4},{6,7},{7,6},{8,9},{9,8},{10,11... | collective-permute-start | bytes 3145736 | tf_op jit(solution)/shard_map/ppermute | solution.py:32
  95.4 2.8 %collective-permute-done.4 = bf16[256,2048]{1,0:T(8,128)(2,1)} collective-permute-done((bf16[256,2048]{1,0:T(8,128)(2,1)}, bf16[256,2048]{1,0:T(8,128)(2,1)}, u32[]{:S(2)}, u32[]{:S(2)}) %collective-permute-start.4) | collective-permute-done | bytes 1048608 | tf_op jit(solution)/shard_map/ppermute | solution.py:32
  98.2 1.7 %add_convert_fusion = bf16[256,2048]{1,0:T(8,128)(2,1)S(1)} fusion(bf16[256,2048]{1,0:T(8,128)(2,1)} %collective-permute-done.4, bf16[256,256]{1,0:T(8,128)(2,1)S(1)} %bitcast.42, bf16[2048,768]{1,0:T(8,128)(2,1)S(1)} %bitcast.33), kind=kOutput, calls=%fused_computation.5 | convolution fusion | flops 270008320 | bytes 3276800 | tf_op jit(solution)/shard_map/dot_general | solution.py:69
  99.9 0.0 copy-start.1
  99.9 1.0 dynamic-slice_bitcast_fusion
  100.9 4.4 %collective-permute-start.6 = (bf16[4,16,2048]{2,1,0:T(8,128)(2,1)}, bf16[4,16,2048]{2,1,0:T(8,128)(2,1)S(1)}, u32[]{:S(2)}, u32[]{:S(2)}) collective-permute-start(bf16[4,16,2048]{2,1,0:T(8,128)(2,1)} %get-tuple-element.16), channel_id=1, source_target_pairs={{0,30},{2,0},{4,2},{6,4},{8,6},{10,8},{12,10},{14,12},{16,14},{18,... | collective-permute-start | bytes 786440 | tf_op jit(solution)/shard_map/ppermute | solution.py:28
  105.3 1.9 %collective-permute-start.5 = (bf16[4,16,2048]{2,1,0:T(8,128)(2,1)}, bf16[4,16,2048]{2,1,0:T(8,128)(2,1)}, u32[]{:S(2)}, u32[]{:S(2)}) collective-permute-start(bf16[4,16,2048]{2,1,0:T(8,128)(2,1)} %get-tuple-element.17), channel_id=1, source_target_pairs={{0,2},{2,4},{4,6},{6,8},{8,10},{10,12},{12,14},{14,16},{16,18},{18... | collective-permute-start | bytes 786440 | tf_op jit(solution)/shard_map/ppermute | solution.py:28
  107.2 0.0 copy-done.1
  107.2 0.7 dynamic-slice_bitcast_fusion.3
  107.9 5.3 %collective-permute-start.8 = (bf16[2,16,2048]{2,1,0:T(8,128)(2,1)}, bf16[2,16,2048]{2,1,0:T(8,128)(2,1)S(1)}, u32[]{:S(2)}, u32[]{:S(2)}) collective-permute-start(bf16[2,16,2048]{2,1,0:T(8,128)(2,1)} %dynamic-slice_bitcast_fusion.3), channel_id=1, source_target_pairs={{0,28},{2,30},{4,0},{6,2},{8,4},{10,6},{12,8},{14,10},{16,12},{18,... | collective-permute-start | bytes 393224 | tf_op jit(solution)/shard_map/ppermute | solution.py:28
  113.2 0.7 slice_bitcast_fusion
  113.8 1.9 %collective-permute-start.7 = (bf16[2,16,2048]{2,1,0:T(8,128)(2,1)}, bf16[2,16,2048]{2,1,0:T(8,128)(2,1)}, u32[]{:S(2)}, u32[]{:S(2)}) collective-permute-start(bf16[2,16,2048]{2,1,0:T(8,128)(2,1)} %slice_bitcast_fusion), channel_id=1, source_target_pairs={{0,4},{2,6},{4,8},{6,10},{8,12},{10,14},{12,16},{14,18},{16,20},{1... | collective-permute-start | bytes 393224 | tf_op jit(solution)/shard_map/ppermute | solution.py:28
  115.8 1.7 %fusion.13 = (bf16[2048,256]{1,0:T(8,128)(2,1)}, bf16[2048,256]{1,0:T(8,128)(2,1)}, bf16[2048,256]{1,0:T(8,128)(2,1)}) fusion(bf16[2048,768]{1,0:T(8,128)(2,1)S(1)} %bitcast.34), kind=kLoop, calls=%fused_computation.39 | loop fusion | bytes 6291456
  117.5 2.3 %copy.15 = bf16[2048,256]{0,1:T(8,128)(2,1)} copy(bf16[2048,256]{1,0:T(8,128)(2,1)} %get-tuple-element.12) | data formatting | bytes 2097152
  119.8 0.0 collective-permute-done.8
  119.8 5.2 %collective-permute-done.7 = bf16[2,16,2048]{2,1,0:T(8,128)(2,1)} collective-permute-done((bf16[2,16,2048]{2,1,0:T(8,128)(2,1)}, bf16[2,16,2048]{2,1,0:T(8,128)(2,1)}, u32[]{:S(2)}, u32[]{:S(2)}) %collective-permute-start.7) | collective-permute-done | bytes 131104 | tf_op jit(solution)/shard_map/ppermute | solution.py:28
  125.0 0.0 collective-permute-done.6
  125.0 0.0 collective-permute-done.5
  125.0 1.2 fusion.6
  126.2 27.3 %all_to_all.10 = bf16[4,16,2048]{2,1,0:T(8,128)(2,1)S(1)} all-to-all(bf16[4,16,2048]{2,1,0:T(8,128)(2,1)S(1)} %fusion.6), channel_id=1, replica_groups=mesh['fs'=16,'zh'=4,'zl'=4,'c'=2] {'zh'}, dimensions={0} | all-to-all | bytes 524288 | tf_op jit(solution)/shard_map/all_to_all | solution.py:76
  153.5 0.7 reduce_sum.22
  (9 shorter events, 0.1 us)
Async XLA Ops:
  1.6 3.1 %collective-permute-start.1 = (bf16[64,256]{1,0:T(8,128)(2,1)S(1)}, bf16[64,256]{1,0:T(8,128)(2,1)S(1)}, u32[]{:S(2)}, u32[]{:S(2)}) collective-permute-start(bf16[64,256]{1,0:T(8,128)(2,1)S(1)} %broadcast_select_fusion.2), channel_id=1, source_target_pairs={{0,1},{1,0},{2,3},{3,2},{4,5},{5,4},{6,7},{7,6},{8,9},{9,8},{10,11... | collective-permute-start | bytes 98312 | tf_op jit(solution)/shard_map/ppermute | solution.py:32
  4.7 6.2 %collective-permute-start.2 = (bf16[128,256]{1,0:T(8,128)(2,1)S(1)}, bf16[128,256]{1,0:T(8,128)(2,1)S(1)}, u32[]{:S(2)}, u32[]{:S(2)}) collective-permute-start(bf16[128,256]{1,0:T(8,128)(2,1)S(1)} %pad_maximum_fusion), channel_id=1, source_target_pairs={{0,0},{2,34},{4,68},{6,102},{8,136},{10,170},{12,204},{14,238},{16... | collective-permute-start | bytes 196616 | tf_op jit(solution)/shard_map/ppermute | solution.py:58
  10.9 7.0 %collective-permute-start.3 = (bf16[128,256]{1,0:T(8,128)(2,1)S(1)}, bf16[128,256]{1,0:T(8,128)(2,1)S(1)}, u32[]{:S(2)}, u32[]{:S(2)}) collective-permute-start(bf16[128,256]{1,0:T(8,128)(2,1)S(1)} %collective-permute-done.2), channel_id=1, source_target_pairs={{0,0},{34,32},{68,64},{102,96},{136,128},{170,160},{204,192},{238,... | collective-permute-start | bytes 196616 | tf_op jit(solution)/shard_map/ppermute | solution.py:59
  19.0 21.6 %copy-start.2 = (bf16[512,64]{0,1:T(8,128)(2,1)S(1)}, bf16[512,64]{0,1:T(8,128)(2,1)}, u32[]{:S(2)}) copy-start(bf16[512,64]{0,1:T(8,128)(2,1)} %param.5) | copy-start | bytes 196612
  19.0 69.7 %all-to-all-start = ((bf16[16,128,768]{2,1,0:T(8,128)(2,1)}), bf16[16,128,768]{2,1,0:T(8,128)(2,1)S(1)}, u32[]{:S(2)}, u32[]{:S(2)}) async-start(bf16[16,128,768]{2,1,0:T(8,128)(2,1)} %broadcast_dynamic-update-slice_fusion), calls=%async_computation | async-start | bytes 6291456 | tf_op jit(solution)/shard_map/all_to_all | solution.py:87
  81.0 4.9 %collective-permute-start = (f16[16,1,64,512]{3,2,1,0:T(8,128)(2,1)}, f16[16,1,64,512]{3,2,1,0:T(8,128)(2,1)}, u32[]{:S(2)}, u32[]{:S(2)}) collective-permute-start(f16[16,1,64,512]{3,2,1,0:T(8,128)(2,1)} %bitcast.2), channel_id=1, source_target_pairs={{0,1},{1,0},{2,3},{3,2},{4,5},{5,4},{6,7},{7,6},{8,9},{9,8},{10,11... | collective-permute-start | bytes 3145736 | tf_op jit(solution)/shard_map/ppermute | solution.py:32
  87.3 1.4 copy-start
  93.3 4.9 %collective-permute-start.4 = (bf16[256,2048]{1,0:T(8,128)(2,1)}, bf16[256,2048]{1,0:T(8,128)(2,1)}, u32[]{:S(2)}, u32[]{:S(2)}) collective-permute-start(bf16[256,2048]{1,0:T(8,128)(2,1)} %convolution_convert_fusion), channel_id=1, source_target_pairs={{0,1},{1,0},{2,3},{3,2},{4,5},{5,4},{6,7},{7,6},{8,9},{9,8},{10,11... | collective-permute-start | bytes 3145736 | tf_op jit(solution)/shard_map/ppermute | solution.py:32
  99.9 7.4 %copy-start.1 = (bf16[256,2048]{1,0:T(8,128)(2,1)}, bf16[256,2048]{1,0:T(8,128)(2,1)S(1)}, u32[]{:S(2)}) copy-start(bf16[256,2048]{1,0:T(8,128)(2,1)S(1)} %add_convert_fusion) | copy-start | bytes 3145732
  100.9 24.1 %collective-permute-start.6 = (bf16[4,16,2048]{2,1,0:T(8,128)(2,1)}, bf16[4,16,2048]{2,1,0:T(8,128)(2,1)S(1)}, u32[]{:S(2)}, u32[]{:S(2)}) collective-permute-start(bf16[4,16,2048]{2,1,0:T(8,128)(2,1)} %get-tuple-element.16), channel_id=1, source_target_pairs={{0,30},{2,0},{4,2},{6,4},{8,6},{10,8},{12,10},{14,12},{16,14},{18,... | collective-permute-start | bytes 786440 | tf_op jit(solution)/shard_map/ppermute | solution.py:28
  105.3 19.7 %collective-permute-start.5 = (bf16[4,16,2048]{2,1,0:T(8,128)(2,1)}, bf16[4,16,2048]{2,1,0:T(8,128)(2,1)}, u32[]{:S(2)}, u32[]{:S(2)}) collective-permute-start(bf16[4,16,2048]{2,1,0:T(8,128)(2,1)} %get-tuple-element.17), channel_id=1, source_target_pairs={{0,2},{2,4},{4,6},{6,8},{8,10},{10,12},{12,14},{14,16},{16,18},{18... | collective-permute-start | bytes 786440 | tf_op jit(solution)/shard_map/ppermute | solution.py:28
  107.9 11.8 %collective-permute-start.8 = (bf16[2,16,2048]{2,1,0:T(8,128)(2,1)}, bf16[2,16,2048]{2,1,0:T(8,128)(2,1)S(1)}, u32[]{:S(2)}, u32[]{:S(2)}) collective-permute-start(bf16[2,16,2048]{2,1,0:T(8,128)(2,1)} %dynamic-slice_bitcast_fusion.3), channel_id=1, source_target_pairs={{0,28},{2,30},{4,0},{6,2},{8,4},{10,6},{12,8},{14,10},{16,12},{18,... | collective-permute-start | bytes 393224 | tf_op jit(solution)/shard_map/ppermute | solution.py:28
  113.8 11.1 %collective-permute-start.7 = (bf16[2,16,2048]{2,1,0:T(8,128)(2,1)}, bf16[2,16,2048]{2,1,0:T(8,128)(2,1)}, u32[]{:S(2)}, u32[]{:S(2)}) collective-permute-start(bf16[2,16,2048]{2,1,0:T(8,128)(2,1)} %slice_bitcast_fusion), channel_id=1, source_target_pairs={{0,4},{2,6},{4,8},{6,10},{8,12},{10,14},{12,16},{14,18},{16,20},{1... | collective-permute-start | bytes 393224 | tf_op jit(solution)/shard_map/ppermute | solution.py:28

commit v5 on v3

--- a/solution.py
+++ b/solution.py
@@ -58,10 +58,10 @@
 def place_down(down_train):
     c = lax.axis_index("c")
     x = down_train.astype(BF).T
+    keep, give = jnp.where(c == 0, x[:, :256], x[:, 256:]), jnp.where(c == 0, x[:, 256:], x[:, :256])
+    x = by_core(c, keep, swap(give), 0)
     x = lax.ppermute(x, FS_TP[:3], [(a * 16 + b, (a ^ b) * 16 + b) for a, b in EVERY])
-    x = lax.ppermute(x, FS_TP[:3], [((a ^ b) * 16 + b, b * 16 + a) for a, b in EVERY])
-    keep, give = jnp.where(c == 0, x[:, :256], x[:, 256:]), jnp.where(c == 0, x[:, 256:], x[:, :256])
-    return by_core(c, keep, swap(give), 0)
+    return lax.ppermute(x, FS_TP[:3], [((a ^ b) * 16 + b, b * 16 + a) for a, b in EVERY])
 
 
 def scatter_sum(hidden, down, ready):
@@ -93,7 +93,8 @@
     sums = lax.dot_general(x, both, (((0,), (0,)), ((), ())), preferred_element_type=F32)
     gate, up = sums[:, :256], sums[:, 256:]
     hidden = (jax.nn.silu(gate * scale) * (up * scale)).astype(BF)
-    return scatter_sum(hidden, down, (both[:, :256], both[:, 256:], down.T))
+    gate_serve, up_serve = both[:, :256], both[:, 256:]
+    return scatter_sum(hidden, down, (gate_serve, up_serve, down.T))
 
 
 def solution(mesh):

time: 164 us -> 162 us (0.988)
  the two profiles are of different devices: /device:TPU:32 before, /device:TPU:64 now
where the time goes in v5:
time: 162 us; the launch traced here: 161 us
  blocking collectives  67.1 us (41%)
  starting transfers between devices  53.2 us (33%)
  waiting for transfers between devices  24.3 us (15%)
  local copies, waits for them, and re-layouts  7.48 us (5%)
  other arithmetic  4.42 us (3%)
  matrix products  3.8 us (2%)
    all_gather x1, blocking collectives, gather_tokens(): mine = lax.all_gather(x, TP[:2])[:, None]  39 us
    all_to_all x1, blocking collectives, scatter_sum(): rows = lax.all_to_all(near, 'zh', 0, 0, tiled=True)  28.1 us
    all_to_all x2, starting transfers between devices, spread(): lax.all_to_all(every, 'fs', 0, 0, tiled=True)  22.5 us
    ppermute x4, starting transfers between devices, shift(): return lax.ppermute(x, TP[:2], [(i, (i + by) % 16) for i in range(16)])  14 us
    all_to_all x2, waiting for transfers between devices, spread(): lax.all_to_all(every, 'fs', 0, 0, tiled=True)  12.4 us
    ppermute x3, starting transfers between devices, swap(): return lax.ppermute(x, 'c', [(0, 1), (1, 0)])  6.24 us
    ppermute x4, waiting for transfers between devices, shift(): return lax.ppermute(x, TP[:2], [(i, (i + by) % 16) for i in range(16)])  5.56 us
    ppermute x1, starting transfers between devices, place_down(): lax.ppermute(x, FS_TP[:3], [(a * 16 + b, (a ^ b) * 16 + b) for a, b in EV...  5.29 us
  transfers between devices with their start and end apart: 11, of which 7 were waited for; matrix products, arithmetic and copies ran while one was open for 6% of the time, Pallas kernels for 0%

profile of v5, /device:TPU:64, one launch (start us, length us, event | category | flops | bytes accessed | tf_op | source)
XLA Modules:
  0.0 161.1 jit_solution(3652232355881781455)
XLA Ops:
  0.6 1.1 multiply_convert_fusion.3
  1.7 1.5 broadcast_in_dim.17
  3.3 0.0 copy-start.1
  3.3 0.0 copy-start
  3.3 7.2 %all-to-all-start = ((bf16[16,128,512]{2,1,0:T(8,128)(2,1)}), bf16[16,128,512]{2,1,0:T(8,128)(2,1)}, u32[]{:S(2)}, u32[]{:S(2)}) async-start(bf16[16,128,512]{2,1,0:T(8,128)(2,1)} %broadcast_in_dim.17), calls=%async_computation | async-start | bytes 4194304 | tf_op jit(solution)/shard_map/all_to_all | solution.py:45
  10.5 0.0 copy-done.1
  10.5 39.0 %all-gather.2 = f16[1024,512]{1,0:T(8,128)(2,1)S(1)} all-gather(f16[64,512]{1,0:T(8,128)(2,1)S(1)} %fusion.6), channel_id=2, replica_groups=mesh['fs'=16,'zh'=4,'zl'=4,'c'=2] {'zh','zl'}, dimensions={0}, use_global_device_ids=true | all-gather | bytes 1114112 | tf_op jit(solution)/shard_map/all_gather | solution.py:51
  49.5 1.9 %collective-permute-start = (f16[16,1,64,512]{3,2,1,0:T(8,128)(2,1)S(1)}, f16[16,1,64,512]{3,2,1,0:T(8,128)(2,1)}, u32[]{:S(2)}, u32[]{:S(2)}) collective-permute-start(f16[16,1,64,512]{3,2,1,0:T(8,128)(2,1)S(1)} %bitcast.43), channel_id=1, source_target_pairs={{0,1},{1,0},{2,3},{3,2},{4,5},{5,4},{6,7},{7,6},{8,9},{9,8},{10,11... | collective-permute-start | bytes 3145736 | tf_op jit(solution)/shard_map/ppermute | solution.py:32
  51.4 0.0 copy-done
  51.5 2.4 %collective-permute-start.1 = (bf16[64,256]{1,0:T(8,128)(2,1)S(1)}, bf16[64,256]{1,0:T(8,128)(2,1)S(1)}, u32[]{:S(2)}, u32[]{:S(2)}) collective-permute-start(bf16[64,256]{1,0:T(8,128)(2,1)S(1)} %broadcast_select_fusion.2), channel_id=1, source_target_pairs={{0,1},{1,0},{2,3},{3,2},{4,5},{5,4},{6,7},{7,6},{8,9},{9,8},{10,11... | collective-permute-start | bytes 98312 | tf_op jit(solution)/shard_map/ppermute | solution.py:32
  53.9 0.2 multiply_convert_fusion
  54.1 0.6 collective-permute-done.1
  54.8 5.3 %collective-permute-start.2 = (bf16[128,256]{1,0:T(8,128)(2,1)S(1)}, bf16[128,256]{1,0:T(8,128)(2,1)S(1)}, u32[]{:S(2)}, u32[]{:S(2)}) collective-permute-start(bf16[128,256]{1,0:T(8,128)(2,1)S(1)} %pad_maximum_fusion.1), channel_id=1, source_target_pairs={{0,0},{2,34},{4,68},{6,102},{8,136},{10,170},{12,204},{14,238},{16... | collective-permute-start | bytes 196616 | tf_op jit(solution)/shard_map/ppermute | solution.py:63
  60.1 0.2 broadcast_in_dim.15
  60.3 0.1 constant_dynamic-update-slice_fusion
  60.4 2.2 %collective-permute-done.2 = bf16[128,256]{1,0:T(8,128)(2,1)S(1)} collective-permute-done((bf16[128,256]{1,0:T(8,128)(2,1)S(1)}, bf16[128,256]{1,0:T(8,128)(2,1)S(1)}, u32[]{:S(2)}, u32[]{:S(2)}) %collective-permute-start.2) | collective-permute-done | bytes 65568 | tf_op jit(solution)/shard_map/ppermute | solution.py:63
  62.7 5.1 %collective-permute-start.3 = (bf16[128,256]{1,0:T(8,128)(2,1)S(1)}, bf16[128,256]{1,0:T(8,128)(2,1)S(1)}, u32[]{:S(2)}, u32[]{:S(2)}) collective-permute-start(bf16[128,256]{1,0:T(8,128)(2,1)S(1)} %collective-permute-done.2), channel_id=1, source_target_pairs={{0,0},{34,32},{68,64},{102,96},{136,128},{170,160},{204,192},{238,... | collective-permute-start | bytes 196616 | tf_op jit(solution)/shard_map/ppermute | solution.py:64
  67.8 0.0 collective-permute-done
  67.8 1.5 fusion.1
  69.3 0.6 multiply_reduce_fusion
  69.9 2.3 %collective-permute-done.3 = bf16[128,256]{1,0:T(8,128)(2,1)S(1)} collective-permute-done((bf16[128,256]{1,0:T(8,128)(2,1)S(1)}, bf16[128,256]{1,0:T(8,128)(2,1)S(1)}, u32[]{:S(2)}, u32[]{:S(2)}) %collective-permute-start.3) | collective-permute-done | bytes 65568 | tf_op jit(solution)/shard_map/ppermute | solution.py:64
  72.1 0.0 all-to-all-done
  72.1 1.1 broadcast_in_dim.18
  73.2 15.3 %all-to-all-start.1 = ((bf16[16,128,256]{2,1,0:T(8,128)(2,1)}), bf16[16,128,256]{2,1,0:T(8,128)(2,1)S(1)}, u32[]{:S(2)}, u32[]{:S(2)}) async-start(bf16[16,128,256]{2,1,0:T(8,128)(2,1)} %broadcast_in_dim.18), calls=%async_computation.1 | async-start | bytes 2097152 | tf_op jit(solution)/shard_map/all_to_all | solution.py:45
  88.5 2.9 %fusion.8 = f32[512,512]{1,0:T(8,128)S(1)} fusion(bf16[2048,512]{1,0:T(8,128)(2,1)S(1)} %bitcast.38, bf16[2048,512]{1,0:T(8,128)(2,1)} %bitcast.4), kind=kOutput, calls=%fused_computation.35 | convolution fusion | flops 1073741824 | bytes 5242880 | tf_op jit(solution)/shard_map/dot_general | solution.py:93
  91.4 0.2 fusion.3
  91.6 12.4 %all-to-all-done.1 = bf16[16,128,256]{2,1,0:T(8,128)(2,1)S(1)} async-done(((bf16[16,128,256]{2,1,0:T(8,128)(2,1)}), bf16[16,128,256]{2,1,0:T(8,128)(2,1)S(1)}, u32[]{:S(2)}, u32[]{:S(2)}) %all-to-all-start.1) | async-done | bytes 1048608 | tf_op jit(solution)/shard_map/all_to_all | solution.py:45
  104.0 0.5 convolution_convert_fusion
  104.5 1.9 %collective-permute-start.4 = (bf16[256,2048]{1,0:T(8,128)(2,1)S(1)}, bf16[256,2048]{1,0:T(8,128)(2,1)S(1)}, u32[]{:S(2)}, u32[]{:S(2)}) collective-permute-start(bf16[256,2048]{1,0:T(8,128)(2,1)S(1)} %convolution_convert_fusion), channel_id=1, source_target_pairs={{0,1},{1,0},{2,3},{3,2},{4,5},{5,4},{6,7},{7,6},{8,9},{9,8},{10,11... | collective-permute-start | bytes 3145736 | tf_op jit(solution)/shard_map/ppermute | solution.py:32
  106.5 1.4 copy.14
  107.9 1.2 collective-permute-done.4
  109.1 0.5 fusion
  109.5 0.1 dynamic-slice_bitcast_fusion
  109.6 1.9 %collective-permute-start.5 = (bf16[4,16,2048]{2,1,0:T(8,128)(2,1)S(1)}, bf16[4,16,2048]{2,1,0:T(8,128)(2,1)S(1)}, u32[]{:S(2)}, u32[]{:S(2)}) collective-permute-start(bf16[4,16,2048]{2,1,0:T(8,128)(2,1)S(1)} %get-tuple-element.16), channel_id=1, source_target_pairs={{0,2},{2,4},{4,6},{6,8},{8,10},{10,12},{12,14},{14,16},{16,18},{18... | collective-permute-start | bytes 786440 | tf_op jit(solution)/shard_map/ppermute | solution.py:28
  111.6 3.9 %collective-permute-start.6 = (bf16[4,16,2048]{2,1,0:T(8,128)(2,1)S(1)}, bf16[4,16,2048]{2,1,0:T(8,128)(2,1)S(1)}, u32[]{:S(2)}, u32[]{:S(2)}) collective-permute-start(bf16[4,16,2048]{2,1,0:T(8,128)(2,1)S(1)} %get-tuple-element.15), channel_id=1, source_target_pairs={{0,30},{2,0},{4,2},{6,4},{8,6},{10,8},{12,10},{14,12},{16,14},{18,... | collective-permute-start | bytes 786440 | tf_op jit(solution)/shard_map/ppermute | solution.py:28
  115.5 3.1 %collective-permute-start.7 = (bf16[2,16,2048]{2,1,0:T(8,128)(2,1)S(1)}, bf16[2,16,2048]{2,1,0:T(8,128)(2,1)S(1)}, u32[]{:S(2)}, u32[]{:S(2)}) collective-permute-start(bf16[2,16,2048]{2,1,0:T(8,128)(2,1)S(1)} %slice_bitcast_fusion), channel_id=1, source_target_pairs={{0,4},{2,6},{4,8},{6,10},{8,12},{10,14},{12,16},{14,18},{16,20},{1... | collective-permute-start | bytes 393224 | tf_op jit(solution)/shard_map/ppermute | solution.py:28
  118.6 5.0 %collective-permute-start.8 = (bf16[2,16,2048]{2,1,0:T(8,128)(2,1)S(1)}, bf16[2,16,2048]{2,1,0:T(8,128)(2,1)S(1)}, u32[]{:S(2)}, u32[]{:S(2)}) collective-permute-start(bf16[2,16,2048]{2,1,0:T(8,128)(2,1)S(1)} %dynamic-slice_bitcast_fusion.3), channel_id=1, source_target_pairs={{0,28},{2,30},{4,0},{6,2},{8,4},{10,6},{12,8},{14,10},{16,12},{18,... | collective-permute-start | bytes 393224 | tf_op jit(solution)/shard_map/ppermute | solution.py:28
  123.7 3.0 %fusion.7 = (bf16[2048,256]{1,0:T(8,128)(2,1)}, bf16[2048,256]{1,0:T(8,128)(2,1)}) fusion(bf16[2048,512]{1,0:T(8,128)(2,1)} %bitcast.4), kind=kLoop, calls=%fused_computation.34 | loop fusion | bytes 4194304 | tf_op jit(solution)/shard_map/slice | solution.py:96
  126.7 1.0 collective-permute-done.7
  127.7 4.6 %collective-permute-done.8 = bf16[2,16,2048]{2,1,0:T(8,128)(2,1)S(1)} collective-permute-done((bf16[2,16,2048]{2,1,0:T(8,128)(2,1)S(1)}, bf16[2,16,2048]{2,1,0:T(8,128)(2,1)S(1)}, u32[]{:S(2)}, u32[]{:S(2)}) %collective-permute-start.8) | collective-permute-done | bytes 131104 | tf_op jit(solution)/shard_map/ppermute | solution.py:28
  132.2 0.0 collective-permute-done.5
  132.2 0.0 collective-permute-done.6
  132.3 0.1 fusion.5
  132.4 28.1 %all_to_all.15 = bf16[4,16,2048]{2,1,0:T(8,128)(2,1)S(1)} all-to-all(bf16[4,16,2048]{2,1,0:T(8,128)(2,1)S(1)} %fusion.5), channel_id=1, replica_groups=mesh['fs'=16,'zh'=4,'zl'=4,'c'=2] {'zh'}, dimensions={0} | all-to-all | bytes 524288 | tf_op jit(solution)/shard_map/all_to_all | solution.py:81
  160.4 0.7 reduce_sum.22
  (10 shorter events, 0.1 us)
Async XLA Ops:
  3.3 7.2 %copy-start.1 = (bf16[512,64]{0,1:T(8,128)(2,1)S(1)}, bf16[512,64]{0,1:T(8,128)(2,1)}, u32[]{:S(2)}) copy-start(bf16[512,64]{0,1:T(8,128)(2,1)} %param.5) | copy-start | bytes 196612
  3.3 48.2 %copy-start = (f32[512,64]{0,1:T(8,128)S(1)}, f32[512,64]{0,1:T(8,128)}, u32[]{:S(2)}) copy-start(f32[512,64]{0,1:T(8,128)} %param.9) | copy-start | bytes 393220
  3.3 68.9 %all-to-all-start = ((bf16[16,128,512]{2,1,0:T(8,128)(2,1)}), bf16[16,128,512]{2,1,0:T(8,128)(2,1)}, u32[]{:S(2)}, u32[]{:S(2)}) async-start(bf16[16,128,512]{2,1,0:T(8,128)(2,1)} %broadcast_in_dim.17), calls=%async_computation | async-start | bytes 4194304 | tf_op jit(solution)/shard_map/all_to_all | solution.py:45
  49.5 18.3 %collective-permute-start = (f16[16,1,64,512]{3,2,1,0:T(8,128)(2,1)S(1)}, f16[16,1,64,512]{3,2,1,0:T(8,128)(2,1)}, u32[]{:S(2)}, u32[]{:S(2)}) collective-permute-start(f16[16,1,64,512]{3,2,1,0:T(8,128)(2,1)S(1)} %bitcast.43), channel_id=1, source_target_pairs={{0,1},{1,0},{2,3},{3,2},{4,5},{5,4},{6,7},{7,6},{8,9},{9,8},{10,11... | collective-permute-start | bytes 3145736 | tf_op jit(solution)/shard_map/ppermute | solution.py:32
  51.5 3.3 %collective-permute-start.1 = (bf16[64,256]{1,0:T(8,128)(2,1)S(1)}, bf16[64,256]{1,0:T(8,128)(2,1)S(1)}, u32[]{:S(2)}, u32[]{:S(2)}) collective-permute-start(bf16[64,256]{1,0:T(8,128)(2,1)S(1)} %broadcast_select_fusion.2), channel_id=1, source_target_pairs={{0,1},{1,0},{2,3},{3,2},{4,5},{5,4},{6,7},{7,6},{8,9},{9,8},{10,11... | collective-permute-start | bytes 98312 | tf_op jit(solution)/shard_map/ppermute | solution.py:32
  54.8 7.9 %collective-permute-start.2 = (bf16[128,256]{1,0:T(8,128)(2,1)S(1)}, bf16[128,256]{1,0:T(8,128)(2,1)S(1)}, u32[]{:S(2)}, u32[]{:S(2)}) collective-permute-start(bf16[128,256]{1,0:T(8,128)(2,1)S(1)} %pad_maximum_fusion.1), channel_id=1, source_target_pairs={{0,0},{2,34},{4,68},{6,102},{8,136},{10,170},{12,204},{14,238},{16... | collective-permute-start | bytes 196616 | tf_op jit(solution)/shard_map/ppermute | solution.py:63
  62.7 9.4 %collective-permute-start.3 = (bf16[128,256]{1,0:T(8,128)(2,1)S(1)}, bf16[128,256]{1,0:T(8,128)(2,1)S(1)}, u32[]{:S(2)}, u32[]{:S(2)}) collective-permute-start(bf16[128,256]{1,0:T(8,128)(2,1)S(1)} %collective-permute-done.2), channel_id=1, source_target_pairs={{0,0},{34,32},{68,64},{102,96},{136,128},{170,160},{204,192},{238,... | collective-permute-start | bytes 196616 | tf_op jit(solution)/shard_map/ppermute | solution.py:64
  73.2 30.9 %all-to-all-start.1 = ((bf16[16,128,256]{2,1,0:T(8,128)(2,1)}), bf16[16,128,256]{2,1,0:T(8,128)(2,1)S(1)}, u32[]{:S(2)}, u32[]{:S(2)}) async-start(bf16[16,128,256]{2,1,0:T(8,128)(2,1)} %broadcast_in_dim.18), calls=%async_computation.1 | async-start | bytes 2097152 | tf_op jit(solution)/shard_map/all_to_all | solution.py:45
  104.5 4.6 %collective-permute-start.4 = (bf16[256,2048]{1,0:T(8,128)(2,1)S(1)}, bf16[256,2048]{1,0:T(8,128)(2,1)S(1)}, u32[]{:S(2)}, u32[]{:S(2)}) collective-permute-start(bf16[256,2048]{1,0:T(8,128)(2,1)S(1)} %convolution_convert_fusion), channel_id=1, source_target_pairs={{0,1},{1,0},{2,3},{3,2},{4,5},{5,4},{6,7},{7,6},{8,9},{9,8},{10,11... | collective-permute-start | bytes 3145736 | tf_op jit(solution)/shard_map/ppermute | solution.py:32
  109.6 22.6 %collective-permute-start.5 = (bf16[4,16,2048]{2,1,0:T(8,128)(2,1)S(1)}, bf16[4,16,2048]{2,1,0:T(8,128)(2,1)S(1)}, u32[]{:S(2)}, u32[]{:S(2)}) collective-permute-start(bf16[4,16,2048]{2,1,0:T(8,128)(2,1)S(1)} %get-tuple-element.16), channel_id=1, source_target_pairs={{0,2},{2,4},{4,6},{6,8},{8,10},{10,12},{12,14},{14,16},{16,18},{18... | collective-permute-start | bytes 786440 | tf_op jit(solution)/shard_map/ppermute | solution.py:28
  111.6 20.7 %collective-permute-start.6 = (bf16[4,16,2048]{2,1,0:T(8,128)(2,1)S(1)}, bf16[4,16,2048]{2,1,0:T(8,128)(2,1)S(1)}, u32[]{:S(2)}, u32[]{:S(2)}) collective-permute-start(bf16[4,16,2048]{2,1,0:T(8,128)(2,1)S(1)} %get-tuple-element.15), channel_id=1, source_target_pairs={{0,30},{2,0},{4,2},{6,4},{8,6},{10,8},{12,10},{14,12},{16,14},{18,... | collective-permute-start | bytes 786440 | tf_op jit(solution)/shard_map/ppermute | solution.py:28
  115.5 12.2 %collective-permute-start.7 = (bf16[2,16,2048]{2,1,0:T(8,128)(2,1)S(1)}, bf16[2,16,2048]{2,1,0:T(8,128)(2,1)S(1)}, u32[]{:S(2)}, u32[]{:S(2)}) collective-permute-start(bf16[2,16,2048]{2,1,0:T(8,128)(2,1)S(1)} %slice_bitcast_fusion), channel_id=1, source_target_pairs={{0,4},{2,6},{4,8},{6,10},{8,12},{10,14},{12,16},{14,18},{16,20},{1... | collective-permute-start | bytes 393224 | tf_op jit(solution)/shard_map/ppermute | solution.py:28
  118.6 13.6 %collective-permute-start.8 = (bf16[2,16,2048]{2,1,0:T(8,128)(2,1)S(1)}, bf16[2,16,2048]{2,1,0:T(8,128)(2,1)S(1)}, u32[]{:S(2)}, u32[]{:S(2)}) collective-permute-start(bf16[2,16,2048]{2,1,0:T(8,128)(2,1)S(1)} %dynamic-slice_bitcast_fusion.3), channel_id=1, source_target_pairs={{0,28},{2,30},{4,0},{6,2},{8,4},{10,6},{12,8},{14,10},{16,12},{18,... | collective-permute-start | bytes 393224 | tf_op jit(solution)/shard_map/ppermute | solution.py:28

commit v6 on v5

--- a/solution.py
+++ b/solution.py
@@ -20,12 +20,17 @@
     return lax.dynamic_index_in_dim(x, i, dim, keepdims=False, allow_negative_indices=False)
 
 
+def part_of(x, at, size, dim):
+    return lax.dynamic_slice_in_dim(x, at, size, dim, allow_negative_indices=False)
+
+
 def put(whole, part, at):
     return lax.dynamic_update_slice(whole, part, at, allow_negative_indices=False)
 
 
-def shift(x, by):
-    return lax.ppermute(x, TP[:2], [(i, (i + by) % 16) for i in range(16)])
+def fan(x, by):
+    pairs = [(2 * z + c, 2 * ((z + (by, -by)[c]) % 16) + c) for z in range(16) for c in range(2)]
+    return lax.ppermute(x, TP, pairs)
 
 
 def swap(x):
@@ -60,8 +65,7 @@
     x = down_train.astype(BF).T
     keep, give = jnp.where(c == 0, x[:, :256], x[:, 256:]), jnp.where(c == 0, x[:, 256:], x[:, :256])
     x = by_core(c, keep, swap(give), 0)
-    x = lax.ppermute(x, FS_TP[:3], [(a * 16 + b, (a ^ b) * 16 + b) for a, b in EVERY])
-    return lax.ppermute(x, FS_TP[:3], [((a ^ b) * 16 + b, b * 16 + a) for a, b in EVERY])
+    return lax.ppermute(x, FS_TP[:3], [(a * 16 + b, b * 16 + a) for a, b in EVERY])
 
 
 def scatter_sum(hidden, down, ready):
@@ -73,10 +77,12 @@
     got = swap(give)
     pair = lax.dot_general(keep, down, across, preferred_element_type=F32) + got.astype(F32)
     pair = pair.astype(BF).reshape(4, 4, 16, D)
-    ahead, behind, far = (pick(pair, (zl + d) & 3, 1) for d in (1, 3, 2))
+    one, two, far = (pick(pair, (zl + d) & 3, 1) for d in (1 + 2 * c, 3 + 2 * c, 2))
     near = pick(pair, zl, 1).astype(F32)
-    near += shift(ahead, 1).astype(F32) + shift(behind, -1).astype(F32)
-    far = jnp.concatenate([shift(far[:2], 2), shift(far[2:], -2)], axis=0)
+    near += fan(one, 1).astype(F32) + fan(two, -1).astype(F32)
+    one = fan(part_of(far, 2 * c, 2, 0), 2)
+    two = fan(part_of(far, 2 - 2 * c, 2, 0), -2)
+    far = by_core(c, one, two, 0)
     near, ready = lax.optimization_barrier(((near + far.astype(F32)).astype(BF), ready))
     rows = lax.all_to_all(near, "zh", 0, 0, tiled=True)
     return (*ready, jnp.sum(rows.astype(F32), axis=0).astype(BF))

time: 162 us -> 158 us (0.975)
  the two profiles are of different devices: /device:TPU:64 before, /device:TPU:1 now
where the time goes in v6:
time: 158 us; the launch traced here: 157 us
  blocking collectives  61.4 us (39%)
  starting transfers between devices  58.2 us (37%)
  waiting for transfers between devices  20.7 us (13%)
  local copies, waits for them, and re-layouts  7.44 us (5%)
  other arithmetic  4.45 us (3%)
  matrix products  3.79 us (2%)
    all_gather x1, blocking collectives, gather_tokens(): mine = lax.all_gather(x, TP[:2])[:, None]  37.5 us
    all_to_all x2, starting transfers between devices, spread(): lax.all_to_all(every, 'fs', 0, 0, tiled=True)  31.8 us
    all_to_all x1, blocking collectives, scatter_sum(): rows = lax.all_to_all(near, 'zh', 0, 0, tiled=True)  24 us
    ppermute x3, starting transfers between devices, swap(): return lax.ppermute(x, 'c', [(0, 1), (1, 0)])  14.2 us
    all_to_all x2, waiting for transfers between devices, spread(): lax.all_to_all(every, 'fs', 0, 0, tiled=True)  12.4 us
    ppermute x4, starting transfers between devices, fan(): return lax.ppermute(x, TP, pairs)  11.5 us
    ppermute x4, waiting for transfers between devices, fan(): return lax.ppermute(x, TP, pairs)  7.69 us
  transfers between devices with their start and end apart: 10, of which 4 were waited for; matrix products, arithmetic and copies ran while one was open for 7% of the time, Pallas kernels for 0%

profile of v6, /device:TPU:1, one launch (start us, length us, event | category | flops | bytes accessed | tf_op | source)
XLA Modules:
  0.0 157.0 jit_solution(6623958074791866193)
XLA Ops:
  0.6 1.1 multiply_convert_fusion.3
  1.7 1.5 broadcast_in_dim.17
  3.2 0.0 copy-start.1
  3.2 0.0 copy-start
  3.3 7.8 %all-to-all-start = ((bf16[16,128,512]{2,1,0:T(8,128)(2,1)}), bf16[16,128,512]{2,1,0:T(8,128)(2,1)}, u32[]{:S(2)}, u32[]{:S(2)}) async-start(bf16[16,128,512]{2,1,0:T(8,128)(2,1)} %broadcast_in_dim.17), calls=%async_computation | async-start | bytes 4194304 | tf_op jit(solution)/shard_map/all_to_all | solution.py:50
  11.0 0.0 copy-done.1
  11.1 37.5 %all-gather.2 = f16[1024,512]{1,0:T(8,128)(2,1)S(1)} all-gather(f16[64,512]{1,0:T(8,128)(2,1)S(1)} %fusion.6), channel_id=2, replica_groups=mesh['fs'=16,'zh'=4,'zl'=4,'c'=2] {'zh','zl'}, dimensions={0}, use_global_device_ids=true | all-gather | bytes 1114112 | tf_op jit(solution)/shard_map/all_gather | solution.py:56
  48.5 7.4 %collective-permute-start = (f16[16,1,64,512]{3,2,1,0:T(8,128)(2,1)S(1)}, f16[16,1,64,512]{3,2,1,0:T(8,128)(2,1)}, u32[]{:S(2)}, u32[]{:S(2)}) collective-permute-start(f16[16,1,64,512]{3,2,1,0:T(8,128)(2,1)S(1)} %bitcast.39), channel_id=1, source_target_pairs={{0,1},{1,0},{2,3},{3,2},{4,5},{5,4},{6,7},{7,6},{8,9},{9,8},{10,11... | collective-permute-start | bytes 3145736 | tf_op jit(solution)/shard_map/ppermute | solution.py:37
  55.9 0.0 copy-done
  56.0 1.9 %collective-permute-start.1 = (bf16[64,256]{1,0:T(8,128)(2,1)S(1)}, bf16[64,256]{1,0:T(8,128)(2,1)S(1)}, u32[]{:S(2)}, u32[]{:S(2)}) collective-permute-start(bf16[64,256]{1,0:T(8,128)(2,1)S(1)} %broadcast_select_fusion.4), channel_id=1, source_target_pairs={{0,1},{1,0},{2,3},{3,2},{4,5},{5,4},{6,7},{7,6},{8,9},{9,8},{10,11... | collective-permute-start | bytes 98312 | tf_op jit(solution)/shard_map/ppermute | solution.py:37
  57.9 0.2 multiply_convert_fusion
  58.1 0.2 broadcast_in_dim.15
  58.4 0.1 constant_dynamic-update-slice_fusion
  58.5 0.6 collective-permute-done.1
  59.1 0.7 collective-permute-start.2
  59.8 0.0 collective-permute-done
  59.8 1.5 fusion.1
  61.3 0.6 multiply_reduce_fusion
  61.8 0.0 collective-permute-done.2
  61.9 0.0 all-to-all-done
  61.9 1.1 broadcast_in_dim.18
  62.9 24.1 %all-to-all-start.1 = ((bf16[16,128,256]{2,1,0:T(8,128)(2,1)}), bf16[16,128,256]{2,1,0:T(8,128)(2,1)S(1)}, u32[]{:S(2)}, u32[]{:S(2)}) async-start(bf16[16,128,256]{2,1,0:T(8,128)(2,1)} %broadcast_in_dim.18), calls=%async_computation.1 | async-start | bytes 2097152 | tf_op jit(solution)/shard_map/all_to_all | solution.py:50
  87.0 2.9 %fusion.8 = f32[512,512]{1,0:T(8,128)S(1)} fusion(bf16[2048,512]{1,0:T(8,128)(2,1)S(1)} %bitcast.34, bf16[2048,512]{1,0:T(8,128)(2,1)} %bitcast.4), kind=kOutput, calls=%fused_computation.36 | convolution fusion | flops 1073741824 | bytes 5242880 | tf_op jit(solution)/shard_map/dot_general | solution.py:99
  89.9 0.2 fusion.3
  90.2 12.4 %all-to-all-done.1 = bf16[16,128,256]{2,1,0:T(8,128)(2,1)S(1)} async-done(((bf16[16,128,256]{2,1,0:T(8,128)(2,1)}), bf16[16,128,256]{2,1,0:T(8,128)(2,1)S(1)}, u32[]{:S(2)}, u32[]{:S(2)}) %all-to-all-start.1) | async-done | bytes 1048608 | tf_op jit(solution)/shard_map/all_to_all | solution.py:50
  102.6 0.5 convolution_convert_fusion
  103.0 4.9 %collective-permute-start.3 = (bf16[256,2048]{1,0:T(8,128)(2,1)S(1)}, bf16[256,2048]{1,0:T(8,128)(2,1)S(1)}, u32[]{:S(2)}, u32[]{:S(2)}) collective-permute-start(bf16[256,2048]{1,0:T(8,128)(2,1)S(1)} %convolution_convert_fusion), channel_id=1, source_target_pairs={{0,1},{1,0},{2,3},{3,2},{4,5},{5,4},{6,7},{7,6},{8,9},{9,8},{10,11... | collective-permute-start | bytes 3145736 | tf_op jit(solution)/shard_map/ppermute | solution.py:37
  108.0 1.4 copy.10
  109.4 3.0 %fusion.7 = (bf16[2048,256]{1,0:T(8,128)(2,1)}, bf16[2048,256]{1,0:T(8,128)(2,1)}) fusion(bf16[2048,512]{1,0:T(8,128)(2,1)} %bitcast.4), kind=kLoop, calls=%fused_computation.35 | loop fusion | bytes 4194304 | tf_op jit(solution)/shard_map/slice | solution.py:102
  112.4 0.0 collective-permute-done.3
  112.4 0.5 fusion
  112.9 1.9 %collective-permute-start.6 = (bf16[2,16,2048]{2,1,0:T(8,128)(2,1)S(1)}, bf16[2,16,2048]{2,1,0:T(8,128)(2,1)S(1)}, u32[]{:S(2)}, u32[]{:S(2)}) collective-permute-start(bf16[2,16,2048]{2,1,0:T(8,128)(2,1)S(1)} %get-tuple-element.14), channel_id=1, source_target_pairs={{0,4},{1,29},{2,6},{3,31},{4,8},{5,1},{6,10},{7,3},{8,12},{9,5},{1... | collective-permute-start | bytes 393224 | tf_op jit(solution)/shard_map/ppermute | solution.py:33
  114.8 4.3 %collective-permute-start.7 = (bf16[2,16,2048]{2,1,0:T(8,128)(2,1)S(1)}, bf16[2,16,2048]{2,1,0:T(8,128)(2,1)S(1)}, u32[]{:S(2)}, u32[]{:S(2)}) collective-permute-start(bf16[2,16,2048]{2,1,0:T(8,128)(2,1)S(1)} %get-tuple-element.15), channel_id=1, source_target_pairs={{0,28},{1,5},{2,30},{3,7},{4,0},{5,9},{6,2},{7,11},{8,4},{9,13},{1... | collective-permute-start | bytes 393224 | tf_op jit(solution)/shard_map/ppermute | solution.py:33
  119.1 1.9 %collective-permute-start.4 = (bf16[4,16,2048]{2,1,0:T(8,128)(2,1)S(1)}, bf16[4,16,2048]{2,1,0:T(8,128)(2,1)S(1)}, u32[]{:S(2)}, u32[]{:S(2)}) collective-permute-start(bf16[4,16,2048]{2,1,0:T(8,128)(2,1)S(1)} %get-tuple-element.16), channel_id=1, source_target_pairs={{0,2},{1,31},{2,4},{3,1},{4,6},{5,3},{6,8},{7,5},{8,10},{9,7},{10,... | collective-permute-start | bytes 786440 | tf_op jit(solution)/shard_map/ppermute | solution.py:33
  121.1 3.4 %collective-permute-start.5 = (bf16[4,16,2048]{2,1,0:T(8,128)(2,1)S(1)}, bf16[4,16,2048]{2,1,0:T(8,128)(2,1)S(1)}, u32[]{:S(2)}, u32[]{:S(2)}) collective-permute-start(bf16[4,16,2048]{2,1,0:T(8,128)(2,1)S(1)} %get-tuple-element.17), channel_id=1, source_target_pairs={{0,30},{1,3},{2,0},{3,5},{4,2},{5,7},{6,4},{7,9},{8,6},{9,11},{10,... | collective-permute-start | bytes 786440 | tf_op jit(solution)/shard_map/ppermute | solution.py:33
  124.4 0.0 collective-permute-done.6
  124.4 0.0 collective-permute-done.7
  124.5 1.8 %collective-permute-done.4 = bf16[4,16,2048]{2,1,0:T(8,128)(2,1)S(1)} collective-permute-done((bf16[4,16,2048]{2,1,0:T(8,128)(2,1)S(1)}, bf16[4,16,2048]{2,1,0:T(8,128)(2,1)S(1)}, u32[]{:S(2)}, u32[]{:S(2)}) %collective-permute-start.4) | collective-permute-done | bytes 262176 | tf_op jit(solution)/shard_map/ppermute | solution.py:33
  126.3 5.9 %collective-permute-done.5 = bf16[4,16,2048]{2,1,0:T(8,128)(2,1)S(1)} collective-permute-done((bf16[4,16,2048]{2,1,0:T(8,128)(2,1)S(1)}, bf16[4,16,2048]{2,1,0:T(8,128)(2,1)S(1)}, u32[]{:S(2)}, u32[]{:S(2)}) %collective-permute-start.5) | collective-permute-done | bytes 262176 | tf_op jit(solution)/shard_map/ppermute | solution.py:33
  132.2 0.1 fusion.5
  132.3 24.0 %all_to_all.15 = bf16[4,16,2048]{2,1,0:T(8,128)(2,1)S(1)} all-to-all(bf16[4,16,2048]{2,1,0:T(8,128)(2,1)S(1)} %fusion.5), channel_id=1, replica_groups=mesh['fs'=16,'zh'=4,'zl'=4,'c'=2] {'zh'}, dimensions={0} | all-to-all | bytes 524288 | tf_op jit(solution)/shard_map/all_to_all | solution.py:87
  156.3 0.7 reduce_sum.22
  (11 shorter events, 0.2 us)
Async XLA Ops:
  3.2 7.8 %copy-start.1 = (bf16[512,64]{0,1:T(8,128)(2,1)S(1)}, bf16[512,64]{0,1:T(8,128)(2,1)}, u32[]{:S(2)}) copy-start(bf16[512,64]{0,1:T(8,128)(2,1)} %param.5) | copy-start | bytes 196612
  3.2 52.7 %copy-start = (f32[512,64]{0,1:T(8,128)S(1)}, f32[512,64]{0,1:T(8,128)}, u32[]{:S(2)}) copy-start(f32[512,64]{0,1:T(8,128)} %param.9) | copy-start | bytes 393220
  3.3 58.6 %all-to-all-start = ((bf16[16,128,512]{2,1,0:T(8,128)(2,1)}), bf16[16,128,512]{2,1,0:T(8,128)(2,1)}, u32[]{:S(2)}, u32[]{:S(2)}) async-start(bf16[16,128,512]{2,1,0:T(8,128)(2,1)} %broadcast_in_dim.17), calls=%async_computation | async-start | bytes 4194304 | tf_op jit(solution)/shard_map/all_to_all | solution.py:50
  48.5 11.3 %collective-permute-start = (f16[16,1,64,512]{3,2,1,0:T(8,128)(2,1)S(1)}, f16[16,1,64,512]{3,2,1,0:T(8,128)(2,1)}, u32[]{:S(2)}, u32[]{:S(2)}) collective-permute-start(f16[16,1,64,512]{3,2,1,0:T(8,128)(2,1)S(1)} %bitcast.39), channel_id=1, source_target_pairs={{0,1},{1,0},{2,3},{3,2},{4,5},{5,4},{6,7},{7,6},{8,9},{9,8},{10,11... | collective-permute-start | bytes 3145736 | tf_op jit(solution)/shard_map/ppermute | solution.py:37
  56.0 3.1 %collective-permute-start.1 = (bf16[64,256]{1,0:T(8,128)(2,1)S(1)}, bf16[64,256]{1,0:T(8,128)(2,1)S(1)}, u32[]{:S(2)}, u32[]{:S(2)}) collective-permute-start(bf16[64,256]{1,0:T(8,128)(2,1)S(1)} %broadcast_select_fusion.4), channel_id=1, source_target_pairs={{0,1},{1,0},{2,3},{3,2},{4,5},{5,4},{6,7},{7,6},{8,9},{9,8},{10,11... | collective-permute-start | bytes 98312 | tf_op jit(solution)/shard_map/ppermute | solution.py:37
  59.1 2.7 %collective-permute-start.2 = (bf16[128,256]{1,0:T(8,128)(2,1)S(1)}, bf16[128,256]{1,0:T(8,128)(2,1)S(1)}, u32[]{:S(2)}, u32[]{:S(2)}) collective-permute-start(bf16[128,256]{1,0:T(8,128)(2,1)S(1)} %pad_maximum_fusion.1), channel_id=1, source_target_pairs={{0,0},{2,32},{4,64},{6,96},{8,128},{10,160},{12,192},{14,224},{16,... | collective-permute-start | bytes 196616 | tf_op jit(solution)/shard_map/ppermute | solution.py:68
  62.9 39.6 %all-to-all-start.1 = ((bf16[16,128,256]{2,1,0:T(8,128)(2,1)}), bf16[16,128,256]{2,1,0:T(8,128)(2,1)S(1)}, u32[]{:S(2)}, u32[]{:S(2)}) async-start(bf16[16,128,256]{2,1,0:T(8,128)(2,1)} %broadcast_in_dim.18), calls=%async_computation.1 | async-start | bytes 2097152 | tf_op jit(solution)/shard_map/all_to_all | solution.py:50
  103.0 9.3 %collective-permute-start.3 = (bf16[256,2048]{1,0:T(8,128)(2,1)S(1)}, bf16[256,2048]{1,0:T(8,128)(2,1)S(1)}, u32[]{:S(2)}, u32[]{:S(2)}) collective-permute-start(bf16[256,2048]{1,0:T(8,128)(2,1)S(1)} %convolution_convert_fusion), channel_id=1, source_target_pairs={{0,1},{1,0},{2,3},{3,2},{4,5},{5,4},{6,7},{7,6},{8,9},{9,8},{10,11... | collective-permute-start | bytes 3145736 | tf_op jit(solution)/shard_map/ppermute | solution.py:37
  112.9 11.6 %collective-permute-start.6 = (bf16[2,16,2048]{2,1,0:T(8,128)(2,1)S(1)}, bf16[2,16,2048]{2,1,0:T(8,128)(2,1)S(1)}, u32[]{:S(2)}, u32[]{:S(2)}) collective-permute-start(bf16[2,16,2048]{2,1,0:T(8,128)(2,1)S(1)} %get-tuple-element.14), channel_id=1, source_target_pairs={{0,4},{1,29},{2,6},{3,31},{4,8},{5,1},{6,10},{7,3},{8,12},{9,5},{1... | collective-permute-start | bytes 393224 | tf_op jit(solution)/shard_map/ppermute | solution.py:33
  114.8 9.6 %collective-permute-start.7 = (bf16[2,16,2048]{2,1,0:T(8,128)(2,1)S(1)}, bf16[2,16,2048]{2,1,0:T(8,128)(2,1)S(1)}, u32[]{:S(2)}, u32[]{:S(2)}) collective-permute-start(bf16[2,16,2048]{2,1,0:T(8,128)(2,1)S(1)} %get-tuple-element.15), channel_id=1, source_target_pairs={{0,28},{1,5},{2,30},{3,7},{4,0},{5,9},{6,2},{7,11},{8,4},{9,13},{1... | collective-permute-start | bytes 393224 | tf_op jit(solution)/shard_map/ppermute | solution.py:33
  119.1 7.1 %collective-permute-start.4 = (bf16[4,16,2048]{2,1,0:T(8,128)(2,1)S(1)}, bf16[4,16,2048]{2,1,0:T(8,128)(2,1)S(1)}, u32[]{:S(2)}, u32[]{:S(2)}) collective-permute-start(bf16[4,16,2048]{2,1,0:T(8,128)(2,1)S(1)} %get-tuple-element.16), channel_id=1, source_target_pairs={{0,2},{1,31},{2,4},{3,1},{4,6},{5,3},{6,8},{7,5},{8,10},{9,7},{10,... | collective-permute-start | bytes 786440 | tf_op jit(solution)/shard_map/ppermute | solution.py:33
  121.1 11.1 %collective-permute-start.5 = (bf16[4,16,2048]{2,1,0:T(8,128)(2,1)S(1)}, bf16[4,16,2048]{2,1,0:T(8,128)(2,1)S(1)}, u32[]{:S(2)}, u32[]{:S(2)}) collective-permute-start(bf16[4,16,2048]{2,1,0:T(8,128)(2,1)S(1)} %get-tuple-element.17), channel_id=1, source_target_pairs={{0,30},{1,3},{2,0},{3,5},{4,2},{5,7},{6,4},{7,9},{8,6},{9,11},{10,... | collective-permute-start | bytes 786440 | tf_op jit(solution)/shard_map/ppermute | solution.py:33

commit v7 on v6

--- a/solution.py
+++ b/solution.py
@@ -10,7 +10,8 @@
 TP = ("zh", "zl", "c")
 FS_TP = ("fs", "zh", "zl", "c")
 EPS = 1e-06
-SCALE = 8192.0
+SCALE = 2.0**13
+WEIGHT_SCALE = 2.0**18
 BF = jnp.bfloat16
 F32 = jnp.float32
 EVERY = [(a, b) for a in range(16) for b in range(16)]
@@ -22,10 +23,6 @@
 
 def part_of(x, at, size, dim):
     return lax.dynamic_slice_in_dim(x, at, size, dim, allow_negative_indices=False)
-
-
-def put(whole, part, at):
-    return lax.dynamic_update_slice(whole, part, at, allow_negative_indices=False)
 
 
 def fan(x, by):
@@ -45,19 +42,20 @@
     return with_layout_constraint(x, Layout(major_to_minor=tuple(range(x.ndim))))
 
 
-def spread(x):
-    every = row_major(jnp.broadcast_to(x, (16, *x.shape)))
-    return row_major(lax.all_to_all(every, "fs", 0, 0, tiled=True)).reshape(D, x.shape[1])
+def packed(x, scale):
+    return (x.astype(F32) * scale).astype(jnp.float16)
 
 
-def gather_tokens(tokens):
+def unpacked(x, scale):
+    return (x.astype(F32) / scale).astype(BF)
+
+
+def gather_tokens(x):
     c = lax.axis_index("c")
-    x = (tokens.T.astype(F32) * SCALE).astype(jnp.float16)
     mine = lax.all_gather(x, TP[:2])[:, None]
+    mine = lax.optimization_barrier(unpacked(mine, SCALE))
     other = swap(mine)
-    mine, other = ((v.astype(F32) / SCALE).astype(BF) for v in (mine, other))
-    whole = put(jnp.zeros((16, 2, 64, 512), BF), mine, (0, c, 0, 0))
-    return put(whole, other, (0, 1 - c, 0, 0)).reshape(D, 512)
+    return by_core(c, mine, other, 1).reshape(D, 512)
 
 
 def place_down(down_train):
@@ -91,16 +89,20 @@
 def body(tokens, norm_gain, gate_train, up_train, down_train):
     gate_local = (norm_gain[:, None] * gate_train).astype(BF)
     up_local = (norm_gain[:, None] * up_train).astype(BF)
-    both = spread(jnp.concatenate([gate_local, up_local], axis=1))
-    down = spread(place_down(down_train))
-    x = gather_tokens(tokens)
+    local = packed(jnp.concatenate([gate_local, up_local], axis=1), WEIGHT_SCALE)
+    x, local = lax.optimization_barrier((packed(tokens.T, SCALE), local))
+    local = jnp.concatenate([local, packed(place_down(down_train), WEIGHT_SCALE)], axis=1)
+    every = row_major(lax.all_gather(row_major(local), "fs", tiled=True))
+    both = unpacked(every[:, :512], WEIGHT_SCALE)
+    down = row_major(unpacked(every[:, 512:], WEIGHT_SCALE))
+    x = gather_tokens(x)
     wide = x.astype(F32)
     scale = lax.rsqrt(jnp.sum(wide * wide, axis=0) / D + EPS)[:, None]
     sums = lax.dot_general(x, both, (((0,), (0,)), ((), ())), preferred_element_type=F32)
     gate, up = sums[:, :256], sums[:, 256:]
     hidden = (jax.nn.silu(gate * scale) * (up * scale)).astype(BF)
     gate_serve, up_serve = both[:, :256], both[:, 256:]
-    return scatter_sum(hidden, down, (gate_serve, up_serve, down.T))
+    return scatter_sum(hidden, down, (gate_serve, up_serve, row_major(down.T)))
 
 
 def solution(mesh):

time: 158 us -> 155 us (0.981)
  blocking collectives: 61.4 us -> 87 us
  starting transfers between devices: 58.2 us -> 43.1 us
  waiting for transfers between devices: 20.7 us -> 7.95 us
  other arithmetic: 4.45 us -> 9.31 us
  local copies, waits for them, and re-layouts: 7.44 us -> 3.82 us
    all_to_all x2 -> x0, starting transfers between devices: 31.8 us -> none  [spread(): lax.all_to_all(every, 'fs', 0, 0, tiled=True)]
    all_gather x0 -> x1, blocking collectives: none -> 31.1 us  [body(): every = row_major(lax.all_gather(row_major(local), 'fs', tiled=True))]
    ppermute x3, starting transfers between devices: 14.2 us -> 31 us  [swap(): return lax.ppermute(x, 'c', [(0, 1), (1, 0)])]
    all_to_all x2 -> x0, waiting for transfers between devices: 12.4 us -> none  [spread(): lax.all_to_all(every, 'fs', 0, 0, tiled=True)]
    all_gather x1, blocking collectives: 37.5 us -> 30.2 us  [gather_tokens(): mine = lax.all_gather(x, TP[:2])[:, None]]
    convert_element_type x2 -> x6, other arithmetic: 0.23 us -> 3.74 us  [the longest x3 2.82 us: unpacked(): return (x.astype(F32) / scale).astype(BF)]
    broadcast_in_dim x3 -> x0, local copies, waits for them, and re-layouts: 2.82 us -> none  [the longest x2 2.59 us: spread(): every = row_major(jnp.broadcast_to(x, (16, *x.shape)))]
    another operation x0 -> x1, local copies, waits for them, and re-layouts: none -> 2.26 us  [row_major(): with_layout_constraint(x, Layout(major_to_minor=tuple(range(x.ndim))))]
  transfers between devices with their start and end apart: 10 -> 8, of which waited for: 4 -> 4; matrix products, arithmetic and copies ran while one was open for 7% -> 6% of each run, Pallas kernels for 0% -> 0%
where the time goes in v7:
time: 155 us; the launch traced here: 154 us
  blocking collectives  87 us (56%)
  starting transfers between devices  43.1 us (28%)
  other arithmetic  9.31 us (6%)
  waiting for transfers between devices  7.95 us (5%)
  local copies, waits for them, and re-layouts  3.82 us (2%)
  matrix products  2.29 us (1%)
    all_gather x1, blocking collectives, body(): every = row_major(lax.all_gather(row_major(local), 'fs', tiled=True))  31.1 us
    ppermute x3, starting transfers between devices, swap(): return lax.ppermute(x, 'c', [(0, 1), (1, 0)])  31 us
    all_gather x1, blocking collectives, gather_tokens(): mine = lax.all_gather(x, TP[:2])[:, None]  30.2 us
    all_to_all x1, blocking collectives, scatter_sum(): rows = lax.all_to_all(near, 'zh', 0, 0, tiled=True)  25.7 us
    ppermute x4, starting transfers between devices, fan(): return lax.ppermute(x, TP, pairs)  11.5 us
    ppermute x4, waiting for transfers between devices, fan(): return lax.ppermute(x, TP, pairs)  7.58 us
  transfers between devices with their start and end apart: 8, of which 4 were waited for; matrix products, arithmetic and copies ran while one was open for 6% of the time, Pallas kernels for 0%

profile of v7, /device:TPU:1, one launch (start us, length us, event | category | flops | bytes accessed | tf_op | source)
XLA Modules:
  0.0 154.3 jit_solution(1268954251422197009)
XLA Ops:
  0.6 0.9 convert_bitcast_fusion
  1.6 8.7 %collective-permute-start.1 = (bf16[64,256]{1,0:T(8,128)(2,1)S(1)}, bf16[64,256]{1,0:T(8,128)(2,1)S(1)}, u32[]{:S(2)}, u32[]{:S(2)}) collective-permute-start(bf16[64,256]{1,0:T(8,128)(2,1)S(1)} %broadcast_select_fusion.6), channel_id=1, source_target_pairs={{0,1},{1,0},{2,3},{3,2},{4,5},{5,4},{6,7},{7,6},{8,9},{9,8},{10,11... | collective-permute-start | bytes 98312 | tf_op jit(solution)/shard_map/ppermute | solution.py:34
  10.3 0.9 fusion.4
  11.2 1.1 multiply_convert_fusion.6
  12.3 30.2 %all-gather.3 = f16[1024,512]{1,0:T(8,128)(2,1)S(1)} all-gather(f16[64,512]{1,0:T(8,128)(2,1)S(1)} %fusion.4), channel_id=2, replica_groups=mesh['fs'=16,'zh'=4,'zl'=4,'c'=2] {'zh','zl'}, dimensions={0}, use_global_device_ids=true | all-gather | bytes 1114112 | tf_op jit(solution)/shard_map/all_gather | solution.py:55
  42.5 0.0 collective-permute-done.1
  42.6 0.7 collective-permute-start.2
  43.2 1.2 multiply_convert_fusion.1
  44.4 8.1 %collective-permute-start = (bf16[16,1,64,512]{3,2,1,0:T(8,128)(2,1)}, bf16[16,1,64,512]{3,2,1,0:T(8,128)(2,1)}, u32[]{:S(2)}, u32[]{:S(2)}) collective-permute-start(bf16[16,1,64,512]{3,2,1,0:T(8,128)(2,1)} %bitcast.1), channel_id=1, source_target_pairs={{0,1},{1,0},{2,3},{3,2},{4,5},{5,4},{6,7},{7,6},{8,9},{9,8},{10,11... | collective-permute-start | bytes 3145736 | tf_op jit(solution)/shard_map/ppermute | solution.py:34
  52.6 0.0 collective-permute-done.2
  52.6 0.1 pad_maximum_fusion.1
  52.7 31.1 %all-gather.4 = f16[2048,768]{1,0:T(8,128)(2,1)S(1)} all-gather(f16[128,768]{1,0:T(8,128)(2,1)S(1)} %pad_maximum_fusion.1), channel_id=1, replica_groups=mesh['fs'=16,'zh'=4,'zl'=4,'c'=2] {'fs'}, dimensions={0}, use_global_device_ids=true | all-gather | bytes 3342336 | tf_op jit(solution)/shard_map/all_gather | solution.py:95
  83.7 1.2 multiply_convert_fusion.2
  84.9 2.3 %copy.10 = bf16[2048,256]{0,1:T(8,128)(2,1)} copy(bf16[2048,256]{1,0:T(8,128)(2,1)} %multiply_convert_fusion.2) | data formatting | bytes 2097152 | tf_op jit(solution)/shard_map/layout_constraint | solution.py:42
  87.2 0.0 collective-permute-done
  87.2 1.7 %broadcast_select_fusion.1 = (bf16[16,1,64,512]{3,2,1,0:T(8,128)(2,1)S(1)}, bf16[16,1,64,512]{3,2,1,0:T(8,128)(2,1)S(1)}) fusion(bf16[16,1,64,512]{3,2,1,0:T(8,128)(2,1)} %bitcast.1, bf16[16,1,64,512]{3,2,1,0:T(8,128)(2,1)} %collective-permute-done, pred[]{:T(512)S(6)} %eq.2), kind=kLoop, calls=%fused_computation.8 | loop fusion | flops 1048576 | bytes 4194305 | tf_op jit(solution)/shard_map/jit(_where)/select_n | solution.py:38
  88.9 0.6 multiply_reduce_fusion
  89.4 0.2 pad_maximum_fusion
  89.6 1.3 fusion.6
  90.9 0.2 fusion.1
  91.2 0.5 convolution_convert_fusion
  91.7 14.1 %collective-permute-start.3 = (bf16[256,2048]{1,0:T(8,128)(2,1)S(1)}, bf16[256,2048]{1,0:T(8,128)(2,1)S(1)}, u32[]{:S(2)}, u32[]{:S(2)}) collective-permute-start(bf16[256,2048]{1,0:T(8,128)(2,1)S(1)} %convolution_convert_fusion), channel_id=1, source_target_pairs={{0,1},{1,0},{2,3},{3,2},{4,5},{5,4},{6,7},{7,6},{8,9},{9,8},{10,11... | collective-permute-start | bytes 3145736 | tf_op jit(solution)/shard_map/ppermute | solution.py:34
  105.8 0.4 multiply_convert_fusion
  106.3 1.5 fusion.7
  107.7 0.4 collective-permute-done.3
  108.1 0.5 add_convert_fusion
  108.6 1.9 %collective-permute-start.6 = (bf16[2,16,2048]{2,1,0:T(8,128)(2,1)S(1)}, bf16[2,16,2048]{2,1,0:T(8,128)(2,1)S(1)}, u32[]{:S(2)}, u32[]{:S(2)}) collective-permute-start(bf16[2,16,2048]{2,1,0:T(8,128)(2,1)S(1)} %get-tuple-element.20), channel_id=1, source_target_pairs={{0,4},{1,29},{2,6},{3,31},{4,8},{5,1},{6,10},{7,3},{8,12},{9,5},{1... | collective-permute-start | bytes 393224 | tf_op jit(solution)/shard_map/ppermute | solution.py:30
  110.6 4.3 %collective-permute-start.7 = (bf16[2,16,2048]{2,1,0:T(8,128)(2,1)S(1)}, bf16[2,16,2048]{2,1,0:T(8,128)(2,1)S(1)}, u32[]{:S(2)}, u32[]{:S(2)}) collective-permute-start(bf16[2,16,2048]{2,1,0:T(8,128)(2,1)S(1)} %get-tuple-element.21), channel_id=1, source_target_pairs={{0,28},{1,5},{2,30},{3,7},{4,0},{5,9},{6,2},{7,11},{8,4},{9,13},{1... | collective-permute-start | bytes 393224 | tf_op jit(solution)/shard_map/ppermute | solution.py:30
  114.9 2.0 %collective-permute-start.4 = (bf16[4,16,2048]{2,1,0:T(8,128)(2,1)S(1)}, bf16[4,16,2048]{2,1,0:T(8,128)(2,1)S(1)}, u32[]{:S(2)}, u32[]{:S(2)}) collective-permute-start(bf16[4,16,2048]{2,1,0:T(8,128)(2,1)S(1)} %get-tuple-element.22), channel_id=1, source_target_pairs={{0,2},{1,31},{2,4},{3,1},{4,6},{5,3},{6,8},{7,5},{8,10},{9,7},{10,... | collective-permute-start | bytes 786440 | tf_op jit(solution)/shard_map/ppermute | solution.py:30
  116.9 3.2 %collective-permute-start.5 = (bf16[4,16,2048]{2,1,0:T(8,128)(2,1)S(1)}, bf16[4,16,2048]{2,1,0:T(8,128)(2,1)S(1)}, u32[]{:S(2)}, u32[]{:S(2)}) collective-permute-start(bf16[4,16,2048]{2,1,0:T(8,128)(2,1)S(1)} %get-tuple-element.23), channel_id=1, source_target_pairs={{0,30},{1,3},{2,0},{3,5},{4,2},{5,7},{6,4},{7,9},{8,6},{9,11},{10,... | collective-permute-start | bytes 786440 | tf_op jit(solution)/shard_map/ppermute | solution.py:30
  120.2 0.0 collective-permute-done.6
  120.2 0.1 collective-permute-done.7
  120.4 3.1 %collective-permute-done.4 = bf16[4,16,2048]{2,1,0:T(8,128)(2,1)S(1)} collective-permute-done((bf16[4,16,2048]{2,1,0:T(8,128)(2,1)S(1)}, bf16[4,16,2048]{2,1,0:T(8,128)(2,1)S(1)}, u32[]{:S(2)}, u32[]{:S(2)}) %collective-permute-start.4) | collective-permute-done | bytes 262176 | tf_op jit(solution)/shard_map/ppermute | solution.py:30
  123.4 4.4 %collective-permute-done.5 = bf16[4,16,2048]{2,1,0:T(8,128)(2,1)S(1)} collective-permute-done((bf16[4,16,2048]{2,1,0:T(8,128)(2,1)S(1)}, bf16[4,16,2048]{2,1,0:T(8,128)(2,1)S(1)}, u32[]{:S(2)}, u32[]{:S(2)}) %collective-permute-start.5) | collective-permute-done | bytes 262176 | tf_op jit(solution)/shard_map/ppermute | solution.py:30
  127.8 0.1 fusion.3
  127.9 25.7 %all_to_all.5 = bf16[4,16,2048]{2,1,0:T(8,128)(2,1)S(1)} all-to-all(bf16[4,16,2048]{2,1,0:T(8,128)(2,1)S(1)} %fusion.3), channel_id=1, replica_groups=mesh['fs'=16,'zh'=4,'zl'=4,'c'=2] {'zh'}, dimensions={0} | all-to-all | bytes 524288 | tf_op jit(solution)/shard_map/all_to_all | solution.py:85
  153.7 0.7 reduce_sum.22
  (10 shorter events, 0.2 us)
Async XLA Ops:
  1.6 41.0 %collective-permute-start.1 = (bf16[64,256]{1,0:T(8,128)(2,1)S(1)}, bf16[64,256]{1,0:T(8,128)(2,1)S(1)}, u32[]{:S(2)}, u32[]{:S(2)}) collective-permute-start(bf16[64,256]{1,0:T(8,128)(2,1)S(1)} %broadcast_select_fusion.6), channel_id=1, source_target_pairs={{0,1},{1,0},{2,3},{3,2},{4,5},{5,4},{6,7},{7,6},{8,9},{9,8},{10,11... | collective-permute-start | bytes 98312 | tf_op jit(solution)/shard_map/ppermute | solution.py:34
  42.6 10.0 %collective-permute-start.2 = (bf16[128,256]{1,0:T(8,128)(2,1)S(1)}, bf16[128,256]{1,0:T(8,128)(2,1)S(1)}, u32[]{:S(2)}, u32[]{:S(2)}) collective-permute-start(bf16[128,256]{1,0:T(8,128)(2,1)S(1)} %pad_maximum_fusion.2), channel_id=1, source_target_pairs={{0,0},{2,32},{4,64},{6,96},{8,128},{10,160},{12,192},{14,224},{16,... | collective-permute-start | bytes 196616 | tf_op jit(solution)/shard_map/ppermute | solution.py:66
  44.4 42.8 %collective-permute-start = (bf16[16,1,64,512]{3,2,1,0:T(8,128)(2,1)}, bf16[16,1,64,512]{3,2,1,0:T(8,128)(2,1)}, u32[]{:S(2)}, u32[]{:S(2)}) collective-permute-start(bf16[16,1,64,512]{3,2,1,0:T(8,128)(2,1)} %bitcast.1), channel_id=1, source_target_pairs={{0,1},{1,0},{2,3},{3,2},{4,5},{5,4},{6,7},{7,6},{8,9},{9,8},{10,11... | collective-permute-start | bytes 3145736 | tf_op jit(solution)/shard_map/ppermute | solution.py:34
  91.7 16.4 %collective-permute-start.3 = (bf16[256,2048]{1,0:T(8,128)(2,1)S(1)}, bf16[256,2048]{1,0:T(8,128)(2,1)S(1)}, u32[]{:S(2)}, u32[]{:S(2)}) collective-permute-start(bf16[256,2048]{1,0:T(8,128)(2,1)S(1)} %convolution_convert_fusion), channel_id=1, source_target_pairs={{0,1},{1,0},{2,3},{3,2},{4,5},{5,4},{6,7},{7,6},{8,9},{9,8},{10,11... | collective-permute-start | bytes 3145736 | tf_op jit(solution)/shard_map/ppermute | solution.py:34
  108.6 11.6 %collective-permute-start.6 = (bf16[2,16,2048]{2,1,0:T(8,128)(2,1)S(1)}, bf16[2,16,2048]{2,1,0:T(8,128)(2,1)S(1)}, u32[]{:S(2)}, u32[]{:S(2)}) collective-permute-start(bf16[2,16,2048]{2,1,0:T(8,128)(2,1)S(1)} %get-tuple-element.20), channel_id=1, source_target_pairs={{0,4},{1,29},{2,6},{3,31},{4,8},{5,1},{6,10},{7,3},{8,12},{9,5},{1... | collective-permute-start | bytes 393224 | tf_op jit(solution)/shard_map/ppermute | solution.py:30
  110.6 9.8 %collective-permute-start.7 = (bf16[2,16,2048]{2,1,0:T(8,128)(2,1)S(1)}, bf16[2,16,2048]{2,1,0:T(8,128)(2,1)S(1)}, u32[]{:S(2)}, u32[]{:S(2)}) collective-permute-start(bf16[2,16,2048]{2,1,0:T(8,128)(2,1)S(1)} %get-tuple-element.21), channel_id=1, source_target_pairs={{0,28},{1,5},{2,30},{3,7},{4,0},{5,9},{6,2},{7,11},{8,4},{9,13},{1... | collective-permute-start | bytes 393224 | tf_op jit(solution)/shard_map/ppermute | solution.py:30
  114.9 8.6 %collective-permute-start.4 = (bf16[4,16,2048]{2,1,0:T(8,128)(2,1)S(1)}, bf16[4,16,2048]{2,1,0:T(8,128)(2,1)S(1)}, u32[]{:S(2)}, u32[]{:S(2)}) collective-permute-start(bf16[4,16,2048]{2,1,0:T(8,128)(2,1)S(1)} %get-tuple-element.22), channel_id=1, source_target_pairs={{0,2},{1,31},{2,4},{3,1},{4,6},{5,3},{6,8},{7,5},{8,10},{9,7},{10,... | collective-permute-start | bytes 786440 | tf_op jit(solution)/shard_map/ppermute | solution.py:30
  116.9 10.9 %collective-permute-start.5 = (bf16[4,16,2048]{2,1,0:T(8,128)(2,1)S(1)}, bf16[4,16,2048]{2,1,0:T(8,128)(2,1)S(1)}, u32[]{:S(2)}, u32[]{:S(2)}) collective-permute-start(bf16[4,16,2048]{2,1,0:T(8,128)(2,1)S(1)} %get-tuple-element.23), channel_id=1, source_target_pairs={{0,30},{1,3},{2,0},{3,5},{4,2},{5,7},{6,4},{7,9},{8,6},{9,11},{10,... | collective-permute-start | bytes 786440 | tf_op jit(solution)/shard_map/ppermute | solution.py:30

commit v8 on v7

--- a/solution.py
+++ b/solution.py
@@ -10,8 +10,7 @@
 TP = ("zh", "zl", "c")
 FS_TP = ("fs", "zh", "zl", "c")
 EPS = 1e-06
-SCALE = 2.0**13
-WEIGHT_SCALE = 2.0**18
+SCALE = 8192.0
 BF = jnp.bfloat16
 F32 = jnp.float32
 EVERY = [(a, b) for a in range(16) for b in range(16)]
@@ -42,18 +41,18 @@
     return with_layout_constraint(x, Layout(major_to_minor=tuple(range(x.ndim))))
 
 
-def packed(x, scale):
-    return (x.astype(F32) * scale).astype(jnp.float16)
+def copies(x):
+    return row_major(jnp.broadcast_to(x, (16, *x.shape)))
 
 
-def unpacked(x, scale):
-    return (x.astype(F32) / scale).astype(BF)
+def spread(every):
+    return row_major(lax.all_to_all(every, "fs", 0, 0, tiled=True)).reshape(D, every.shape[2])
 
 
 def gather_tokens(x):
     c = lax.axis_index("c")
     mine = lax.all_gather(x, TP[:2])[:, None]
-    mine = lax.optimization_barrier(unpacked(mine, SCALE))
+    mine = lax.optimization_barrier((mine.astype(F32) / SCALE).astype(BF))
     other = swap(mine)
     return by_core(c, mine, other, 1).reshape(D, 512)
 
@@ -89,12 +88,10 @@
 def body(tokens, norm_gain, gate_train, up_train, down_train):
     gate_local = (norm_gain[:, None] * gate_train).astype(BF)
     up_local = (norm_gain[:, None] * up_train).astype(BF)
-    local = packed(jnp.concatenate([gate_local, up_local], axis=1), WEIGHT_SCALE)
-    x, local = lax.optimization_barrier((packed(tokens.T, SCALE), local))
-    local = jnp.concatenate([local, packed(place_down(down_train), WEIGHT_SCALE)], axis=1)
-    every = row_major(lax.all_gather(row_major(local), "fs", tiled=True))
-    both = unpacked(every[:, :512], WEIGHT_SCALE)
-    down = row_major(unpacked(every[:, 512:], WEIGHT_SCALE))
+    both = spread(copies(jnp.concatenate([gate_local, up_local], axis=1)))
+    x = (tokens.T.astype(F32) * SCALE).astype(jnp.float16)
+    x, placed = lax.optimization_barrier((x, copies(place_down(down_train))))
+    down = spread(placed)
     x = gather_tokens(x)
     wide = x.astype(F32)
     scale = lax.rsqrt(jnp.sum(wide * wide, axis=0) / D + EPS)[:, None]
@@ -102,7 +99,7 @@
     gate, up = sums[:, :256], sums[:, 256:]
     hidden = (jax.nn.silu(gate * scale) * (up * scale)).astype(BF)
     gate_serve, up_serve = both[:, :256], both[:, 256:]
-    return scatter_sum(hidden, down, (gate_serve, up_serve, row_major(down.T)))
+    return scatter_sum(hidden, down, (gate_serve, up_serve, down.T))
 
 
 def solution(mesh):

time: 155 us -> 166 us (1.071)
  waiting for transfers between devices: 7.95 us -> 23.7 us
  blocking collectives: 87 us -> 75.2 us
  starting transfers between devices: 43.1 us -> 47.1 us
  matrix products: 2.29 us -> 6 us
  other arithmetic: 9.31 us -> 6.74 us
  local copies, waits for them, and re-layouts: 3.82 us -> 5.59 us
    all_gather x1 -> x0, blocking collectives: 31.1 us -> none  [body(): every = row_major(lax.all_gather(row_major(local), 'fs', tiled=True))]
    all_gather x1, blocking collectives: 30.2 us -> 49.9 us  [gather_tokens(): mine = lax.all_gather(x, TP[:2])[:, None]]
    all_to_all x0 -> x2, waiting for transfers between devices: none -> 13.2 us  [spread(): lax.all_to_all(every, 'fs', 0, 0, tiled=True)]
    all_to_all x0 -> x2, starting transfers between devices: none -> 11.2 us  [spread(): lax.all_to_all(every, 'fs', 0, 0, tiled=True)]
    ppermute x3, starting transfers between devices: 31 us -> 23.8 us  [swap(): return lax.ppermute(x, 'c', [(0, 1), (1, 0)])]
    convert_element_type x6 -> x2, other arithmetic: 3.74 us -> 0.23 us  [the longest x1 0.21 us: gather_tokens(): mine = lax.optimization_barrier((mine.astype(F32) / SCALE).astype(BF))]
    broadcast_in_dim x0 -> x2, local copies, waits for them, and re-layouts: none -> 2.61 us  [copies(): return row_major(jnp.broadcast_to(x, (16, *x.shape)))]
    another operation x1 -> x0, local copies, waits for them, and re-layouts: 2.26 us -> none  [row_major(): with_layout_constraint(x, Layout(major_to_minor=tuple(range(x.ndim))))]
  transfers between devices with their start and end apart: 8 -> 10, of which waited for: 4 -> 5; matrix products, arithmetic and copies ran while one was open for 6% -> 8% of each run, Pallas kernels for 0% -> 0%
where the time goes in v8:
time: 166 us; the launch traced here: 165 us
  blocking collectives  75.2 us (45%)
  starting transfers between devices  47.1 us (28%)
  waiting for transfers between devices  23.7 us (14%)
  other arithmetic  6.74 us (4%)
  matrix products  6 us (4%)
  local copies, waits for them, and re-layouts  5.59 us (3%)
    all_gather x1, blocking collectives, gather_tokens(): mine = lax.all_gather(x, TP[:2])[:, None]  49.9 us
    all_to_all x1, blocking collectives, scatter_sum(): rows = lax.all_to_all(near, 'zh', 0, 0, tiled=True)  25.3 us
    ppermute x3, starting transfers between devices, swap(): return lax.ppermute(x, 'c', [(0, 1), (1, 0)])  23.8 us
    all_to_all x2, waiting for transfers between devices, spread(): lax.all_to_all(every, 'fs', 0, 0, tiled=True)  13.2 us
    ppermute x4, starting transfers between devices, fan(): return lax.ppermute(x, TP, pairs)  11.5 us
    all_to_all x2, starting transfers between devices, spread(): lax.all_to_all(every, 'fs', 0, 0, tiled=True)  11.2 us
    ppermute x4, waiting for transfers between devices, fan(): return lax.ppermute(x, TP, pairs)  8.12 us
  transfers between devices with their start and end apart: 10, of which 5 were waited for; matrix products, arithmetic and copies ran while one was open for 8% of the time, Pallas kernels for 0%

profile of v8, /device:TPU:1, one launch (start us, length us, event | category | flops | bytes accessed | tf_op | source)
XLA Modules:
  0.0 165.3 jit_solution(8067202606273929808)
XLA Ops:
  0.6 0.9 convert_bitcast_fusion
  1.6 8.7 %collective-permute-start = (bf16[64,256]{1,0:T(8,128)(2,1)S(1)}, bf16[64,256]{1,0:T(8,128)(2,1)S(1)}, u32[]{:S(2)}, u32[]{:S(2)}) collective-permute-start(bf16[64,256]{1,0:T(8,128)(2,1)S(1)} %broadcast_select_fusion.6), channel_id=1, source_target_pairs={{0,1},{1,0},{2,3},{3,2},{4,5},{5,4},{6,7},{7,6},{8,9},{9,8},{10,11... | collective-permute-start | bytes 98312 | tf_op jit(solution)/shard_map/ppermute | solution.py:33
  10.3 1.1 multiply_convert_fusion.2
  11.4 1.5 broadcast_in_dim.5
  13.0 0.0 copy-start
  13.0 3.8 %all-to-all-start = ((bf16[16,128,512]{2,1,0:T(8,128)(2,1)}), bf16[16,128,512]{2,1,0:T(8,128)(2,1)S(1)}, u32[]{:S(2)}, u32[]{:S(2)}) async-start(bf16[16,128,512]{2,1,0:T(8,128)(2,1)} %broadcast_in_dim.5), calls=%async_computation | async-start | bytes 4194304 | tf_op jit(solution)/shard_map/all_to_all | solution.py:49
  16.8 0.0 collective-permute-done
  16.9 0.7 collective-permute-start.1
  17.5 0.0 copy-done
  17.6 0.0 collective-permute-done.1
  17.6 1.1 broadcast_in_dim.4
  18.7 49.9 %all-gather.2 = f16[1024,512]{1,0:T(8,128)(2,1)S(1)} all-gather(f16[64,512]{1,0:T(8,128)(2,1)S(1)} %fusion.4), channel_id=2, replica_groups=mesh['fs'=16,'zh'=4,'zl'=4,'c'=2] {'zh','zl'}, dimensions={0}, use_global_device_ids=true | all-gather | bytes 1114112 | tf_op jit(solution)/shard_map/all_gather | solution.py:54
  68.6 0.2 multiply_convert_fusion
  68.8 11.0 %collective-permute-start.2 = (bf16[16,1,64,512]{3,2,1,0:T(8,128)(2,1)S(1)}, bf16[16,1,64,512]{3,2,1,0:T(8,128)(2,1)}, u32[]{:S(2)}, u32[]{:S(2)}) collective-permute-start(bf16[16,1,64,512]{3,2,1,0:T(8,128)(2,1)S(1)} %bitcast.38), channel_id=1, source_target_pairs={{0,1},{1,0},{2,3},{3,2},{4,5},{5,4},{6,7},{7,6},{8,9},{9,8},{10,11... | collective-permute-start | bytes 3145736 | tf_op jit(solution)/shard_map/ppermute | solution.py:33
  79.8 2.4 %collective-permute-done.2 = bf16[16,1,64,512]{3,2,1,0:T(8,128)(2,1)} collective-permute-done((bf16[16,1,64,512]{3,2,1,0:T(8,128)(2,1)S(1)}, bf16[16,1,64,512]{3,2,1,0:T(8,128)(2,1)}, u32[]{:S(2)}, u32[]{:S(2)}) %collective-permute-start.2) | collective-permute-done | bytes 1048608 | tf_op jit(solution)/shard_map/ppermute | solution.py:33
  82.2 1.4 broadcast_select_fusion.1
  83.6 0.6 multiply_reduce_fusion
  84.2 1.5 pad_maximum_fusion
  85.7 0.0 all-to-all-done
  85.7 7.4 %all-to-all-start.1 = ((bf16[16,128,256]{2,1,0:T(8,128)(2,1)}), bf16[16,128,256]{2,1,0:T(8,128)(2,1)S(1)}, u32[]{:S(2)}, u32[]{:S(2)}) async-start(bf16[16,128,256]{2,1,0:T(8,128)(2,1)} %broadcast_in_dim.4), calls=%async_computation.1 | async-start | bytes 2097152 | tf_op jit(solution)/shard_map/all_to_all | solution.py:49
  93.1 2.9 %fusion.6 = f32[512,512]{1,0:T(8,128)S(1)} fusion(bf16[2048,512]{1,0:T(8,128)(2,1)} %bitcast.40, bf16[2048,512]{1,0:T(8,128)(2,1)S(1)} %bitcast.33), kind=kOutput, calls=%fused_computation.35 | convolution fusion | flops 1073741824 | bytes 5242880 | tf_op jit(solution)/shard_map/dot_general | solution.py:98
  95.9 0.2 fusion.1
  96.2 13.2 %all-to-all-done.1 = bf16[16,128,256]{2,1,0:T(8,128)(2,1)S(1)} async-done(((bf16[16,128,256]{2,1,0:T(8,128)(2,1)}), bf16[16,128,256]{2,1,0:T(8,128)(2,1)S(1)}, u32[]{:S(2)}, u32[]{:S(2)}) %all-to-all-start.1) | async-done | bytes 1048608 | tf_op jit(solution)/shard_map/all_to_all | solution.py:49
  109.4 1.4 convolution_convert_fusion
  110.8 4.0 %collective-permute-start.3 = (bf16[256,2048]{1,0:T(8,128)(2,1)}, bf16[256,2048]{1,0:T(8,128)(2,1)}, u32[]{:S(2)}, u32[]{:S(2)}) collective-permute-start(bf16[256,2048]{1,0:T(8,128)(2,1)} %convolution_convert_fusion), channel_id=1, source_target_pairs={{0,1},{1,0},{2,3},{3,2},{4,5},{5,4},{6,7},{7,6},{8,9},{9,8},{10,11... | collective-permute-start | bytes 3145736 | tf_op jit(solution)/shard_map/ppermute | solution.py:33
  114.9 1.4 copy.10
  116.3 1.4 fusion.5
  117.8 0.0 collective-permute-done.3
  117.8 1.7 %add_convert_fusion = bf16[256,2048]{1,0:T(8,128)(2,1)S(1)} fusion(bf16[256,2048]{1,0:T(8,128)(2,1)} %collective-permute-done.3, bf16[256,256]{1,0:T(8,128)(2,1)S(1)} %bitcast.43, bf16[2048,256]{1,0:T(8,128)(2,1)S(1)} %bitcast.32), kind=kOutput, calls=%fused_computation.4 | convolution fusion | flops 270008320 | bytes 3276800 | tf_op jit(solution)/shard_map/dot_general | solution.py:75
  119.5 4.0 %collective-permute-start.6 = (bf16[2,16,2048]{2,1,0:T(8,128)(2,1)S(1)}, bf16[2,16,2048]{2,1,0:T(8,128)(2,1)S(1)}, u32[]{:S(2)}, u32[]{:S(2)}) collective-permute-start(bf16[2,16,2048]{2,1,0:T(8,128)(2,1)S(1)} %get-tuple-element.20), channel_id=1, source_target_pairs={{0,4},{1,29},{2,6},{3,31},{4,8},{5,1},{6,10},{7,3},{8,12},{9,5},{1... | collective-permute-start | bytes 393224 | tf_op jit(solution)/shard_map/ppermute | solution.py:29
  123.5 2.2 %collective-permute-start.7 = (bf16[2,16,2048]{2,1,0:T(8,128)(2,1)S(1)}, bf16[2,16,2048]{2,1,0:T(8,128)(2,1)S(1)}, u32[]{:S(2)}, u32[]{:S(2)}) collective-permute-start(bf16[2,16,2048]{2,1,0:T(8,128)(2,1)S(1)} %get-tuple-element.21), channel_id=1, source_target_pairs={{0,28},{1,5},{2,30},{3,7},{4,0},{5,9},{6,2},{7,11},{8,4},{9,13},{1... | collective-permute-start | bytes 393224 | tf_op jit(solution)/shard_map/ppermute | solution.py:29
  125.7 2.6 %collective-permute-start.4 = (bf16[4,16,2048]{2,1,0:T(8,128)(2,1)S(1)}, bf16[4,16,2048]{2,1,0:T(8,128)(2,1)S(1)}, u32[]{:S(2)}, u32[]{:S(2)}) collective-permute-start(bf16[4,16,2048]{2,1,0:T(8,128)(2,1)S(1)} %get-tuple-element.22), channel_id=1, source_target_pairs={{0,2},{1,31},{2,4},{3,1},{4,6},{5,3},{6,8},{7,5},{8,10},{9,7},{10,... | collective-permute-start | bytes 786440 | tf_op jit(solution)/shard_map/ppermute | solution.py:29
  128.3 2.7 %collective-permute-start.5 = (bf16[4,16,2048]{2,1,0:T(8,128)(2,1)S(1)}, bf16[4,16,2048]{2,1,0:T(8,128)(2,1)S(1)}, u32[]{:S(2)}, u32[]{:S(2)}) collective-permute-start(bf16[4,16,2048]{2,1,0:T(8,128)(2,1)S(1)} %get-tuple-element.23), channel_id=1, source_target_pairs={{0,30},{1,3},{2,0},{3,5},{4,2},{5,7},{6,4},{7,9},{8,6},{9,11},{10,... | collective-permute-start | bytes 786440 | tf_op jit(solution)/shard_map/ppermute | solution.py:29
  131.0 0.0 collective-permute-done.6
  131.1 0.5 collective-permute-done.7
  131.6 1.8 %collective-permute-done.4 = bf16[4,16,2048]{2,1,0:T(8,128)(2,1)S(1)} collective-permute-done((bf16[4,16,2048]{2,1,0:T(8,128)(2,1)S(1)}, bf16[4,16,2048]{2,1,0:T(8,128)(2,1)S(1)}, u32[]{:S(2)}, u32[]{:S(2)}) %collective-permute-start.4) | collective-permute-done | bytes 262176 | tf_op jit(solution)/shard_map/ppermute | solution.py:29
  133.4 5.8 %collective-permute-done.5 = bf16[4,16,2048]{2,1,0:T(8,128)(2,1)S(1)} collective-permute-done((bf16[4,16,2048]{2,1,0:T(8,128)(2,1)S(1)}, bf16[4,16,2048]{2,1,0:T(8,128)(2,1)S(1)}, u32[]{:S(2)}, u32[]{:S(2)}) %collective-permute-start.5) | collective-permute-done | bytes 262176 | tf_op jit(solution)/shard_map/ppermute | solution.py:29
  139.2 0.1 fusion.3
  139.3 25.3 %all_to_all.15 = bf16[4,16,2048]{2,1,0:T(8,128)(2,1)S(1)} all-to-all(bf16[4,16,2048]{2,1,0:T(8,128)(2,1)S(1)} %fusion.3), channel_id=1, replica_groups=mesh['fs'=16,'zh'=4,'zl'=4,'c'=2] {'zh'}, dimensions={0} | all-to-all | bytes 524288 | tf_op jit(solution)/shard_map/all_to_all | solution.py:84
  164.6 0.7 reduce_sum.22
  (10 shorter events, 0.2 us)
Async XLA Ops:
  1.6 15.3 %collective-permute-start = (bf16[64,256]{1,0:T(8,128)(2,1)S(1)}, bf16[64,256]{1,0:T(8,128)(2,1)S(1)}, u32[]{:S(2)}, u32[]{:S(2)}) collective-permute-start(bf16[64,256]{1,0:T(8,128)(2,1)S(1)} %broadcast_select_fusion.6), channel_id=1, source_target_pairs={{0,1},{1,0},{2,3},{3,2},{4,5},{5,4},{6,7},{7,6},{8,9},{9,8},{10,11... | collective-permute-start | bytes 98312 | tf_op jit(solution)/shard_map/ppermute | solution.py:33
  13.0 4.6 %copy-start = (bf16[512,64]{0,1:T(8,128)(2,1)S(1)}, bf16[512,64]{0,1:T(8,128)(2,1)}, u32[]{:S(2)}) copy-start(bf16[512,64]{0,1:T(8,128)(2,1)} %param.5) | copy-start | bytes 196612
  13.0 72.7 %all-to-all-start = ((bf16[16,128,512]{2,1,0:T(8,128)(2,1)}), bf16[16,128,512]{2,1,0:T(8,128)(2,1)S(1)}, u32[]{:S(2)}, u32[]{:S(2)}) async-start(bf16[16,128,512]{2,1,0:T(8,128)(2,1)} %broadcast_in_dim.5), calls=%async_computation | async-start | bytes 4194304 | tf_op jit(solution)/shard_map/all_to_all | solution.py:49
  16.9 0.7 collective-permute-start.1
  68.8 13.4 %collective-permute-start.2 = (bf16[16,1,64,512]{3,2,1,0:T(8,128)(2,1)S(1)}, bf16[16,1,64,512]{3,2,1,0:T(8,128)(2,1)}, u32[]{:S(2)}, u32[]{:S(2)}) collective-permute-start(bf16[16,1,64,512]{3,2,1,0:T(8,128)(2,1)S(1)} %bitcast.38), channel_id=1, source_target_pairs={{0,1},{1,0},{2,3},{3,2},{4,5},{5,4},{6,7},{7,6},{8,9},{9,8},{10,11... | collective-permute-start | bytes 3145736 | tf_op jit(solution)/shard_map/ppermute | solution.py:33
  85.7 23.7 %all-to-all-start.1 = ((bf16[16,128,256]{2,1,0:T(8,128)(2,1)}), bf16[16,128,256]{2,1,0:T(8,128)(2,1)S(1)}, u32[]{:S(2)}, u32[]{:S(2)}) async-start(bf16[16,128,256]{2,1,0:T(8,128)(2,1)} %broadcast_in_dim.4), calls=%async_computation.1 | async-start | bytes 2097152 | tf_op jit(solution)/shard_map/all_to_all | solution.py:49
  110.8 6.9 %collective-permute-start.3 = (bf16[256,2048]{1,0:T(8,128)(2,1)}, bf16[256,2048]{1,0:T(8,128)(2,1)}, u32[]{:S(2)}, u32[]{:S(2)}) collective-permute-start(bf16[256,2048]{1,0:T(8,128)(2,1)} %convolution_convert_fusion), channel_id=1, source_target_pairs={{0,1},{1,0},{2,3},{3,2},{4,5},{5,4},{6,7},{7,6},{8,9},{9,8},{10,11... | collective-permute-start | bytes 3145736 | tf_op jit(solution)/shard_map/ppermute | solution.py:33
  119.5 11.6 %collective-permute-start.6 = (bf16[2,16,2048]{2,1,0:T(8,128)(2,1)S(1)}, bf16[2,16,2048]{2,1,0:T(8,128)(2,1)S(1)}, u32[]{:S(2)}, u32[]{:S(2)}) collective-permute-start(bf16[2,16,2048]{2,1,0:T(8,128)(2,1)S(1)} %get-tuple-element.20), channel_id=1, source_target_pairs={{0,4},{1,29},{2,6},{3,31},{4,8},{5,1},{6,10},{7,3},{8,12},{9,5},{1... | collective-permute-start | bytes 393224 | tf_op jit(solution)/shard_map/ppermute | solution.py:29
  123.5 8.1 %collective-permute-start.7 = (bf16[2,16,2048]{2,1,0:T(8,128)(2,1)S(1)}, bf16[2,16,2048]{2,1,0:T(8,128)(2,1)S(1)}, u32[]{:S(2)}, u32[]{:S(2)}) collective-permute-start(bf16[2,16,2048]{2,1,0:T(8,128)(2,1)S(1)} %get-tuple-element.21), channel_id=1, source_target_pairs={{0,28},{1,5},{2,30},{3,7},{4,0},{5,9},{6,2},{7,11},{8,4},{9,13},{1... | collective-permute-start | bytes 393224 | tf_op jit(solution)/shard_map/ppermute | solution.py:29
  125.7 7.7 %collective-permute-start.4 = (bf16[4,16,2048]{2,1,0:T(8,128)(2,1)S(1)}, bf16[4,16,2048]{2,1,0:T(8,128)(2,1)S(1)}, u32[]{:S(2)}, u32[]{:S(2)}) collective-permute-start(bf16[4,16,2048]{2,1,0:T(8,128)(2,1)S(1)} %get-tuple-element.22), channel_id=1, source_target_pairs={{0,2},{1,31},{2,4},{3,1},{4,6},{5,3},{6,8},{7,5},{8,10},{9,7},{10,... | collective-permute-start | bytes 786440 | tf_op jit(solution)/shard_map/ppermute | solution.py:29
  128.3 10.9 %collective-permute-start.5 = (bf16[4,16,2048]{2,1,0:T(8,128)(2,1)S(1)}, bf16[4,16,2048]{2,1,0:T(8,128)(2,1)S(1)}, u32[]{:S(2)}, u32[]{:S(2)}) collective-permute-start(bf16[4,16,2048]{2,1,0:T(8,128)(2,1)S(1)} %get-tuple-element.23), channel_id=1, source_target_pairs={{0,30},{1,3},{2,0},{3,5},{4,2},{5,7},{6,4},{7,9},{8,6},{9,11},{10,... | collective-permute-start | bytes 786440 | tf_op jit(solution)/shard_map/ppermute | solution.py:29

commit v9 on v6

--- a/solution.py
+++ b/solution.py
@@ -37,10 +37,6 @@
     return lax.ppermute(x, "c", [(0, 1), (1, 0)])
 
 
-def by_core(c, mine, other, dim):
-    return jnp.concatenate([jnp.where(c == 0, mine, other), jnp.where(c == 0, other, mine)], axis=dim)
-
-
 def row_major(x):
     return with_layout_constraint(x, Layout(major_to_minor=tuple(range(x.ndim))))
 
@@ -54,18 +50,17 @@
     c = lax.axis_index("c")
     x = (tokens.T.astype(F32) * SCALE).astype(jnp.float16)
     mine = lax.all_gather(x, TP[:2])[:, None]
+    mine = lax.optimization_barrier((mine.astype(F32) / SCALE).astype(BF))
     other = swap(mine)
-    mine, other = ((v.astype(F32) / SCALE).astype(BF) for v in (mine, other))
     whole = put(jnp.zeros((16, 2, 64, 512), BF), mine, (0, c, 0, 0))
     return put(whole, other, (0, 1 - c, 0, 0)).reshape(D, 512)
 
 
-def place_down(down_train):
-    c = lax.axis_index("c")
+def gather_down(down_train):
     x = down_train.astype(BF).T
-    keep, give = jnp.where(c == 0, x[:, :256], x[:, 256:]), jnp.where(c == 0, x[:, 256:], x[:, :256])
-    x = by_core(c, keep, swap(give), 0)
-    return lax.ppermute(x, FS_TP[:3], [(a * 16 + b, b * 16 + a) for a, b in EVERY])
+    x = lax.ppermute(x, FS_TP[:3], [(a * 16 + b, b * 16 + a) for a, b in EVERY])
+    x = jnp.broadcast_to(jnp.stack([x[:, :256], x[:, 256:]]), (16, 2, 64, 256)).reshape(32, 64, 256)
+    return row_major(lax.all_to_all(row_major(x), ("fs", "c"), 0, 0, tiled=True)).reshape(D, 256)
 
 
 def scatter_sum(hidden, down, ready):
@@ -82,7 +77,8 @@
     near += fan(one, 1).astype(F32) + fan(two, -1).astype(F32)
     one = fan(part_of(far, 2 * c, 2, 0), 2)
     two = fan(part_of(far, 2 - 2 * c, 2, 0), -2)
-    far = by_core(c, one, two, 0)
+    half = lax.broadcasted_iota(jnp.int32, (2, 1, 1, 1), 0)
+    far = jnp.where(half == c, one[None], two[None]).reshape(4, 16, D)
     near, ready = lax.optimization_barrier(((near + far.astype(F32)).astype(BF), ready))
     rows = lax.all_to_all(near, "zh", 0, 0, tiled=True)
     return (*ready, jnp.sum(rows.astype(F32), axis=0).astype(BF))
@@ -92,7 +88,7 @@
     gate_local = (norm_gain[:, None] * gate_train).astype(BF)
     up_local = (norm_gain[:, None] * up_train).astype(BF)
     both = spread(jnp.concatenate([gate_local, up_local], axis=1))
-    down = spread(place_down(down_train))
+    down = gather_down(down_train)
     x = gather_tokens(tokens)
     wide = x.astype(F32)
     scale = lax.rsqrt(jnp.sum(wide * wide, axis=0) / D + EPS)[:, None]

time: 158 us -> 152 us (0.962)
  the two profiles are of different devices: /device:TPU:1 before, /device:TPU:64 now
where the time goes in v9:
time: 152 us
  blocking collectives  64.5 us (42%)
  starting transfers between devices  47 us (31%)
  waiting for transfers between devices  23.5 us (15%)
  local copies, waits for them, and re-layouts  8.98 us (6%)
  matrix products  3.8 us (2%)
  other arithmetic  2.98 us (2%)
    all_gather x1, blocking collectives, gather_tokens(): mine = lax.all_gather(x, TP[:2])[:, None]  39.1 us
    all_to_all x1, blocking collectives, scatter_sum(): rows = lax.all_to_all(near, 'zh', 0, 0, tiled=True)  25.4 us
    ppermute x4, starting transfers between devices, fan(): return lax.ppermute(x, TP, pairs)  15.5 us
    all_to_all x1, waiting for transfers between devices, gather_down(): lax.all_to_all(row_major(x), ('fs', 'c'), 0, 0, tiled=True)  13.5 us
    all_to_all x1, starting transfers between devices, gather_down(): lax.all_to_all(row_major(x), ('fs', 'c'), 0, 0, tiled=True)  13 us
    ppermute x1, starting transfers between devices, gather_down(): x = lax.ppermute(x, FS_TP[:3], [(a * 16 + b, b * 16 + a) for a, b in EVERY])  7.4 us
    all_to_all x1, starting transfers between devices, spread(): lax.all_to_all(every, 'fs', 0, 0, tiled=True)  7.22 us
    ppermute x1, waiting for transfers between devices, gather_down(): x = lax.ppermute(x, FS_TP[:3], [(a * 16 + b, b * 16 + a) for a, b in EVERY])  5.84 us
  transfers between devices with their start and end apart: 9, of which 4 were waited for; matrix products, arithmetic and copies ran while one was open for 7% of the time, Pallas kernels for 0%

profile of v9, /device:TPU:64, one launch (start us, length us, event | category | flops | bytes accessed | tf_op | source)
XLA Modules:
  0.0 151.7 jit_solution(9513358399799215044)
XLA Ops:
  0.6 1.1 multiply_convert_fusion.2
  1.7 1.5 broadcast_in_dim.48
  3.2 0.0 copy-start.1
  3.2 7.2 %all-to-all-start = ((bf16[16,128,512]{2,1,0:T(8,128)(2,1)}), bf16[16,128,512]{2,1,0:T(8,128)(2,1)}, u32[]{:S(2)}, u32[]{:S(2)}) async-start(bf16[16,128,512]{2,1,0:T(8,128)(2,1)} %broadcast_in_dim.48), calls=%async_computation | async-start | bytes 4194304 | tf_op jit(solution)/shard_map/all_to_all | solution.py:46
  10.5 0.0 copy-done.1
  10.5 0.0 copy-start
  10.5 39.1 %all-gather.2 = f16[1024,512]{1,0:T(8,128)(2,1)S(1)} all-gather(f16[64,512]{1,0:T(8,128)(2,1)S(1)} %fusion.4), channel_id=2, replica_groups=mesh['fs'=16,'zh'=4,'zl'=4,'c'=2] {'zh','zl'}, dimensions={0}, use_global_device_ids=true | all-gather | bytes 1114112 | tf_op jit(solution)/shard_map/all_gather | solution.py:52
  49.7 0.2 multiply_convert_fusion
  49.9 1.9 %collective-permute-start = (bf16[16,1,64,512]{3,2,1,0:T(8,128)(2,1)S(1)}, bf16[16,1,64,512]{3,2,1,0:T(8,128)(2,1)}, u32[]{:S(2)}, u32[]{:S(2)}) collective-permute-start(bf16[16,1,64,512]{3,2,1,0:T(8,128)(2,1)S(1)} %bitcast.48), channel_id=1, source_target_pairs={{0,1},{1,0},{2,3},{3,2},{4,5},{5,4},{6,7},{7,6},{8,9},{9,8},{10,11... | collective-permute-start | bytes 3145736 | tf_op jit(solution)/shard_map/ppermute | solution.py:37
  51.8 0.0 copy-done
  51.8 7.4 %collective-permute-start.1 = (bf16[64,512]{1,0:T(8,128)(2,1)S(1)}, bf16[64,512]{1,0:T(8,128)(2,1)S(1)}, u32[]{:S(2)}, u32[]{:S(2)}) collective-permute-start(bf16[64,512]{1,0:T(8,128)(2,1)S(1)} %convert_bitcast_fusion), channel_id=1, source_target_pairs={{0,0},{2,32},{4,64},{6,96},{8,128},{10,160},{12,192},{14,224},{16,... | collective-permute-start | bytes 196616 | tf_op jit(solution)/shard_map/ppermute | solution.py:61
  59.2 0.2 broadcast_in_dim.47
  59.5 0.1 constant_dynamic-update-slice_fusion.1
  59.6 5.8 %collective-permute-done.1 = bf16[64,512]{1,0:T(8,128)(2,1)S(1)} collective-permute-done((bf16[64,512]{1,0:T(8,128)(2,1)S(1)}, bf16[64,512]{1,0:T(8,128)(2,1)S(1)}, u32[]{:S(2)}, u32[]{:S(2)}) %collective-permute-start.1) | collective-permute-done | bytes 65568 | tf_op jit(solution)/shard_map/ppermute | solution.py:61
  65.4 0.0 collective-permute-done
  65.5 1.3 constant_dynamic-update-slice_fusion
  66.8 0.0 all-to-all-done
  66.8 1.1 broadcast_in_dim.49
  67.9 13.0 %all-to-all-start.1 = ((bf16[32,64,256]{2,1,0:T(8,128)(2,1)}), bf16[32,64,256]{2,1,0:T(8,128)(2,1)S(1)}, u32[]{:S(2)}, u32[]{:S(2)}) async-start(bf16[32,64,256]{2,1,0:T(8,128)(2,1)} %bitcast.50), calls=%async_computation.1 | async-start | bytes 2097152 | tf_op jit(solution)/shard_map/all_to_all | solution.py:63
  80.9 0.6 multiply_reduce_fusion
  81.4 2.9 %fusion.6 = f32[512,512]{1,0:T(8,128)S(1)} fusion(bf16[2048,512]{1,0:T(8,128)(2,1)S(1)} %bitcast.44, bf16[2048,512]{1,0:T(8,128)(2,1)} %bitcast.3), kind=kOutput, calls=%fused_computation.32 | convolution fusion | flops 1073741824 | bytes 5242880 | tf_op jit(solution)/shard_map/dot_general | solution.py:95
  84.3 0.2 fusion.1
  84.6 13.5 %all-to-all-done.1 = bf16[32,64,256]{2,1,0:T(8,128)(2,1)S(1)} async-done(((bf16[32,64,256]{2,1,0:T(8,128)(2,1)}), bf16[32,64,256]{2,1,0:T(8,128)(2,1)S(1)}, u32[]{:S(2)}, u32[]{:S(2)}) %all-to-all-start.1) | async-done | bytes 1048608 | tf_op jit(solution)/shard_map/all_to_all | solution.py:63
  98.1 0.5 convolution_convert_fusion
  98.6 2.0 %collective-permute-start.2 = (bf16[256,2048]{1,0:T(8,128)(2,1)S(1)}, bf16[256,2048]{1,0:T(8,128)(2,1)S(1)}, u32[]{:S(2)}, u32[]{:S(2)}) collective-permute-start(bf16[256,2048]{1,0:T(8,128)(2,1)S(1)} %convolution_convert_fusion), channel_id=1, source_target_pairs={{0,1},{1,0},{2,3},{3,2},{4,5},{5,4},{6,7},{7,6},{8,9},{9,8},{10,11... | collective-permute-start | bytes 3145736 | tf_op jit(solution)/shard_map/ppermute | solution.py:37
  100.6 0.1 broadcast_in_dim.50
  100.7 0.1 broadcast_in_dim.51
  100.8 1.4 copy.10
  102.2 0.9 collective-permute-done.2
  103.1 0.5 add_convert_fusion
  103.6 0.1 dynamic-slice_bitcast_fusion.1
  103.6 2.0 %collective-permute-start.3 = (bf16[4,16,2048]{2,1,0:T(8,128)(2,1)S(1)}, bf16[4,16,2048]{2,1,0:T(8,128)(2,1)S(1)}, u32[]{:S(2)}, u32[]{:S(2)}) collective-permute-start(bf16[4,16,2048]{2,1,0:T(8,128)(2,1)S(1)} %get-tuple-element.16), channel_id=1, source_target_pairs={{0,2},{1,31},{2,4},{3,1},{4,6},{5,3},{6,8},{7,5},{8,10},{9,7},{10,... | collective-permute-start | bytes 786440 | tf_op jit(solution)/shard_map/ppermute | solution.py:33
  105.6 3.9 %collective-permute-start.4 = (bf16[4,16,2048]{2,1,0:T(8,128)(2,1)S(1)}, bf16[4,16,2048]{2,1,0:T(8,128)(2,1)S(1)}, u32[]{:S(2)}, u32[]{:S(2)}) collective-permute-start(bf16[4,16,2048]{2,1,0:T(8,128)(2,1)S(1)} %get-tuple-element.17), channel_id=1, source_target_pairs={{0,30},{1,3},{2,0},{3,5},{4,2},{5,7},{6,4},{7,9},{8,6},{9,11},{10,... | collective-permute-start | bytes 786440 | tf_op jit(solution)/shard_map/ppermute | solution.py:33
  109.5 6.8 %collective-permute-start.5 = (bf16[2,16,2048]{2,1,0:T(8,128)(2,1)S(1)}, bf16[2,16,2048]{2,1,0:T(8,128)(2,1)S(1)}, u32[]{:S(2)}, u32[]{:S(2)}) collective-permute-start(bf16[2,16,2048]{2,1,0:T(8,128)(2,1)S(1)} %get-tuple-element.14), channel_id=1, source_target_pairs={{0,4},{1,29},{2,6},{3,31},{4,8},{5,1},{6,10},{7,3},{8,12},{9,5},{1... | collective-permute-start | bytes 393224 | tf_op jit(solution)/shard_map/ppermute | solution.py:33
  116.4 2.8 %collective-permute-start.6 = (bf16[2,16,2048]{2,1,0:T(8,128)(2,1)S(1)}, bf16[2,16,2048]{2,1,0:T(8,128)(2,1)S(1)}, u32[]{:S(2)}, u32[]{:S(2)}) collective-permute-start(bf16[2,16,2048]{2,1,0:T(8,128)(2,1)S(1)} %get-tuple-element.15), channel_id=1, source_target_pairs={{0,28},{1,5},{2,30},{3,7},{4,0},{5,9},{6,2},{7,11},{8,4},{9,13},{1... | collective-permute-start | bytes 393224 | tf_op jit(solution)/shard_map/ppermute | solution.py:33
  119.2 3.0 %fusion.5 = (bf16[2048,256]{1,0:T(8,128)(2,1)}, bf16[2048,256]{1,0:T(8,128)(2,1)}) fusion(bf16[2048,512]{1,0:T(8,128)(2,1)} %bitcast.3), kind=kLoop, calls=%fused_computation.31 | loop fusion | bytes 4194304 | tf_op jit(solution)/shard_map/slice | solution.py:98
  122.2 0.0 collective-permute-done.5
  122.2 3.2 %collective-permute-done.6 = bf16[2,16,2048]{2,1,0:T(8,128)(2,1)S(1)} collective-permute-done((bf16[2,16,2048]{2,1,0:T(8,128)(2,1)S(1)}, bf16[2,16,2048]{2,1,0:T(8,128)(2,1)S(1)}, u32[]{:S(2)}, u32[]{:S(2)}) %collective-permute-start.6) | collective-permute-done | bytes 131104 | tf_op jit(solution)/shard_map/ppermute | solution.py:33
  125.4 0.0 collective-permute-done.3
  125.4 0.0 collective-permute-done.4
  125.4 0.2 fusion.3
  125.6 25.4 %all_to_all.15 = bf16[4,16,2048]{2,1,0:T(8,128)(2,1)S(1)} all-to-all(bf16[4,16,2048]{2,1,0:T(8,128)(2,1)S(1)} %fusion.3), channel_id=1, replica_groups=mesh['fs'=16,'zh'=4,'zl'=4,'c'=2] {'zh'}, dimensions={0} | all-to-all | bytes 524288 | tf_op jit(solution)/shard_map/all_to_all | solution.py:83
  151.0 0.7 reduce_sum.22
  (9 shorter events, 0.1 us)
Async XLA Ops:
  3.2 7.2 %copy-start.1 = (bf16[512,64]{0,1:T(8,128)(2,1)S(1)}, bf16[512,64]{0,1:T(8,128)(2,1)}, u32[]{:S(2)}) copy-start(bf16[512,64]{0,1:T(8,128)(2,1)} %param.5) | copy-start | bytes 196612
  3.2 63.6 %all-to-all-start = ((bf16[16,128,512]{2,1,0:T(8,128)(2,1)}), bf16[16,128,512]{2,1,0:T(8,128)(2,1)}, u32[]{:S(2)}, u32[]{:S(2)}) async-start(bf16[16,128,512]{2,1,0:T(8,128)(2,1)} %broadcast_in_dim.48), calls=%async_computation | async-start | bytes 4194304 | tf_op jit(solution)/shard_map/all_to_all | solution.py:46
  10.5 41.3 %copy-start = (f32[512,64]{0,1:T(8,128)S(1)}, f32[512,64]{0,1:T(8,128)}, u32[]{:S(2)}) copy-start(f32[512,64]{0,1:T(8,128)} %param.9) | copy-start | bytes 393220
  49.9 15.6 %collective-permute-start = (bf16[16,1,64,512]{3,2,1,0:T(8,128)(2,1)S(1)}, bf16[16,1,64,512]{3,2,1,0:T(8,128)(2,1)}, u32[]{:S(2)}, u32[]{:S(2)}) collective-permute-start(bf16[16,1,64,512]{3,2,1,0:T(8,128)(2,1)S(1)} %bitcast.48), channel_id=1, source_target_pairs={{0,1},{1,0},{2,3},{3,2},{4,5},{5,4},{6,7},{7,6},{8,9},{9,8},{10,11... | collective-permute-start | bytes 3145736 | tf_op jit(solution)/shard_map/ppermute | solution.py:37
  51.8 13.6 %collective-permute-start.1 = (bf16[64,512]{1,0:T(8,128)(2,1)S(1)}, bf16[64,512]{1,0:T(8,128)(2,1)S(1)}, u32[]{:S(2)}, u32[]{:S(2)}) collective-permute-start(bf16[64,512]{1,0:T(8,128)(2,1)S(1)} %convert_bitcast_fusion), channel_id=1, source_target_pairs={{0,0},{2,32},{4,64},{6,96},{8,128},{10,160},{12,192},{14,224},{16,... | collective-permute-start | bytes 196616 | tf_op jit(solution)/shard_map/ppermute | solution.py:61
  67.9 30.2 %all-to-all-start.1 = ((bf16[32,64,256]{2,1,0:T(8,128)(2,1)}), bf16[32,64,256]{2,1,0:T(8,128)(2,1)S(1)}, u32[]{:S(2)}, u32[]{:S(2)}) async-start(bf16[32,64,256]{2,1,0:T(8,128)(2,1)} %bitcast.50), calls=%async_computation.1 | async-start | bytes 2097152 | tf_op jit(solution)/shard_map/all_to_all | solution.py:63
  98.6 4.6 %collective-permute-start.2 = (bf16[256,2048]{1,0:T(8,128)(2,1)S(1)}, bf16[256,2048]{1,0:T(8,128)(2,1)S(1)}, u32[]{:S(2)}, u32[]{:S(2)}) collective-permute-start(bf16[256,2048]{1,0:T(8,128)(2,1)S(1)} %convolution_convert_fusion), channel_id=1, source_target_pairs={{0,1},{1,0},{2,3},{3,2},{4,5},{5,4},{6,7},{7,6},{8,9},{9,8},{10,11... | collective-permute-start | bytes 3145736 | tf_op jit(solution)/shard_map/ppermute | solution.py:37
  103.6 21.8 %collective-permute-start.3 = (bf16[4,16,2048]{2,1,0:T(8,128)(2,1)S(1)}, bf16[4,16,2048]{2,1,0:T(8,128)(2,1)S(1)}, u32[]{:S(2)}, u32[]{:S(2)}) collective-permute-start(bf16[4,16,2048]{2,1,0:T(8,128)(2,1)S(1)} %get-tuple-element.16), channel_id=1, source_target_pairs={{0,2},{1,31},{2,4},{3,1},{4,6},{5,3},{6,8},{7,5},{8,10},{9,7},{10,... | collective-permute-start | bytes 786440 | tf_op jit(solution)/shard_map/ppermute | solution.py:33
  105.6 19.8 %collective-permute-start.4 = (bf16[4,16,2048]{2,1,0:T(8,128)(2,1)S(1)}, bf16[4,16,2048]{2,1,0:T(8,128)(2,1)S(1)}, u32[]{:S(2)}, u32[]{:S(2)}) collective-permute-start(bf16[4,16,2048]{2,1,0:T(8,128)(2,1)S(1)} %get-tuple-element.17), channel_id=1, source_target_pairs={{0,30},{1,3},{2,0},{3,5},{4,2},{5,7},{6,4},{7,9},{8,6},{9,11},{10,... | collective-permute-start | bytes 786440 | tf_op jit(solution)/shard_map/ppermute | solution.py:33
  109.5 12.7 %collective-permute-start.5 = (bf16[2,16,2048]{2,1,0:T(8,128)(2,1)S(1)}, bf16[2,16,2048]{2,1,0:T(8,128)(2,1)S(1)}, u32[]{:S(2)}, u32[]{:S(2)}) collective-permute-start(bf16[2,16,2048]{2,1,0:T(8,128)(2,1)S(1)} %get-tuple-element.14), channel_id=1, source_target_pairs={{0,4},{1,29},{2,6},{3,31},{4,8},{5,1},{6,10},{7,3},{8,12},{9,5},{1... | collective-permute-start | bytes 393224 | tf_op jit(solution)/shard_map/ppermute | solution.py:33
  116.4 9.0 %collective-permute-start.6 = (bf16[2,16,2048]{2,1,0:T(8,128)(2,1)S(1)}, bf16[2,16,2048]{2,1,0:T(8,128)(2,1)S(1)}, u32[]{:S(2)}, u32[]{:S(2)}) collective-permute-start(bf16[2,16,2048]{2,1,0:T(8,128)(2,1)S(1)} %get-tuple-element.15), channel_id=1, source_target_pairs={{0,28},{1,5},{2,30},{3,7},{4,0},{5,9},{6,2},{7,11},{8,4},{9,13},{1... | collective-permute-start | bytes 393224 | tf_op jit(solution)/shard_map/ppermute | solution.py:33

commit v10 on v6

--- a/solution.py
+++ b/solution.py
@@ -54,8 +54,8 @@
     c = lax.axis_index("c")
     x = (tokens.T.astype(F32) * SCALE).astype(jnp.float16)
     mine = lax.all_gather(x, TP[:2])[:, None]
+    mine = lax.optimization_barrier((mine.astype(F32) / SCALE).astype(BF))
     other = swap(mine)
-    mine, other = ((v.astype(F32) / SCALE).astype(BF) for v in (mine, other))
     whole = put(jnp.zeros((16, 2, 64, 512), BF), mine, (0, c, 0, 0))
     return put(whole, other, (0, 1 - c, 0, 0)).reshape(D, 512)
 
@@ -82,7 +82,8 @@
     near += fan(one, 1).astype(F32) + fan(two, -1).astype(F32)
     one = fan(part_of(far, 2 * c, 2, 0), 2)
     two = fan(part_of(far, 2 - 2 * c, 2, 0), -2)
-    far = by_core(c, one, two, 0)
+    half = lax.broadcasted_iota(jnp.int32, (2, 1, 1, 1), 0)
+    far = jnp.where(half == c, one[None], two[None]).reshape(4, 16, D)
     near, ready = lax.optimization_barrier(((near + far.astype(F32)).astype(BF), ready))
     rows = lax.all_to_all(near, "zh", 0, 0, tiled=True)
     return (*ready, jnp.sum(rows.astype(F32), axis=0).astype(BF))

time: 158 us -> 156 us (0.987)
  the two profiles are of different devices: /device:TPU:1 before, /device:TPU:33 now
where the time goes in v10:
time: 156 us; the launch traced here: 155 us
  blocking collectives  61.7 us (40%)
  starting transfers between devices  58 us (37%)
  waiting for transfers between devices  18.8 us (12%)
  local copies, waits for them, and re-layouts  8.97 us (6%)
  matrix products  3.79 us (2%)
  other arithmetic  3 us (2%)
    all_gather x1, blocking collectives, gather_tokens(): mine = lax.all_gather(x, TP[:2])[:, None]  35.1 us
    all_to_all x1, blocking collectives, scatter_sum(): rows = lax.all_to_all(near, 'zh', 0, 0, tiled=True)  26.6 us
    all_to_all x2, starting transfers between devices, spread(): lax.all_to_all(every, 'fs', 0, 0, tiled=True)  24.8 us
    ppermute x3, starting transfers between devices, swap(): return lax.ppermute(x, 'c', [(0, 1), (1, 0)])  14.5 us
    ppermute x4, starting transfers between devices, fan(): return lax.ppermute(x, TP, pairs)  13.5 us
    all_to_all x2, waiting for transfers between devices, spread(): lax.all_to_all(every, 'fs', 0, 0, tiled=True)  12.5 us
    ppermute x1, starting transfers between devices, place_down(): lax.ppermute(x, FS_TP[:3], [(a * 16 + b, b * 16 + a) for a, b in EVERY])  5.25 us
    ppermute x4, waiting for transfers between devices, fan(): return lax.ppermute(x, TP, pairs)  4.48 us
  transfers between devices with their start and end apart: 10, of which 5 were waited for; matrix products, arithmetic and copies ran while one was open for 7% of the time, Pallas kernels for 0%

profile of v10, /device:TPU:33, one launch (start us, length us, event | category | flops | bytes accessed | tf_op | source)
XLA Modules:
  0.0 155.2 jit_solution(16809108134928641373)
XLA Ops:
  0.6 1.1 multiply_convert_fusion.2
  1.7 1.5 broadcast_in_dim.48
  3.3 0.0 copy-start.1
  3.3 6.9 %all-to-all-start = ((bf16[16,128,512]{2,1,0:T(8,128)(2,1)}), bf16[16,128,512]{2,1,0:T(8,128)(2,1)}, u32[]{:S(2)}, u32[]{:S(2)}) async-start(bf16[16,128,512]{2,1,0:T(8,128)(2,1)} %broadcast_in_dim.48), calls=%async_computation | async-start | bytes 4194304 | tf_op jit(solution)/shard_map/all_to_all | solution.py:50
  10.2 0.0 copy-done.1
  10.2 0.0 copy-start
  10.2 35.1 %all-gather.2 = f16[1024,512]{1,0:T(8,128)(2,1)S(1)} all-gather(f16[64,512]{1,0:T(8,128)(2,1)S(1)} %fusion.5), channel_id=2, replica_groups=mesh['fs'=16,'zh'=4,'zl'=4,'c'=2] {'zh','zl'}, dimensions={0}, use_global_device_ids=true | all-gather | bytes 1114112 | tf_op jit(solution)/shard_map/all_gather | solution.py:56
  45.3 0.2 multiply_convert_fusion
  45.6 7.7 %collective-permute-start = (bf16[16,1,64,512]{3,2,1,0:T(8,128)(2,1)S(1)}, bf16[16,1,64,512]{3,2,1,0:T(8,128)(2,1)}, u32[]{:S(2)}, u32[]{:S(2)}) collective-permute-start(bf16[16,1,64,512]{3,2,1,0:T(8,128)(2,1)S(1)} %bitcast.43), channel_id=1, source_target_pairs={{0,1},{1,0},{2,3},{3,2},{4,5},{5,4},{6,7},{7,6},{8,9},{9,8},{10,11... | collective-permute-start | bytes 3145736 | tf_op jit(solution)/shard_map/ppermute | solution.py:37
  53.3 0.0 copy-done
  53.3 1.9 %collective-permute-start.1 = (bf16[64,256]{1,0:T(8,128)(2,1)S(1)}, bf16[64,256]{1,0:T(8,128)(2,1)S(1)}, u32[]{:S(2)}, u32[]{:S(2)}) collective-permute-start(bf16[64,256]{1,0:T(8,128)(2,1)S(1)} %broadcast_select_fusion.2), channel_id=1, source_target_pairs={{0,1},{1,0},{2,3},{3,2},{4,5},{5,4},{6,7},{7,6},{8,9},{9,8},{10,11... | collective-permute-start | bytes 98312 | tf_op jit(solution)/shard_map/ppermute | solution.py:37
  55.3 0.2 broadcast_in_dim.47
  55.5 0.1 constant_dynamic-update-slice_fusion.1
  55.6 0.8 collective-permute-done.1
  56.5 5.3 %collective-permute-start.2 = (bf16[128,256]{1,0:T(8,128)(2,1)S(1)}, bf16[128,256]{1,0:T(8,128)(2,1)S(1)}, u32[]{:S(2)}, u32[]{:S(2)}) collective-permute-start(bf16[128,256]{1,0:T(8,128)(2,1)S(1)} %pad_maximum_fusion.1), channel_id=1, source_target_pairs={{0,0},{2,32},{4,64},{6,96},{8,128},{10,160},{12,192},{14,224},{16,... | collective-permute-start | bytes 196616 | tf_op jit(solution)/shard_map/ppermute | solution.py:68
  61.7 0.0 collective-permute-done
  61.7 1.3 constant_dynamic-update-slice_fusion
  63.1 0.6 multiply_reduce_fusion
  63.6 0.4 collective-permute-done.2
  64.0 0.0 all-to-all-done
  64.0 1.1 broadcast_in_dim.49
  65.1 17.9 %all-to-all-start.1 = ((bf16[16,128,256]{2,1,0:T(8,128)(2,1)}), bf16[16,128,256]{2,1,0:T(8,128)(2,1)S(1)}, u32[]{:S(2)}, u32[]{:S(2)}) async-start(bf16[16,128,256]{2,1,0:T(8,128)(2,1)} %broadcast_in_dim.49), calls=%async_computation.1 | async-start | bytes 2097152 | tf_op jit(solution)/shard_map/all_to_all | solution.py:50
  83.0 2.9 %fusion.7 = f32[512,512]{1,0:T(8,128)S(1)} fusion(bf16[2048,512]{1,0:T(8,128)(2,1)S(1)} %bitcast.39, bf16[2048,512]{1,0:T(8,128)(2,1)} %bitcast.3), kind=kOutput, calls=%fused_computation.35 | convolution fusion | flops 1073741824 | bytes 5242880 | tf_op jit(solution)/shard_map/dot_general | solution.py:100
  85.8 0.2 fusion.2
  86.1 12.5 %all-to-all-done.1 = bf16[16,128,256]{2,1,0:T(8,128)(2,1)S(1)} async-done(((bf16[16,128,256]{2,1,0:T(8,128)(2,1)}), bf16[16,128,256]{2,1,0:T(8,128)(2,1)S(1)}, u32[]{:S(2)}, u32[]{:S(2)}) %all-to-all-start.1) | async-done | bytes 1048608 | tf_op jit(solution)/shard_map/all_to_all | solution.py:50
  98.6 0.5 convolution_convert_fusion
  99.1 4.8 %collective-permute-start.3 = (bf16[256,2048]{1,0:T(8,128)(2,1)S(1)}, bf16[256,2048]{1,0:T(8,128)(2,1)S(1)}, u32[]{:S(2)}, u32[]{:S(2)}) collective-permute-start(bf16[256,2048]{1,0:T(8,128)(2,1)S(1)} %convolution_convert_fusion), channel_id=1, source_target_pairs={{0,1},{1,0},{2,3},{3,2},{4,5},{5,4},{6,7},{7,6},{8,9},{9,8},{10,11... | collective-permute-start | bytes 3145736 | tf_op jit(solution)/shard_map/ppermute | solution.py:37
  103.9 0.1 broadcast_in_dim.50
  104.0 0.1 broadcast_in_dim.51
  104.1 1.4 copy.10
  105.5 0.7 collective-permute-done.3
  106.2 0.5 fusion
  106.6 0.1 dynamic-slice_bitcast_fusion.1
  106.7 5.3 %collective-permute-start.4 = (bf16[4,16,2048]{2,1,0:T(8,128)(2,1)S(1)}, bf16[4,16,2048]{2,1,0:T(8,128)(2,1)S(1)}, u32[]{:S(2)}, u32[]{:S(2)}) collective-permute-start(bf16[4,16,2048]{2,1,0:T(8,128)(2,1)S(1)} %get-tuple-element.16), channel_id=1, source_target_pairs={{0,2},{1,31},{2,4},{3,1},{4,6},{5,3},{6,8},{7,5},{8,10},{9,7},{10,... | collective-permute-start | bytes 786440 | tf_op jit(solution)/shard_map/ppermute | solution.py:33
  112.0 1.9 %collective-permute-start.5 = (bf16[4,16,2048]{2,1,0:T(8,128)(2,1)S(1)}, bf16[4,16,2048]{2,1,0:T(8,128)(2,1)S(1)}, u32[]{:S(2)}, u32[]{:S(2)}) collective-permute-start(bf16[4,16,2048]{2,1,0:T(8,128)(2,1)S(1)} %get-tuple-element.17), channel_id=1, source_target_pairs={{0,30},{1,3},{2,0},{3,5},{4,2},{5,7},{6,4},{7,9},{8,6},{9,11},{10,... | collective-permute-start | bytes 786440 | tf_op jit(solution)/shard_map/ppermute | solution.py:33
  114.0 4.3 %collective-permute-start.6 = (bf16[2,16,2048]{2,1,0:T(8,128)(2,1)S(1)}, bf16[2,16,2048]{2,1,0:T(8,128)(2,1)S(1)}, u32[]{:S(2)}, u32[]{:S(2)}) collective-permute-start(bf16[2,16,2048]{2,1,0:T(8,128)(2,1)S(1)} %get-tuple-element.14), channel_id=1, source_target_pairs={{0,4},{1,29},{2,6},{3,31},{4,8},{5,1},{6,10},{7,3},{8,12},{9,5},{1... | collective-permute-start | bytes 393224 | tf_op jit(solution)/shard_map/ppermute | solution.py:33
  118.3 1.9 %collective-permute-start.7 = (bf16[2,16,2048]{2,1,0:T(8,128)(2,1)S(1)}, bf16[2,16,2048]{2,1,0:T(8,128)(2,1)S(1)}, u32[]{:S(2)}, u32[]{:S(2)}) collective-permute-start(bf16[2,16,2048]{2,1,0:T(8,128)(2,1)S(1)} %get-tuple-element.15), channel_id=1, source_target_pairs={{0,28},{1,5},{2,30},{3,7},{4,0},{5,9},{6,2},{7,11},{8,4},{9,13},{1... | collective-permute-start | bytes 393224 | tf_op jit(solution)/shard_map/ppermute | solution.py:33
  120.2 3.0 %fusion.6 = (bf16[2048,256]{1,0:T(8,128)(2,1)}, bf16[2048,256]{1,0:T(8,128)(2,1)}) fusion(bf16[2048,512]{1,0:T(8,128)(2,1)} %bitcast.3), kind=kLoop, calls=%fused_computation.34 | loop fusion | bytes 4194304 | tf_op jit(solution)/shard_map/slice | solution.py:103
  123.2 0.0 collective-permute-done.6
  123.2 4.5 %collective-permute-done.7 = bf16[2,16,2048]{2,1,0:T(8,128)(2,1)S(1)} collective-permute-done((bf16[2,16,2048]{2,1,0:T(8,128)(2,1)S(1)}, bf16[2,16,2048]{2,1,0:T(8,128)(2,1)S(1)}, u32[]{:S(2)}, u32[]{:S(2)}) %collective-permute-start.7) | collective-permute-done | bytes 131104 | tf_op jit(solution)/shard_map/ppermute | solution.py:33
  127.7 0.0 collective-permute-done.4
  127.7 0.0 collective-permute-done.5
  127.7 0.2 fusion.4
  127.9 26.6 %all_to_all.15 = bf16[4,16,2048]{2,1,0:T(8,128)(2,1)S(1)} all-to-all(bf16[4,16,2048]{2,1,0:T(8,128)(2,1)S(1)} %fusion.4), channel_id=1, replica_groups=mesh['fs'=16,'zh'=4,'zl'=4,'c'=2] {'zh'}, dimensions={0} | all-to-all | bytes 524288 | tf_op jit(solution)/shard_map/all_to_all | solution.py:88
  154.5 0.7 reduce_sum.22
  (10 shorter events, 0.1 us)
Async XLA Ops:
  3.3 6.9 %copy-start.1 = (bf16[512,64]{0,1:T(8,128)(2,1)S(1)}, bf16[512,64]{0,1:T(8,128)(2,1)}, u32[]{:S(2)}) copy-start(bf16[512,64]{0,1:T(8,128)(2,1)} %param.5) | copy-start | bytes 196612
  3.3 60.8 %all-to-all-start = ((bf16[16,128,512]{2,1,0:T(8,128)(2,1)}), bf16[16,128,512]{2,1,0:T(8,128)(2,1)}, u32[]{:S(2)}, u32[]{:S(2)}) async-start(bf16[16,128,512]{2,1,0:T(8,128)(2,1)} %broadcast_in_dim.48), calls=%async_computation | async-start | bytes 4194304 | tf_op jit(solution)/shard_map/all_to_all | solution.py:50
  10.2 43.1 %copy-start = (f32[512,64]{0,1:T(8,128)S(1)}, f32[512,64]{0,1:T(8,128)}, u32[]{:S(2)}) copy-start(f32[512,64]{0,1:T(8,128)} %param.9) | copy-start | bytes 393220
  45.6 16.2 %collective-permute-start = (bf16[16,1,64,512]{3,2,1,0:T(8,128)(2,1)S(1)}, bf16[16,1,64,512]{3,2,1,0:T(8,128)(2,1)}, u32[]{:S(2)}, u32[]{:S(2)}) collective-permute-start(bf16[16,1,64,512]{3,2,1,0:T(8,128)(2,1)S(1)} %bitcast.43), channel_id=1, source_target_pairs={{0,1},{1,0},{2,3},{3,2},{4,5},{5,4},{6,7},{7,6},{8,9},{9,8},{10,11... | collective-permute-start | bytes 3145736 | tf_op jit(solution)/shard_map/ppermute | solution.py:37
  53.3 3.1 %collective-permute-start.1 = (bf16[64,256]{1,0:T(8,128)(2,1)S(1)}, bf16[64,256]{1,0:T(8,128)(2,1)S(1)}, u32[]{:S(2)}, u32[]{:S(2)}) collective-permute-start(bf16[64,256]{1,0:T(8,128)(2,1)S(1)} %broadcast_select_fusion.2), channel_id=1, source_target_pairs={{0,1},{1,0},{2,3},{3,2},{4,5},{5,4},{6,7},{7,6},{8,9},{9,8},{10,11... | collective-permute-start | bytes 98312 | tf_op jit(solution)/shard_map/ppermute | solution.py:37
  56.5 7.6 %collective-permute-start.2 = (bf16[128,256]{1,0:T(8,128)(2,1)S(1)}, bf16[128,256]{1,0:T(8,128)(2,1)S(1)}, u32[]{:S(2)}, u32[]{:S(2)}) collective-permute-start(bf16[128,256]{1,0:T(8,128)(2,1)S(1)} %pad_maximum_fusion.1), channel_id=1, source_target_pairs={{0,0},{2,32},{4,64},{6,96},{8,128},{10,160},{12,192},{14,224},{16,... | collective-permute-start | bytes 196616 | tf_op jit(solution)/shard_map/ppermute | solution.py:68
  65.1 33.5 %all-to-all-start.1 = ((bf16[16,128,256]{2,1,0:T(8,128)(2,1)}), bf16[16,128,256]{2,1,0:T(8,128)(2,1)S(1)}, u32[]{:S(2)}, u32[]{:S(2)}) async-start(bf16[16,128,256]{2,1,0:T(8,128)(2,1)} %broadcast_in_dim.49), calls=%async_computation.1 | async-start | bytes 2097152 | tf_op jit(solution)/shard_map/all_to_all | solution.py:50
  99.1 7.1 %collective-permute-start.3 = (bf16[256,2048]{1,0:T(8,128)(2,1)S(1)}, bf16[256,2048]{1,0:T(8,128)(2,1)S(1)}, u32[]{:S(2)}, u32[]{:S(2)}) collective-permute-start(bf16[256,2048]{1,0:T(8,128)(2,1)S(1)} %convolution_convert_fusion), channel_id=1, source_target_pairs={{0,1},{1,0},{2,3},{3,2},{4,5},{5,4},{6,7},{7,6},{8,9},{9,8},{10,11... | collective-permute-start | bytes 3145736 | tf_op jit(solution)/shard_map/ppermute | solution.py:37
  106.7 21.0 %collective-permute-start.4 = (bf16[4,16,2048]{2,1,0:T(8,128)(2,1)S(1)}, bf16[4,16,2048]{2,1,0:T(8,128)(2,1)S(1)}, u32[]{:S(2)}, u32[]{:S(2)}) collective-permute-start(bf16[4,16,2048]{2,1,0:T(8,128)(2,1)S(1)} %get-tuple-element.16), channel_id=1, source_target_pairs={{0,2},{1,31},{2,4},{3,1},{4,6},{5,3},{6,8},{7,5},{8,10},{9,7},{10,... | collective-permute-start | bytes 786440 | tf_op jit(solution)/shard_map/ppermute | solution.py:33
  112.0 15.7 %collective-permute-start.5 = (bf16[4,16,2048]{2,1,0:T(8,128)(2,1)S(1)}, bf16[4,16,2048]{2,1,0:T(8,128)(2,1)S(1)}, u32[]{:S(2)}, u32[]{:S(2)}) collective-permute-start(bf16[4,16,2048]{2,1,0:T(8,128)(2,1)S(1)} %get-tuple-element.17), channel_id=1, source_target_pairs={{0,30},{1,3},{2,0},{3,5},{4,2},{5,7},{6,4},{7,9},{8,6},{9,11},{10,... | collective-permute-start | bytes 786440 | tf_op jit(solution)/shard_map/ppermute | solution.py:33
  114.0 9.2 %collective-permute-start.6 = (bf16[2,16,2048]{2,1,0:T(8,128)(2,1)S(1)}, bf16[2,16,2048]{2,1,0:T(8,128)(2,1)S(1)}, u32[]{:S(2)}, u32[]{:S(2)}) collective-permute-start(bf16[2,16,2048]{2,1,0:T(8,128)(2,1)S(1)} %get-tuple-element.14), channel_id=1, source_target_pairs={{0,4},{1,29},{2,6},{3,31},{4,8},{5,1},{6,10},{7,3},{8,12},{9,5},{1... | collective-permute-start | bytes 393224 | tf_op jit(solution)/shard_map/ppermute | solution.py:33
  118.3 9.4 %collective-permute-start.7 = (bf16[2,16,2048]{2,1,0:T(8,128)(2,1)S(1)}, bf16[2,16,2048]{2,1,0:T(8,128)(2,1)S(1)}, u32[]{:S(2)}, u32[]{:S(2)}) collective-permute-start(bf16[2,16,2048]{2,1,0:T(8,128)(2,1)S(1)} %get-tuple-element.15), channel_id=1, source_target_pairs={{0,28},{1,5},{2,30},{3,7},{4,0},{5,9},{6,2},{7,11},{8,4},{9,13},{1... | collective-permute-start | bytes 393224 | tf_op jit(solution)/shard_map/ppermute | solution.py:33
